TPU v7x, 32 devices: a whole 2x2x4 slice. The times are simulated.
32 devices in a mesh: sp: 8 (over z, y), tp: 4 (over x, core).
Axes of the slice: x: 2, y: 2, z: 4, core: 2. Of those that a mesh axis runs over, the one named last changes fastest.
Arguments:
- queries: bfloat16 [6144, 1024], P('sp', 'tp'), may hold values from -6 to 6
- keys: bfloat16 [6144, 1024], P('sp', 'tp'), may hold values from -6 to 6
- values: bfloat16 [6144, 2048], P('sp', 'tp'), may hold values from -6 to 6
- out_gate: bfloat16 [6144, 2048], P('sp', 'tp'), may hold values from -6 to 6
- input_gates: float32 [2, 4, 6144], P(None, 'tp', 'sp'), may hold values from -4 to 300
- forget_gates: float32 [2, 4, 6144], P(None, 'tp', 'sp'), may hold values from -1 to 16
- doc_ids: int32 [6144], P('sp'), may hold values from 0 to 3, never falling along the last dimension, each value on 1 to 3072 neighbouring positions
- head_gain: float32 [2048], P('tp'), may hold values from 0.1 to 1.9
- w_out: bfloat16 [2048, 2048], P('tp'), may hold values from -0.25 to 0.25
- resid: bfloat16 [6144, 2048], P(('sp', 'tp')), may hold values from -30 to 30
- norm_gain: float32 [2048], replicated, may hold values from 0.1 to 1.9
- w_up: bfloat16 [2048, 8192], P('sp', 'tp'), may hold values from -0.125 to 0.125
- w_down: bfloat16 [8192, 2048], P('tp', 'sp'), may hold values from -0.0625 to 0.0625
Outputs:
- layer_out: bfloat16 [6144, 2048], P(('sp', 'tp'))
Inputs may be any that keep to these rules, and one draw needn't show every extreme that they name: `doc_ids`: document numbers never fall along the positions.
All inputs are finite; a program needn't handle non-finite values.
Results may differ from a plain program's by a relative error of at most 0.013.
Values may be sent and summed in bfloat16 or wider, within the bound.
No kernel may reach another device: no remote copies, remote signals or barrier semaphores. Data moves between devices by JAX's collectives and lax.ppermute only.
A program may use at most 128 MiB of HBM per device.

v0:
```python
import functools

import jax
import jax.numpy as jnp
from jax import lax
from jax.experimental import pallas as pl
from jax.experimental.pallas import tpu as pltpu
from jax.sharding import PartitionSpec as P

EPS = 1e-06
FAR_LOW = -1e30
LONGEST_DOC = 3072
LANES = 128
EXTRA = LANES


def places(axis):
    outer = lax.axis_size(axis) // 2
    assert outer * 2 == lax.axis_size(axis)
    index = lax.axis_index(axis)
    return outer, index // 2, index % 2


def flip(value, axis):
    return lax.ppermute(value, axis, [(i, i ^ 1) for i in range(lax.axis_size(axis))])


def shift(value, axis, step, cross=0):
    outer = lax.axis_size(axis) // 2
    moves = [
        (2 * a + c, 2 * ((a + step) % outer) + (c ^ cross)) for a in range(outer) for c in range(2)
    ]
    return lax.ppermute(value, axis, moves)


def neighbour(value):
    moves = [(i, i ^ 2) for i in range(lax.axis_size("sp"))]
    return lax.ppermute(value, "sp", moves)


def carry_shift(value, step):
    outer = lax.axis_size("sp") // 2
    moves = [(2 * a, 2 * (a - step)) for a in range(step, outer)]
    moves += [(2 * a + 1, 2 * (a + step) + 1) for a in range(outer - step)]
    return lax.ppermute(value, "sp", moves)


def running_sums(rows):
    length = rows.shape[1]
    lane = lax.broadcasted_iota(jnp.int32, rows.shape, 1)
    left, right = rows, rows
    step = 1
    while step < length:
        left = left + jnp.where(lane >= step, pltpu.roll(left, step, 1), 0.0)
        right = right + jnp.where(lane < length - step, pltpu.roll(right, length - step, 1), 0.0)
        step *= 2
    return left, right


def log_sigmoid(x):
    return jnp.minimum(x, 0.0) - jnp.log1p(jnp.exp(-jnp.abs(x)))


def three_parts(x):
    high = x.astype(jnp.bfloat16).astype(jnp.float32)
    rest = x - high
    mid = rest.astype(jnp.bfloat16).astype(jnp.float32)
    return high, mid, rest - mid


def pack_side(sums, peak, total, edge, shape):
    lane = lax.broadcasted_iota(jnp.int32, shape, 1)
    high = sums.astype(jnp.bfloat16).astype(jnp.float32)
    side = jnp.where(lane == 0, high, jnp.where(lane == 1, sums - high, 0.0))
    for at, part in enumerate(three_parts(peak) + three_parts(total) + (edge,)):
        side = jnp.where(lane == 2 + at, part, side)
    return side.astype(jnp.bfloat16)


def merge(states, valid, dv):
    between = jnp.zeros((1, 1), jnp.float32)
    heights, links = [], []
    for state, there in zip(states, valid):
        side = state[:16, dv:].astype(jnp.float32)[:1]
        peak = side[:, 2:3] + side[:, 3:4] + side[:, 4:5]
        total = side[:, 5:6] + side[:, 6:7] + side[:, 7:8]
        edge = side[:, 8:9]
        wanted = wanted if links else edge
        link = jnp.logical_and(edge == wanted, edge >= 0.0)
        if there is not None:
            link = jnp.logical_and(link, there)
        heights.append(jnp.where(link, peak + between, FAR_LOW))
        links.append(link)
        between = between + total
    top = heights[0]
    for height in heights[1:]:
        top = jnp.maximum(top, height)
    carry = None
    for state, height, link in zip(states, heights, links):
        part = jnp.where(link, jnp.exp(height - top), 0.0) * state[...].astype(jnp.float32)
        carry = part if carry is None else carry + part
    return carry, top, between, jnp.where(links[0], wanted, -1.0)


def put_state(out, carry, top, total, edge, dv):
    out[:, :dv] = carry[:, :dv].astype(jnp.bfloat16)
    sums = carry[:, dv : dv + 1] + carry[:, dv + 1 : dv + 2]
    out[:, dv:] = pack_side(sums, top, total, edge, (carry.shape[0], EXTRA))


def summary_kernel(info, keys, values, gates, give, mine):
    dqk = keys.shape[1]
    dv = values.shape[1]
    length = keys.shape[0]
    rows = gates[...]
    left, right = running_sums(log_sigmoid(rows))
    doc = rows[4:5]
    first, last = doc[:, :1], doc[:, length - 1 :]
    keys_t = keys[...].astype(jnp.float32).T
    vals = values[...]
    upper = info[0] == 1
    for cum, total, in_gate, edge, holder in (
        (left[2:3], left[2:3, length - 1 :], rows[0:1], last, upper),
        (right[3:4], right[3:4, :1], rows[1:2], first, jnp.logical_not(upper)),
    ):
        exponent = jnp.where(doc == edge, total - cum + in_gate, FAR_LOW)
        peak = jnp.max(exponent, axis=1, keepdims=True)
        weighted = (keys_t * jnp.exp(exponent - peak)).astype(jnp.bfloat16)
        memory = jnp.dot(weighted, vals, preferred_element_type=jnp.float32).astype(jnp.bfloat16)
        sums = jnp.sum(weighted.astype(jnp.float32), axis=1, keepdims=True)
        side = pack_side(sums, peak, total, edge, (dqk, EXTRA))

        @pl.when(holder)
        def _():
            mine[:, :dv] = memory
            mine[:, dv:] = side

        @pl.when(jnp.logical_not(holder))
        def _():
            give[:, :dv] = memory
            give[:, dv:] = side


SMALL = pl.BlockSpec(memory_space=pltpu.SMEM)
LOCAL = pl.BlockSpec(memory_space=pltpu.VMEM)


def summaries(info, keys, values, gates):
    shape = jax.ShapeDtypeStruct((keys.shape[1], values.shape[1] + EXTRA), jnp.bfloat16)
    return pl.pallas_call(
        summary_kernel,
        out_shape=(shape, shape),
        in_specs=[SMALL, LOCAL, LOCAL, LOCAL],
        name="summary",
    )(info, keys, values, gates)


def pair_kernel(mine, got, out):
    dv = mine.shape[1] - EXTRA
    put_state(out, *merge((mine, got), (None, None), dv), dv)


def pair_state(mine, got):
    return pl.pallas_call(
        pair_kernel, out_shape=jax.ShapeDtypeStruct(mine.shape, mine.dtype), name="pair"
    )(mine, got)


def lead_kernel(info, *refs):
    states, out = refs[:-1], refs[-1]
    dv = out.shape[1] - EXTRA
    valid = [info[1] > j for j in range(len(states))]
    put_state(out, *merge(states, valid, dv), dv)


def lead_state(info, states):
    return pl.pallas_call(
        lead_kernel,
        out_shape=jax.ShapeDtypeStruct(states[0].shape, states[0].dtype),
        in_specs=[SMALL] + [LOCAL] * len(states),
        name="lead",
    )(info, *states)


def intra_kernel(queries, keys, values, gates, num_f, num_b, stats, row_buf, col_buf):
    tile = queries.shape[0]
    step = pl.program_id(0)
    scale = queries.shape[1] ** (-0.5)

    @pl.when(step == 0)
    def _():
        rows = gates[...]
        left, right = running_sums(log_sigmoid(rows))
        doc = rows[4:5]
        cums = [left[2:3], right[3:4], rows[0:1] - left[2:3], rows[1:2] - right[3:4]]
        pack = jnp.concatenate(cums + [doc] * 4, axis=0)
        row_buf[...] = pack
        col_buf[...] = pack.T

    scores = (
        lax.dot_general(
            queries[...], keys[...], (((1,), (1,)), ((), ())), preferred_element_type=jnp.float32
        )
        * scale
    )
    cols = col_buf[pl.ds(step * tile, tile), :]
    rows = row_buf[...]
    at_t = step * tile + lax.broadcasted_iota(jnp.int32, scores.shape, 0)
    at_s = lax.broadcasted_iota(jnp.int32, scores.shape, 1)
    same = cols[:, 4:5] == rows[4:5]
    found = []
    for way, out in enumerate((num_f, num_b)):
        order = at_t >= at_s if way == 0 else at_t <= at_s
        keep = jnp.logical_and(order, same)
        inside = rows[2 + way : 3 + way]
        peak = jnp.max(jnp.where(keep, inside, FAR_LOW), axis=1, keepdims=True)
        weights = jnp.where(keep, scores * jnp.exp(inside - peak), 0.0)
        out[...] = jnp.dot(
            weights.astype(jnp.bfloat16), values[...], preferred_element_type=jnp.float32
        )
        found.append((cols[:, way : way + 1], peak, jnp.sum(weights, axis=1, keepdims=True)))
    lane = lax.broadcasted_iota(jnp.int32, (tile, LANES), 1)
    side = jnp.where(lane == 6, cols[:, 4:5], 0.0)
    for at, part in enumerate(found[0] + found[1]):
        side = jnp.where(lane == at, part, side)
    stats[...] = side


def intra(queries, keys, values, gates):
    length, dqk = queries.shape
    dv = values.shape[1]
    tile = length // 3 if length % 384 == 0 else length
    whole = lambda a: pl.BlockSpec(a.shape, lambda i: (0, 0))
    by_rows = lambda width: pl.BlockSpec((tile, width), lambda i: (i, 0))
    wide = lambda width: jax.ShapeDtypeStruct((length, width), jnp.float32)
    return pl.pallas_call(
        intra_kernel,
        out_shape=(wide(dv), wide(dv), wide(LANES)),
        grid=(length // tile,),
        in_specs=[by_rows(dqk), whole(keys), whole(values), whole(gates)],
        out_specs=(by_rows(dv), by_rows(dv), by_rows(LANES)),
        scratch_shapes=[pltpu.VMEM((8, length), jnp.float32), pltpu.VMEM((length, 8), jnp.float32)],
        name="intra",
    )(queries, keys, values, gates)


def emit_kernel(reach, info, queries, num_f, num_b, stats, out_gate, gain, *rest):
    states, handed = rest[: reach + 1], rest[reach + 1]
    outs, (carry_buf, top_buf) = rest[reach + 2 : -2], rest[-2:]
    dv = num_f.shape[1]
    step = pl.program_id(0)
    scale = queries.shape[1] ** (-0.5)

    @pl.when(step == 0)
    def _():
        valid = [None] + [info[1] > j for j in range(reach)]
        for way, got, there in ((1 - info[0], states, valid), (info[0], (handed,), (None,))):
            carry, top, _, edge = merge(got, there, dv)
            carry_buf[way, :, :dv] = carry[:, :dv].astype(jnp.bfloat16)
            sums = carry[:, dv : dv + 1] + carry[:, dv + 1 : dv + 2]
            carry_buf[way, :, dv:] = pack_side(sums, top, top, edge, (carry.shape[0], EXTRA))
            top_buf[way] = jnp.broadcast_to(jnp.concatenate([top, edge], axis=0), (2, LANES))

    query = queries[...]
    side = stats[...]
    memory = None
    for way, num in enumerate((num_f, num_b)):
        _, peak, denom = (side[:, 3 * way + k : 3 * way + k + 1] for k in range(3))
        usable = side[:, 6:7] == top_buf[way, 1:2, :1]
        carried = jnp.where(usable, top_buf[way, :1, :1], FAR_LOW)
        most = jnp.maximum(carried, peak)
        local = jnp.exp(peak - most)
        inter = jnp.where(usable, jnp.exp(carried - most), 0.0) * scale
        got = jnp.dot(query, carry_buf[way], preferred_element_type=jnp.float32)
        denom = denom * local + inter * (got[:, dv : dv + 1] + got[:, dv + 1 : dv + 2])
        share = 1.0 / jnp.maximum(jnp.abs(denom), 1.0)
        part = num[...] * (local * share) + got[:, :dv] * (inter * share)
        memory = part if memory is None else memory + part
    factor = lax.rsqrt(jnp.mean(memory * memory, axis=1, keepdims=True) + EPS)
    gate = 1.0 / (1.0 + jnp.exp(-out_gate[...].astype(jnp.float32)))
    readout = (memory * factor * gain[...] * gate).astype(jnp.bfloat16)
    for slot, out in enumerate(outs):

        @pl.when(info[2 + step] == slot)
        def _():
            out[...] = readout


def emit(info, queries, inner, out_gate, gain, states, handed, count):
    length, dqk = queries.shape
    num_f, num_b, stats = inner
    dv = num_f.shape[1]
    tile = length // count
    whole = lambda a: pl.BlockSpec(a.shape, lambda i, *_: (0, 0))
    by_rows = lambda width: pl.BlockSpec((tile, width), lambda i, *_: (i, 0))
    shape = jax.ShapeDtypeStruct((tile, dv), jnp.bfloat16)
    return pl.pallas_call(
        functools.partial(emit_kernel, len(states) - 1),
        out_shape=(shape,) * count,
        grid_spec=pltpu.PrefetchScalarGridSpec(
            num_scalar_prefetch=1,
            grid=(count,),
            in_specs=[by_rows(dqk), by_rows(dv), by_rows(dv), by_rows(LANES), by_rows(dv), whole(gain)]
            + [whole(s) for s in (*states, handed)],
            out_specs=(whole(shape),) * count,
            scratch_shapes=[
                pltpu.VMEM((2, dqk, dv + EXTRA), jnp.bfloat16),
                pltpu.VMEM((2, 2, LANES), jnp.float32),
            ],
        ),
        name="emit",
    )(info, queries, num_f, num_b, stats, out_gate, gain, *states, handed)


def project_kernel(count, turn, info, *refs):
    pieces, weights = refs[:count], refs[count : 2 * count]
    resid, gain, mixed_out, normed_out, beside_out, whole = refs[2 * count :]
    mixed = resid[...].astype(jnp.float32)
    for piece, weight in zip(pieces, weights):
        mixed = mixed + jnp.dot(piece[...], weight[...], preferred_element_type=jnp.float32)
    mixed_out[...] = mixed
    factor = lax.rsqrt(jnp.mean(mixed * mixed, axis=1, keepdims=True) + EPS)
    normed = mixed * factor * gain[...]
    if not turn:
        normed_out[...] = normed.astype(jnp.bfloat16)
        beside_out[...] = normed_out[...]
        return
    whole[...] = normed
    depth = mixed.shape[1] // turn
    for k in range(turn):
        at = pl.multiple_of(info[k] * depth, LANES)
        part = whole[:, pl.ds(at, depth)].astype(jnp.bfloat16)
        normed_out[:, k * depth : (k + 1) * depth] = part
        beside_out[:, (k ^ 1) * depth : ((k ^ 1) + 1) * depth] = part


def project(pieces, weights, resid, gain, sources, depth):
    inside = depth % LANES == 0
    mixed, normed, beside = pl.pallas_call(
        functools.partial(project_kernel, len(pieces), len(sources) if inside else 0),
        out_shape=(
            jax.ShapeDtypeStruct(resid.shape, jnp.float32),
            jax.ShapeDtypeStruct(resid.shape, jnp.bfloat16),
            jax.ShapeDtypeStruct(resid.shape, jnp.bfloat16),
        ),
        in_specs=[SMALL] + [LOCAL] * (2 * len(pieces) + 2),
        scratch_shapes=[pltpu.VMEM(resid.shape, jnp.float32)],
        name="project",
    )(jnp.stack(sources).astype(jnp.int32), *pieces, *weights, resid, gain)
    if not inside:
        cuts = [lax.dynamic_slice_in_dim(normed, at * depth, depth, 1) for at in sources]
        normed = jnp.concatenate(cuts, axis=1)
        beside = jnp.concatenate([cuts[k ^ 1] for k in range(len(cuts))], axis=1)
    return mixed, normed, beside


ANYWHERE = pl.BlockSpec(memory_space=pl.ANY)


def pack_kernel(*refs):
    parts, out, sems = refs[:-2], refs[-2], refs[-1]
    copies = [
        pltpu.make_async_copy(part, out.at[k], sems.at[k]) for k, part in enumerate(parts)
    ]
    for copy in copies:
        copy.start()
    for copy in copies:
        copy.wait()


def pack(parts):
    return pl.pallas_call(
        pack_kernel,
        out_shape=jax.ShapeDtypeStruct((len(parts),) + parts[0].shape, parts[0].dtype),
        in_specs=[ANYWHERE] * len(parts),
        out_specs=ANYWHERE,
        scratch_shapes=[pltpu.SemaphoreType.DMA((len(parts),))],
    )(*parts)


def up_kernel(blocks, steps, *refs):
    rows = refs[:blocks]
    mine = refs[blocks : blocks + steps]
    theirs = refs[blocks + steps : blocks + 2 * steps]
    out, row_buf, buf, sems = refs[blocks + 2 * steps :]
    each, depth, width = mine[0].shape
    copies, at = [], 0
    for k, source in enumerate(rows):
        span = pl.ds(at, source.shape[0])
        copies.append(pltpu.make_async_copy(source, row_buf.at[span], sems.at[k]))
        at += source.shape[0]
    for core, weights in enumerate((mine, theirs)):
        for k, weight in enumerate(weights):
            copies.append(
                pltpu.make_async_copy(
                    weight,
                    buf.at[core, pl.ds(k * each, each)],
                    sems.at[blocks + core * steps + k],
                )
            )
    for copy in copies:
        copy.start()
    for core in range(2):
        for copy in copies[: blocks + steps] if core == 0 else copies[blocks + steps :]:
            copy.wait()
        here = jnp.dot(
            row_buf[...],
            buf[core].reshape(steps * each * depth, width),
            preferred_element_type=jnp.float32,
        )
        out[:, core * width : (core + 1) * width] = jnp.square(jnp.maximum(here, 0.0)).astype(
            jnp.bfloat16
        )


def up_product(rows, mine, theirs):
    steps = len(mine)
    each, depth, width = mine[0].shape
    total = sum(r.shape[0] for r in rows)
    return pl.pallas_call(
        functools.partial(up_kernel, len(rows), steps),
        out_shape=jax.ShapeDtypeStruct((total, 2 * width), jnp.bfloat16),
        in_specs=[ANYWHERE] * (len(rows) + 2 * steps),
        scratch_shapes=[
            pltpu.VMEM((total, rows[0].shape[1]), jnp.bfloat16),
            pltpu.VMEM((2, steps * each, depth, width), jnp.bfloat16),
            pltpu.SemaphoreType.DMA((len(rows) + 2 * steps,)),
        ],
    )(*rows, *mine, *theirs)


def split_of(line_first):
    return ((0, 2), (1, 3)) if line_first else ((0, 1), (2, 3))


def down_kernel(orders, early, late, *refs):
    groups = len(orders)
    weights = refs[: 2 * groups]
    outs = refs[2 * groups : 4 * groups]
    buf, sems = refs[4 * groups :]
    split = early.shape[0]
    copies = [
        pltpu.make_async_copy(early, buf.at[pl.ds(0, split)], sems.at[0]),
        pltpu.make_async_copy(late, buf.at[pl.ds(split, late.shape[0])], sems.at[1]),
    ]
    for copy in copies:
        copy.start()
    for copy in copies:
        copy.wait()
    half = buf.shape[1] // 2
    rows = buf.shape[0] // 4
    for g, line_first in enumerate(orders):
        mine, theirs = weights[2 * g : 2 * g + 2]
        keep, send = outs[2 * g : 2 * g + 2]
        width = mine.shape[2]
        kept, sent = split_of(line_first)
        for k in range(2):
            part = jnp.dot(
                buf[:, :half], mine[k], preferred_element_type=jnp.float32
            ) + jnp.dot(buf[:, half:], theirs[k], preferred_element_type=jnp.float32)
            for at, block in enumerate(kept):
                keep[at * rows : (at + 1) * rows, k * width : (k + 1) * width] = part[
                    block * rows : (block + 1) * rows
                ]
            to = (1 - k) if line_first else k
            for at, block in enumerate(sent):
                send[at * rows : (at + 1) * rows, to * width : (to + 1) * width] = part[
                    block * rows : (block + 1) * rows
                ].astype(jnp.bfloat16)


def down_product(early, late, weights, orders):
    half = (early.shape[0] + late.shape[0]) // 2
    width = 2 * weights[0][0].shape[2]
    shapes = [
        jax.ShapeDtypeStruct((half, width), kind)
        for _ in orders
        for kind in (jnp.float32, jnp.bfloat16)
    ]
    flat = [w for pair in weights for w in pair]
    return pl.pallas_call(
        functools.partial(down_kernel, orders),
        out_shape=shapes,
        in_specs=[ANYWHERE] * 2 + [LOCAL] * len(flat),
        scratch_shapes=[
            pltpu.VMEM((2 * half, early.shape[1]), jnp.bfloat16),
            pltpu.SemaphoreType.DMA((2,)),
        ],
    )(early, late, *flat)


def add_kernel(kept, sent, turn, ours, theirs, keep, send):
    rows = keep.shape[0] // len(kept)
    add = lambda k: (
        ours[k * rows : (k + 1) * rows].astype(jnp.float32)
        + theirs[k * rows : (k + 1) * rows].astype(jnp.float32)
    )
    for at, k in enumerate(kept):
        keep[at * rows : (at + 1) * rows] = add(k)
    half = send.shape[1] // 2
    for at, k in enumerate(sent):
        value = add(k).astype(jnp.bfloat16)
        span = slice(at * rows, (at + 1) * rows)
        if turn:
            send[span, :half] = value[:, half:]
            send[span, half:] = value[:, :half]
        else:
            send[span] = value


def add_blocks(ours, theirs, kept, sent, turn):
    rows = ours.shape[0] // (len(kept) + len(sent))
    width = ours.shape[1]
    return pl.pallas_call(
        functools.partial(add_kernel, kept, sent, turn),
        out_shape=(
            jax.ShapeDtypeStruct((rows * len(kept), width), jnp.float32),
            jax.ShapeDtypeStruct((rows * len(sent), width), jnp.bfloat16),
        ),
    )(ours, theirs)


def finish_kernel(count, info, mixed, *refs):
    kept, got, out = refs[:count], refs[count : 2 * count], refs[-1]
    width = kept[0].shape[1] // 2
    for k in range(2 * count):
        at = pl.multiple_of(info[k] * width, LANES)
        cols = slice((k % 2) * width, (k % 2 + 1) * width)
        total = mixed[:, pl.ds(at, width)] + kept[k // 2][:, cols]
        total = total + got[k // 2][:, cols].astype(jnp.float32)
        out[:, pl.ds(at, width)] = total.astype(jnp.bfloat16)


def finish(sources, mixed, kept, got):
    width = kept[0].shape[1] // 2
    if width % LANES == 0:
        return pl.pallas_call(
            functools.partial(finish_kernel, len(kept)),
            out_shape=jax.ShapeDtypeStruct(mixed.shape, jnp.bfloat16),
            in_specs=[SMALL] + [LOCAL] * (1 + 2 * len(kept)),
            name="finish",
        )(jnp.stack(sources).astype(jnp.int32), mixed, *kept, *got)
    out = jnp.zeros(mixed.shape, jnp.bfloat16)
    for k, source in enumerate(sources):
        cols = slice((k % 2) * width, (k % 2 + 1) * width)
        total = lax.dynamic_slice_in_dim(mixed, source * width, width, 1) + kept[k // 2][:, cols]
        total = total + got[k // 2][:, cols].astype(jnp.float32)
        out = lax.dynamic_update_slice_in_dim(out, total.astype(jnp.bfloat16), source * width, 1)
    return out


def tp_slots():
    outer, a, c = places("tp")
    return [2 * ((d // 2 - a) % outer) + ((d % 2) ^ c) for d in range(2 * outer)]


def tp_exchange(blocks):
    got = [blocks[0]]
    for slot, block in enumerate(blocks[1:], 1):
        step, cross = slot // 2, slot % 2
        got.append(shift(block, "tp", step, cross))
    return got


def tp_weights(value):
    outer = places("tp")[0]
    got = []
    for step in range(outer):
        here = shift(value, "tp", step) if step else value
        got += [here, flip(here, "tp")]
    return got


def row_blocks(value, given):
    outer = places("tp")[0]
    assert outer == 2
    across = shift(value, "tp", 1)
    beside = neighbour(given)
    return (value, beside, across), shift(beside, "tp", 1)


def sum_back(keep, send, line_first):
    across = lambda x: shift(x, "tp", 1)
    along = lambda x: neighbour(x)
    hops = (along, across) if line_first else (across, along)
    keep, send = add_blocks(keep, hops[0](send), (0,), (1,), not line_first)
    return keep, hops[1](send)


def half_shards(shard, dim):
    outer, a, _ = places("sp")
    size = shard.shape[dim] // 2
    kept = lax.dynamic_slice_in_dim(shard, (a % 2) * size, size, dim)
    given = lax.dynamic_slice_in_dim(shard, (1 - a % 2) * size, size, dim)
    steps = [[kept, neighbour(given)]]
    for _ in range(1, outer // 2):
        steps.append([shift(x, "sp", 2) for x in steps[-1]])
    return steps


def both_cores(packed):
    return packed, flip(packed, "tp")


def up_shards(shard):
    mine, theirs = [], []
    for here in half_shards(shard, 1):
        there = [flip(x, "sp") for x in here]
        packed = pack(here + there)
        mine.append(packed)
        theirs.append(flip(packed, "tp"))
    return mine, theirs


def down_shards(shard):
    got = []
    for step, here in enumerate(half_shards(shard, 0)):
        packed = pack(here)
        if step == 0:
            there = flip(packed, "sp")
        else:
            there = [flip(x, "sp") for x in here]
            there = pack(there)
        got.append(both_cores(packed))
        got.append(both_cores(there))
    return got


def ring_sources():
    outer, a, c = places("sp")
    assert outer % 2 == 0
    return [
        2 * (((a - 2 * step) % outer) ^ k) + (c ^ cross)
        for step in range(outer // 2)
        for cross in range(2)
        for k in range(2)
    ]


def shards(
    queries,
    keys,
    values,
    out_gate,
    input_gates,
    forget_gates,
    doc_ids,
    head_gain,
    w_out,
    resid,
    norm_gain,
    w_up,
    w_down,
):
    length = queries.shape[0]
    heads = input_gates.shape[1]
    outer, a, c = places("sp")
    up_mine, up_theirs = up_shards(w_up)
    down_groups = down_shards(w_down)
    out_shards = tp_weights(w_out)

    reach = min(2 * outer - 1, -(-(LONGEST_DOC - 1) // length))
    hops = min(outer - 1, -(-reach // 2))
    doc_pos = doc_ids.astype(jnp.float32)[None]
    slots = tp_slots()
    info = jnp.stack([c, jnp.where(c == 1, a, outer - 1 - a)] + slots).astype(jnp.int32)
    readouts = []
    for h in range(heads):
        cut = lambda x: x.reshape(length, heads, -1)[:, h]
        k, v = cut(keys), cut(values)
        gates = jnp.concatenate(
            [input_gates[:, h], forget_gates[:, h], doc_pos, jnp.zeros((3, length), jnp.float32)]
        )
        give, mine = summaries(info, k, v, gates)
        got = flip(give, "sp")
        pair = pair_state(mine, got)
        ahead = [carry_shift(pair, j) for j in range(1, hops + 1)]
        handed = flip(lead_state(info, ahead), "sp")
        inner = intra(cut(queries), k, v, gates)
        gain = head_gain.reshape(heads, 1, -1)[h]
        readouts.append(
            emit(
                info, cut(queries), inner, cut(out_gate), gain, [got] + ahead, handed, len(slots)
            )
        )
    blocks = readouts[0]
    if heads > 1:
        blocks = [jnp.concatenate(b, axis=1) for b in zip(*readouts)]
    sources = ring_sources()
    mixed, normed, given = project(
        tp_exchange(blocks), out_shards, resid, norm_gain[None], sources, w_up.shape[0]
    )
    early, late = row_blocks(normed, given)
    early = up_product(early, up_mine, up_theirs)
    late = up_product([late], up_mine, up_theirs)

    parts = down_product(early, late, down_groups[:2], (False, True))
    for step in range(2, len(down_groups)):
        parts += down_product(early, late, down_groups[step : step + 1], (step % 2 == 1,))
    kept, got = [], []
    for step in range(len(down_groups)):
        keep, send = parts[2 * step : 2 * step + 2]
        keep, last = sum_back(keep, send, step % 2 == 1)
        kept.append(keep)
        got.append(last)
    return finish(sources, mixed, kept, got)


def solution(mesh):
    in_specs = (
        P("sp", "tp"),
        P("sp", "tp"),
        P("sp", "tp"),
        P("sp", "tp"),
        P(None, "tp", "sp"),
        P(None, "tp", "sp"),
        P("sp"),
        P("tp"),
        P("tp", None),
        P(("sp", "tp"), None),
        P(),
        P("sp", "tp"),
        P("tp", "sp"),
    )
    out_specs = P(("sp", "tp"), None)

    return jax.shard_map(shards, mesh=mesh, in_specs=in_specs, out_specs=out_specs, check_vma=False)
```

profile of v0, /device:TPU:0, one launch (start us, length us, event | category | flops | bytes accessed | tf_op | source)
XLA Modules:
  0.0 468.5 jit_solution(9330557193300409400)
XLA Ops:
  0.0 3.0 collective-permute-start.8
  3.1 1.3 constant_dynamic-slice_fusion.2
  4.3 1.6 collective-permute-start.13
  5.9 2.6 collective-permute-start.15
  8.5 1.6 collective-permute-start.12
  10.2 0.7 maximum_maximum_fusion.gates
  11.5 4.1 summary.1
  16.1 0.9 constant_dynamic-slice_fusion
  17.0 7.8 %collective-permute-done.got.rest_0_ = bf16[256,640]{1,0:T(8,128)(2,1)S(1)} collective-permute-done((bf16[256,640]{1,0:T(8,128)(2,1)}, bf16[256,640]{1,0:T(8,128)(2,1)S(1)}, u32[]{:S(2)}, u32[]{:S(2)}) %collective-permute-start) | collective-permute-done | bytes 327712 | tf_op jit(solution)/shard_map/ppermute | solution.py:25
  24.8 1.6 collective-permute-start.22
  26.4 2.4 pair.1
  28.8 3.3 collective-permute-done.12.refs_1_
  32.1 1.3 collective-permute-start.1
  33.4 1.3 collective-permute-start.2
  34.8 14.2 %collective-permute-done.8.refs_6_ = bf16[512,2048]{1,0:T(8,128)(2,1)} collective-permute-done((bf16[512,2048]{1,0:T(8,128)(2,1)}, bf16[512,2048]{1,0:T(8,128)(2,1)}, u32[]{:S(2)}, u32[]{:S(2)}) %collective-permute-start.8) | collective-permute-done | bytes 2097184 | tf_op jit(solution)/shard_map/ppermute | solution.py:33
  49.0 7.7 %collective-permute-done.1.refs_0_.rest_1_ = bf16[256,640]{1,0:T(8,128)(2,1)S(1)} collective-permute-done((bf16[256,640]{1,0:T(8,128)(2,1)}, bf16[256,640]{1,0:T(8,128)(2,1)S(1)}, u32[]{:S(2)}, u32[]{:S(2)}) %collective-permute-start.1) | collective-permute-done | bytes 327712 | tf_op jit(solution)/shard_map/ppermute | solution.py:45
  56.8 1.9 collective-permute-start.14
  58.6 2.4 lead.1
  61.1 0.7 collective-permute-start.3
  61.8 16.0 %collective-permute-done.3.rest_3_ = bf16[256,640]{1,0:T(8,128)(2,1)S(1)} collective-permute-done((bf16[256,640]{1,0:T(8,128)(2,1)}, bf16[256,640]{1,0:T(8,128)(2,1)S(1)}, u32[]{:S(2)}, u32[]{:S(2)}) %collective-permute-start.3) | collective-permute-done | bytes 327712 | tf_op jit(solution)/shard_map/ppermute | solution.py:25
  77.8 1.6 collective-permute-start.17
  79.4 2.5 collective-permute-done.16.refs_1_
  82.4 7.5 %intra.1 = (f32[768,512]{1,0:T(8,128)}, f32[768,512]{1,0:T(8,128)}, f32[768,128]{1,0:T(8,128)}) custom-call(bf16[768,256]{1,0:T(8,128)(2,1)} %queries.3, bf16[768,256]{1,0:T(8,128)(2,1)} %keys.3, bf16[768,512]{1,0:T(8,128)(2,1)} %values.3, f32[8,768]{1,0:T(8,128)} %maximum_maximum_fusion.gates), custom_call_target="tpu_custom_call" | custom-call | tf_op jit(solution)/shard_map/intra/pallas_call | solution.py:236
  89.9 8.8 %emit.1 = (bf16[192,512]{1,0:T(8,128)(2,1)}, bf16[192,512]{1,0:T(8,128)(2,1)}, bf16[192,512]{1,0:T(8,128)(2,1)}, bf16[192,512]{1,0:T(8,128)(2,1)}) custom-call(s32[6]{0:T(128)} %stack.72.info, bf16[768,256]{1,0:T(8,128)(2,1)} %queries.3, f32[768,512]{1,0:T(8,128)} %get-tuple-element.33.num_f, f32[768,512]{1,0:T(8,128)} %get-tuple-element.34.num_b, ...), custom_call_target="tpu_custom_call" | custom-call | tf_op jit(solution)/shard_map/emit/pallas_call | solution.py:297
  98.8 64.7 %shard_map.127.refs_3_.refs_1_ = bf16[4,256,1024]{2,1,0:T(8,128)(2,1)} custom-call(bf16[256,1024]{1,0:T(8,128)(2,1)} %copy-done.3, bf16[256,1024]{1,0:T(8,128)(2,1)} %collective-permute-done.12.refs_1_, bf16[256,1024]{1,0:T(8,128)(2,1)} %collective-permute-done.13.refs_2_, bf16[256,1024]{1,0:T(8,128)(2,1)} %copy-done.12), custom_call_target="tpu_custom_call" | custom-call | tf_op jit(solution)/shard_map/pallas_call | solution.py:372
  164.1 64.7 %shard_map.128.refs_4_.refs_2_ = bf16[4,256,1024]{2,1,0:T(8,128)(2,1)} custom-call(bf16[256,1024]{1,0:T(8,128)(2,1)} %collective-permute-done.15.refs_0_, bf16[256,1024]{1,0:T(8,128)(2,1)} %copy-done.11, bf16[256,1024]{1,0:T(8,128)(2,1)} %copy-done.13, bf16[256,1024]{1,0:T(8,128)(2,1)} %collective-permute-done.18.refs_3_), custom_call_target="tpu_custom_call" | custom-call | tf_op jit(solution)/shard_map/pallas_call | solution.py:372
  229.5 6.7 %collective-permute-done.5.refs_2_ = bf16[192,512]{1,0:T(8,128)(2,1)S(1)} collective-permute-done((bf16[192,512]{1,0:T(8,128)(2,1)S(1)}, bf16[192,512]{1,0:T(8,128)(2,1)S(1)}, u32[]{:S(2)}, u32[]{:S(2)}) %collective-permute-start.5) | collective-permute-done | bytes 196640 | tf_op jit(solution)/shard_map/ppermute | solution.py:33
  236.3 32.9 %shard_map.131.refs_0_ = bf16[2,1024,256]{2,1,0:T(8,128)(2,1)} custom-call(bf16[1024,256]{1,0:T(8,128)(2,1)} %copy-done.2, bf16[1024,256]{1,0:T(8,128)(2,1)} %collective-permute-done.22.refs_1_), custom_call_target="tpu_custom_call" | custom-call | tf_op jit(solution)/shard_map/pallas_call | solution.py:372
  269.2 1.8 collective-permute-start.24
  271.0 2.7 collective-permute-start.29
  274.0 0.7 stack.65.info
  274.7 7.8 %project.1 = (f32[192,2048]{1,0:T(8,128)}, bf16[192,2048]{1,0:T(8,128)(2,1)}, bf16[192,2048]{1,0:T(8,128)(2,1)}) custom-call(s32[8]{0:T(128)} %stack.65.info, bf16[192,512]{1,0:T(8,128)(2,1)} %get-tuple-element.38.refs_0_, bf16[192,512]{1,0:T(8,128)(2,1)} %copy-done.23, bf16[192,512]{1,0:T(8,128)(2,1)} %copy-done.24, bf16[192,512]{1,0:T(8,128)(2,1)} %copy-done.25, ...), custom_call_target="tpu_custom_call" | custom-call | tf_op jit(solution)/shard_map/project/pallas_call | solution.py:339
  282.4 15.3 %collective-permute-done.29.refs_1_ = bf16[1024,256]{1,0:T(8,128)(2,1)} collective-permute-done((bf16[1024,256]{1,0:T(8,128)(2,1)}, bf16[1024,256]{1,0:T(8,128)(2,1)}, u32[]{:S(2)}, u32[]{:S(2)}) %collective-permute-start.29) | collective-permute-done | bytes 524320 | tf_op jit(solution)/shard_map/ppermute | solution.py:33
  297.7 8.8 %collective-permute-done.32.refs_0_ = bf16[1024,256]{1,0:T(8,128)(2,1)} collective-permute-done((bf16[1024,256]{1,0:T(8,128)(2,1)}, bf16[1024,256]{1,0:T(8,128)(2,1)}, u32[]{:S(2)}, u32[]{:S(2)}) %collective-permute-start.32) | collective-permute-done | bytes 524320 | tf_op jit(solution)/shard_map/ppermute | solution.py:25
  306.5 1.5 collective-permute-start.11
  308.0 1.7 collective-permute-start.33
  309.7 12.1 %collective-permute-done.33.refs_1_ = bf16[1024,256]{1,0:T(8,128)(2,1)S(1)} collective-permute-done((bf16[1024,256]{1,0:T(8,128)(2,1)}, bf16[1024,256]{1,0:T(8,128)(2,1)S(1)}, u32[]{:S(2)}, u32[]{:S(2)}) %collective-permute-start.33) | collective-permute-done | bytes 524320 | tf_op jit(solution)/shard_map/ppermute | solution.py:25
  321.8 0.8 copy-done.10
  322.6 32.9 %shard_map.135.refs_0_ = bf16[2,1024,256]{2,1,0:T(8,128)(2,1)} custom-call(bf16[1024,256]{1,0:T(8,128)(2,1)} %collective-permute-done.28.refs_0_, bf16[1024,256]{1,0:T(8,128)(2,1)} %collective-permute-done.29.refs_1_), custom_call_target="tpu_custom_call" | custom-call | tf_op jit(solution)/shard_map/pallas_call | solution.py:372
  356.1 32.9 %shard_map.138.refs_0_ = bf16[2,1024,256]{2,1,0:T(8,128)(2,1)} custom-call(bf16[1024,256]{1,0:T(8,128)(2,1)} %collective-permute-done.32.refs_0_, bf16[1024,256]{1,0:T(8,128)(2,1)} %copy-done.10), custom_call_target="tpu_custom_call" | custom-call | tf_op jit(solution)/shard_map/pallas_call | solution.py:372
  389.5 9.6 %shard_map.129.early = bf16[576,2048]{1,0:T(8,128)(2,1)} custom-call(bf16[192,2048]{1,0:T(8,128)(2,1)} %get-tuple-element.43.refs_0_, bf16[192,2048]{1,0:T(8,128)(2,1)} %collective-permute-done.10.refs_1_, bf16[192,2048]{1,0:T(8,128)(2,1)} %collective-permute-done.11.refs_2_, bf16[4,256,1024]{2,1,0:T(8,128)(2,1)} %shard_map.127.refs_3_.refs_1_, ...), custom_call_target="tpu_custom_call" | custom-call | tf_op jit(solution)/shard_map/pallas_call | solution.py:420
  399.1 10.1 %collective-permute-done.21.refs_0_ = bf16[192,2048]{1,0:T(8,128)(2,1)S(1)} collective-permute-done((bf16[192,2048]{1,0:T(8,128)(2,1)}, bf16[192,2048]{1,0:T(8,128)(2,1)S(1)}, u32[]{:S(2)}, u32[]{:S(2)}) %collective-permute-start.21) | collective-permute-done | bytes 786464 | tf_op jit(solution)/shard_map/ppermute | solution.py:33
  409.2 0.9 copy-done.9
  410.1 5.6 %shard_map.130.late = bf16[192,2048]{1,0:T(8,128)(2,1)} custom-call(bf16[192,2048]{1,0:T(8,128)(2,1)} %copy-done.9, bf16[4,256,1024]{2,1,0:T(8,128)(2,1)} %shard_map.127.refs_3_.refs_1_, bf16[4,256,1024]{2,1,0:T(8,128)(2,1)} %shard_map.128.refs_4_.refs_2_, bf16[4,256,1024]{2,1,0:T(8,128)(2,1)} %copy-done, ...), custom_call_target="tpu_custom_call" | custom-call | tf_op jit(solution)/shard_map/pallas_call | solution.py:420
  415.8 8.5 %shard_map.132 = (f32[384,512]{1,0:T(8,128)}, bf16[384,512]{1,0:T(8,128)(2,1)}, f32[384,512]{1,0:T(8,128)}, bf16[384,512]{1,0:T(8,128)(2,1)}) custom-call(bf16[576,2048]{1,0:T(8,128)(2,1)} %shard_map.129.early, bf16[192,2048]{1,0:T(8,128)(2,1)} %shard_map.130.late, bf16[2,1024,256]{2,1,0:T(8,128)(2,1)} %shard_map.131.refs_0_, ...), custom_call_target="tpu_custom_call" | custom-call | tf_op jit(solution)/shard_map/pallas_call | solution.py:481
  424.7 3.9 collective-permute-start.27
  428.6 6.2 %shard_map.136 = (f32[384,512]{1,0:T(8,128)}, bf16[384,512]{1,0:T(8,128)(2,1)}) custom-call(bf16[576,2048]{1,0:T(8,128)(2,1)} %shard_map.129.early, bf16[192,2048]{1,0:T(8,128)(2,1)} %shard_map.130.late, bf16[2,1024,256]{2,1,0:T(8,128)(2,1)} %shard_map.135.refs_0_, bf16[2,1024,256]{2,1,0:T(8,128)(2,1)} %collective-permute-done.30.refs_1_), custom_call_target="tpu_custom_call" | custom-call | tf_op jit(solution)/shard_map/pallas_call | solution.py:481
  434.7 1.7 collective-permute-start.31
  436.5 1.0 copy-done.7
  437.4 6.2 %shard_map.139 = (f32[384,512]{1,0:T(8,128)}, bf16[384,512]{1,0:T(8,128)(2,1)}) custom-call(bf16[576,2048]{1,0:T(8,128)(2,1)} %shard_map.129.early, bf16[192,2048]{1,0:T(8,128)(2,1)} %shard_map.130.late, bf16[2,1024,256]{2,1,0:T(8,128)(2,1)} %shard_map.138.refs_0_, bf16[2,1024,256]{2,1,0:T(8,128)(2,1)} %copy-done.7), custom_call_target="tpu_custom_call" | custom-call | tf_op jit(solution)/shard_map/pallas_call | solution.py:481
  443.8 0.7 copy-done.17
  444.5 2.1 shard_map.133
  446.6 2.0 collective-permute-start.36
  448.6 0.7 copy-done.16
  449.4 2.1 shard_map.134
  451.8 0.7 copy-done.14
  452.6 2.1 shard_map.137
  454.7 1.3 collective-permute-done.35.theirs
  455.9 0.7 copy-done.15
  456.7 2.1 shard_map.140
  459.2 0.8 collective-permute-done.36.refs_4_
  460.0 2.1 collective-permute-done.38.refs_6_
  462.1 2.5 collective-permute-done.39.refs_7_
  465.3 3.2 finish.1
  (109 shorter events, 6.6 us)
Async XLA Ops:
  0.0 10.1 %copy-start.28 = (s32[768]{0:T(1024)S(1)}, s32[768]{0:T(1024)}, u32[]{:S(2)}) copy-start(s32[768]{0:T(1024)} %param.19) | copy-start | bytes 9220
  0.0 10.2 %copy-start.26 = (f32[2,1,768]{2,1,0:T(1,128)S(1)}, f32[2,1,768]{2,1,0:T(1,128)}, u32[]{:S(2)}) copy-start(f32[2,1,768]{2,1,0:T(1,128)} %param.18) | copy-start | bytes 18436
  0.0 10.2 %copy-start.27 = (f32[2,1,768]{2,1,0:T(1,128)S(1)}, f32[2,1,768]{2,1,0:T(1,128)}, u32[]{:S(2)}) copy-start(f32[2,1,768]{2,1,0:T(1,128)} %param.17) | copy-start | bytes 18436
  0.0 16.1 %copy-start.8 = (bf16[2048,256]{1,0:T(8,128)(2,1)S(1)}, bf16[2048,256]{1,0:T(8,128)(2,1)}, u32[]{:S(2)}) copy-start(bf16[2048,256]{1,0:T(8,128)(2,1)} %param.25) | copy-start | bytes 3145732
  0.0 49.0 %collective-permute-start.8 = (bf16[512,2048]{1,0:T(8,128)(2,1)}, bf16[512,2048]{1,0:T(8,128)(2,1)}, u32[]{:S(2)}, u32[]{:S(2)}) collective-permute-start(bf16[512,2048]{1,0:T(8,128)(2,1)} %refs_4_.1), channel_id=1, source_target_pairs={{0,2},{1,3},{2,0},{3,1},{4,6},{5,7},{6,4},{7,5},{8,10},{9,11},{10,... | collective-permute-start | bytes 6291464 | tf_op jit(solution)/shard_map/ppermute | solution.py:33
  4.3 24.5 %copy-start.3 = (bf16[256,1024]{1,0:T(8,128)(2,1)}, bf16[256,1024]{1,0:T(8,128)(2,1)S(1)}, u32[]{:S(2)}) copy-start(bf16[256,1024]{1,0:T(8,128)(2,1)S(1)} %get-tuple-element.64.refs_0_) | copy-start | bytes 1572868
  4.3 29.1 %collective-permute-start.13 = (bf16[256,1024]{1,0:T(8,128)(2,1)S(1)}, bf16[256,1024]{1,0:T(8,128)(2,1)}, u32[]{:S(2)}, u32[]{:S(2)}) collective-permute-start(bf16[256,1024]{1,0:T(8,128)(2,1)S(1)} %get-tuple-element.64.refs_0_), channel_id=1, source_target_pairs={{0,4},{4,0},{8,12},{12,8},{16,20},{20,16},{24,28},{28,24},{1,5},{5... | collective-permute-start | bytes 1572872 | tf_op jit(solution)/shard_map/ppermute | solution.py:25
  5.9 28.8 %collective-permute-start.15 = (bf16[256,1024]{1,0:T(8,128)(2,1)S(1)}, bf16[256,1024]{1,0:T(8,128)(2,1)}, u32[]{:S(2)}, u32[]{:S(2)}) collective-permute-start(bf16[256,1024]{1,0:T(8,128)(2,1)S(1)} %get-tuple-element.64.refs_0_), channel_id=1, source_target_pairs={{0,16},{4,20},{8,24},{12,28},{16,0},{20,4},{24,8},{28,12},{1,17},{... | collective-permute-start | bytes 1572872 | tf_op jit(solution)/shard_map/ppermute | solution.py:33
  8.5 23.6 %collective-permute-start.12 = (bf16[256,1024]{1,0:T(8,128)(2,1)S(1)}, bf16[256,1024]{1,0:T(8,128)(2,1)}, u32[]{:S(2)}, u32[]{:S(2)}) collective-permute-start(bf16[256,1024]{1,0:T(8,128)(2,1)S(1)} %get-tuple-element.63), channel_id=1, source_target_pairs={{0,8},{4,12},{8,0},{12,4},{16,24},{20,28},{24,16},{28,20},{1,9},{5... | collective-permute-start | bytes 1572872 | tf_op jit(solution)/shard_map/ppermute | solution.py:38
  15.6 9.2 %collective-permute-start = (bf16[256,640]{1,0:T(8,128)(2,1)}, bf16[256,640]{1,0:T(8,128)(2,1)S(1)}, u32[]{:S(2)}, u32[]{:S(2)}) collective-permute-start(bf16[256,640]{1,0:T(8,128)(2,1)} %get-tuple-element.36), channel_id=1, source_target_pairs={{0,4},{4,0},{8,12},{12,8},{16,20},{20,16},{24,28},{28,24},{1,5},{5... | collective-permute-start | bytes 983048 | tf_op jit(solution)/shard_map/ppermute | solution.py:25
  17.0 81.7 %copy-start.2 = (bf16[1024,256]{1,0:T(8,128)(2,1)}, bf16[1024,256]{1,0:T(8,128)(2,1)S(1)}, u32[]{:S(2)}) copy-start(bf16[1024,256]{1,0:T(8,128)(2,1)S(1)} %get-tuple-element.62.refs_0_) | copy-start | bytes 1572868
  24.8 1.6 copy-start.6
  24.8 36.3 %collective-permute-start.22 = (bf16[1024,256]{1,0:T(8,128)(2,1)}, bf16[1024,256]{1,0:T(8,128)(2,1)}, u32[]{:S(2)}, u32[]{:S(2)}) collective-permute-start(bf16[1024,256]{1,0:T(8,128)(2,1)} %get-tuple-element.61), channel_id=1, source_target_pairs={{0,8},{4,12},{8,0},{12,4},{16,24},{20,28},{24,16},{28,20},{1,9},{5... | collective-permute-start | bytes 1572872 | tf_op jit(solution)/shard_map/ppermute | solution.py:38
  32.1 24.6 %collective-permute-start.1 = (bf16[256,640]{1,0:T(8,128)(2,1)}, bf16[256,640]{1,0:T(8,128)(2,1)S(1)}, u32[]{:S(2)}, u32[]{:S(2)}) collective-permute-start(bf16[256,640]{1,0:T(8,128)(2,1)} %pair.1), channel_id=1, source_target_pairs={{8,0},{16,8},{24,16},{4,12},{12,20},{20,28},{9,1},{17,9},{25,17},{... | collective-permute-start | bytes 983048 | tf_op jit(solution)/shard_map/ppermute | solution.py:45
  33.4 23.3 %collective-permute-start.2 = (bf16[256,640]{1,0:T(8,128)(2,1)}, bf16[256,640]{1,0:T(8,128)(2,1)S(1)}, u32[]{:S(2)}, u32[]{:S(2)}) collective-permute-start(bf16[256,640]{1,0:T(8,128)(2,1)} %pair.1), channel_id=1, source_target_pairs={{16,0},{24,8},{4,20},{12,28},{17,1},{25,9},{5,21},{13,29},{18,2},{... | collective-permute-start | bytes 983048 | tf_op jit(solution)/shard_map/ppermute | solution.py:45
  34.7 236.3 %collective-permute-start.7 = (bf16[512,2048]{1,0:T(8,128)(2,1)}, bf16[512,2048]{1,0:T(8,128)(2,1)}, u32[]{:S(2)}, u32[]{:S(2)}) collective-permute-start(bf16[512,2048]{1,0:T(8,128)(2,1)} %refs_4_.1), channel_id=1, source_target_pairs={{0,1},{1,0},{2,3},{3,2},{4,5},{5,4},{6,7},{7,6},{8,9},{9,8},{10,11... | collective-permute-start | bytes 6291464 | tf_op jit(solution)/shard_map/ppermute | solution.py:25
  49.0 224.7 %collective-permute-start.9 = (bf16[512,2048]{1,0:T(8,128)(2,1)}, bf16[512,2048]{1,0:T(8,128)(2,1)}, u32[]{:S(2)}, u32[]{:S(2)}) collective-permute-start(bf16[512,2048]{1,0:T(8,128)(2,1)} %collective-permute-done.8.refs_6_), channel_id=1, source_target_pairs={{0,1},{1,0},{2,3},{3,2},{4,5},{5,4},{6,7},{7,6},{8,9},{9,8},{10,11... | collective-permute-start | bytes 6291464 | tf_op jit(solution)/shard_map/ppermute | solution.py:25
  56.7 1.9 copy-start.4
  56.7 25.2 %collective-permute-start.16 = (bf16[256,1024]{1,0:T(8,128)(2,1)}, bf16[256,1024]{1,0:T(8,128)(2,1)S(1)}, u32[]{:S(2)}, u32[]{:S(2)}) collective-permute-start(bf16[256,1024]{1,0:T(8,128)(2,1)} %collective-permute-done.12.refs_1_), channel_id=1, source_target_pairs={{0,16},{4,20},{8,24},{12,28},{16,0},{20,4},{24,8},{28,12},{1,17},{... | collective-permute-start | bytes 1572872 | tf_op jit(solution)/shard_map/ppermute | solution.py:33
  56.7 1.9 copy-start.5
  56.8 25.4 %collective-permute-start.14 = (bf16[256,1024]{1,0:T(8,128)(2,1)}, bf16[256,1024]{1,0:T(8,128)(2,1)S(1)}, u32[]{:S(2)}, u32[]{:S(2)}) collective-permute-start(bf16[256,1024]{1,0:T(8,128)(2,1)} %collective-permute-done.12.refs_1_), channel_id=1, source_target_pairs={{0,4},{4,0},{8,12},{12,8},{16,20},{20,16},{24,28},{28,24},{1,5},{5... | collective-permute-start | bytes 1572872 | tf_op jit(solution)/shard_map/ppermute | solution.py:25
  61.1 16.7 %collective-permute-start.3 = (bf16[256,640]{1,0:T(8,128)(2,1)}, bf16[256,640]{1,0:T(8,128)(2,1)S(1)}, u32[]{:S(2)}, u32[]{:S(2)}) collective-permute-start(bf16[256,640]{1,0:T(8,128)(2,1)} %lead.1), channel_id=1, source_target_pairs={{0,4},{4,0},{8,12},{12,8},{16,20},{20,16},{24,28},{28,24},{1,5},{5... | collective-permute-start | bytes 983048 | tf_op jit(solution)/shard_map/ppermute | solution.py:25
  77.8 12.1 %copy-start.18 = (bf16[256,640]{1,0:T(8,128)(2,1)}, bf16[256,640]{1,0:T(8,128)(2,1)S(1)}, u32[]{:S(2)}) copy-start(bf16[256,640]{1,0:T(8,128)(2,1)S(1)} %collective-permute-done.3.rest_3_) | copy-start | bytes 983044
  77.8 20.9 %collective-permute-start.17 = (bf16[256,1024]{1,0:T(8,128)(2,1)}, bf16[256,1024]{1,0:T(8,128)(2,1)S(1)}, u32[]{:S(2)}, u32[]{:S(2)}) collective-permute-start(bf16[256,1024]{1,0:T(8,128)(2,1)} %collective-permute-done.15.refs_0_), channel_id=1, source_target_pairs={{0,4},{4,0},{8,12},{12,8},{16,20},{20,16},{24,28},{28,24},{1,5},{5... | collective-permute-start | bytes 1572872 | tf_op jit(solution)/shard_map/ppermute | solution.py:25
  81.9 16.8 %copy-start.11 = (bf16[256,1024]{1,0:T(8,128)(2,1)}, bf16[256,1024]{1,0:T(8,128)(2,1)S(1)}, u32[]{:S(2)}) copy-start(bf16[256,1024]{1,0:T(8,128)(2,1)S(1)} %collective-permute-done.16.refs_1_) | copy-start | bytes 1572868
  81.9 81.6 %collective-permute-start.18 = (bf16[256,1024]{1,0:T(8,128)(2,1)S(1)}, bf16[256,1024]{1,0:T(8,128)(2,1)}, u32[]{:S(2)}, u32[]{:S(2)}) collective-permute-start(bf16[256,1024]{1,0:T(8,128)(2,1)S(1)} %collective-permute-done.16.refs_1_), channel_id=1, source_target_pairs={{0,4},{4,0},{8,12},{12,8},{16,20},{20,16},{24,28},{28,24},{1,5},{5... | collective-permute-start | bytes 1572872 | tf_op jit(solution)/shard_map/ppermute | solution.py:25
  82.2 16.6 %copy-start.12 = (bf16[256,1024]{1,0:T(8,128)(2,1)}, bf16[256,1024]{1,0:T(8,128)(2,1)S(1)}, u32[]{:S(2)}) copy-start(bf16[256,1024]{1,0:T(8,128)(2,1)S(1)} %collective-permute-done.14.refs_3_) | copy-start | bytes 1572868
  82.2 146.6 %collective-permute-start.28 = (bf16[1024,256]{1,0:T(8,128)(2,1)S(1)}, bf16[1024,256]{1,0:T(8,128)(2,1)}, u32[]{:S(2)}, u32[]{:S(2)}) collective-permute-start(bf16[1024,256]{1,0:T(8,128)(2,1)S(1)} %get-tuple-element.62.refs_0_), channel_id=1, source_target_pairs={{0,16},{4,20},{8,24},{12,28},{16,0},{20,4},{24,8},{28,12},{1,17},{... | collective-permute-start | bytes 1572872 | tf_op jit(solution)/shard_map/ppermute | solution.py:33
  98.7 64.8 %copy-start.13 = (bf16[256,1024]{1,0:T(8,128)(2,1)}, bf16[256,1024]{1,0:T(8,128)(2,1)S(1)}, u32[]{:S(2)}) copy-start(bf16[256,1024]{1,0:T(8,128)(2,1)S(1)} %collective-permute-done.17.refs_2_) | copy-start | bytes 1572868
  98.8 130.1 %collective-permute-start.4 = (bf16[192,512]{1,0:T(8,128)(2,1)}, bf16[192,512]{1,0:T(8,128)(2,1)S(1)}, u32[]{:S(2)}, u32[]{:S(2)}) collective-permute-start(bf16[192,512]{1,0:T(8,128)(2,1)} %get-tuple-element.39), channel_id=1, source_target_pairs={{0,1},{1,0},{2,3},{3,2},{4,5},{5,4},{6,7},{7,6},{8,9},{9,8},{10,11... | collective-permute-start | bytes 589832 | tf_op jit(solution)/shard_map/ppermute | solution.py:33
  163.5 65.4 %copy-start.30 = (bf16[192,512]{1,0:T(8,128)(2,1)S(1)}, bf16[192,512]{1,0:T(8,128)(2,1)}, u32[]{:S(2)}) copy-start(bf16[192,512]{1,0:T(8,128)(2,1)} %get-tuple-element.40) | copy-start | bytes 589828
  163.5 72.7 %copy-start.29 = (bf16[192,512]{1,0:T(8,128)(2,1)S(1)}, bf16[192,512]{1,0:T(8,128)(2,1)}, u32[]{:S(2)}) copy-start(bf16[192,512]{1,0:T(8,128)(2,1)} %get-tuple-element.41) | copy-start | bytes 589828
  163.6 158.2 %collective-permute-start.19 = (bf16[4,256,1024]{2,1,0:T(8,128)(2,1)}, bf16[4,256,1024]{2,1,0:T(8,128)(2,1)S(1)}, u32[]{:S(2)}, u32[]{:S(2)}) collective-permute-start(bf16[4,256,1024]{2,1,0:T(8,128)(2,1)} %shard_map.127.refs_3_.refs_1_), channel_id=1, source_target_pairs={{0,1},{1,0},{2,3},{3,2},{4,5},{5,4},{6,7},{7,6},{8,9},{9,8},{10,11... | collective-permute-start | bytes 6291464 | tf_op jit(solution)/shard_map/ppermute | solution.py:25
  228.8 126.7 %collective-permute-start.20 = (bf16[4,256,1024]{2,1,0:T(8,128)(2,1)}, bf16[4,256,1024]{2,1,0:T(8,128)(2,1)}, u32[]{:S(2)}, u32[]{:S(2)}) collective-permute-start(bf16[4,256,1024]{2,1,0:T(8,128)(2,1)} %shard_map.128.refs_4_.refs_2_), channel_id=1, source_target_pairs={{0,1},{1,0},{2,3},{3,2},{4,5},{5,4},{6,7},{7,6},{8,9},{9,8},{10,11... | collective-permute-start | bytes 6291464 | tf_op jit(solution)/shard_map/ppermute | solution.py:25
  228.9 45.8 %copy-start.23 = (bf16[192,512]{1,0:T(8,128)(2,1)}, bf16[192,512]{1,0:T(8,128)(2,1)S(1)}, u32[]{:S(2)}) copy-start(bf16[192,512]{1,0:T(8,128)(2,1)S(1)} %collective-permute-done.4.refs_1_) | copy-start | bytes 589828
  228.9 7.3 %collective-permute-start.5 = (bf16[192,512]{1,0:T(8,128)(2,1)S(1)}, bf16[192,512]{1,0:T(8,128)(2,1)S(1)}, u32[]{:S(2)}, u32[]{:S(2)}) collective-permute-start(bf16[192,512]{1,0:T(8,128)(2,1)S(1)} %copy-done.30), channel_id=1, source_target_pairs={{0,2},{1,3},{2,0},{3,1},{4,6},{5,7},{6,4},{7,5},{8,10},{9,11},{10,... | collective-permute-start | bytes 589832 | tf_op jit(solution)/shard_map/ppermute | solution.py:33
  236.2 38.4 %copy-start.24 = (bf16[192,512]{1,0:T(8,128)(2,1)}, bf16[192,512]{1,0:T(8,128)(2,1)S(1)}, u32[]{:S(2)}) copy-start(bf16[192,512]{1,0:T(8,128)(2,1)S(1)} %collective-permute-done.5.refs_2_) | copy-start | bytes 589828
  236.2 32.9 %collective-permute-start.6 = (bf16[192,512]{1,0:T(8,128)(2,1)S(1)}, bf16[192,512]{1,0:T(8,128)(2,1)S(1)}, u32[]{:S(2)}, u32[]{:S(2)}) collective-permute-start(bf16[192,512]{1,0:T(8,128)(2,1)S(1)} %copy-done.29), channel_id=1, source_target_pairs={{0,3},{1,2},{2,1},{3,0},{4,7},{5,6},{6,5},{7,4},{8,11},{9,10},{10,... | collective-permute-start | bytes 589832 | tf_op jit(solution)/shard_map/ppermute | solution.py:33
  269.2 5.5 %copy-start.25 = (bf16[192,512]{1,0:T(8,128)(2,1)}, bf16[192,512]{1,0:T(8,128)(2,1)S(1)}, u32[]{:S(2)}) copy-start(bf16[192,512]{1,0:T(8,128)(2,1)S(1)} %collective-permute-done.6.refs_3_) | copy-start | bytes 589828
  269.2 38.8 %collective-permute-start.24 = (bf16[2,1024,256]{2,1,0:T(8,128)(2,1)}, bf16[2,1024,256]{2,1,0:T(8,128)(2,1)}, u32[]{:S(2)}, u32[]{:S(2)}) collective-permute-start(bf16[2,1024,256]{2,1,0:T(8,128)(2,1)} %shard_map.131.refs_0_), channel_id=1, source_target_pairs={{0,4},{4,0},{8,12},{12,8},{16,20},{20,16},{24,28},{28,24},{1,5},{5... | collective-permute-start | bytes 3145736 | tf_op jit(solution)/shard_map/ppermute | solution.py:25
  271.0 26.8 %collective-permute-start.29 = (bf16[1024,256]{1,0:T(8,128)(2,1)}, bf16[1024,256]{1,0:T(8,128)(2,1)}, u32[]{:S(2)}, u32[]{:S(2)}) collective-permute-start(bf16[1024,256]{1,0:T(8,128)(2,1)} %collective-permute-done.22.refs_1_), channel_id=1, source_target_pairs={{0,16},{4,20},{8,24},{12,28},{16,0},{20,4},{24,8},{28,12},{1,17},{... | collective-permute-start | bytes 1572872 | tf_op jit(solution)/shard_map/ppermute | solution.py:33
  273.7 32.8 %collective-permute-start.32 = (bf16[1024,256]{1,0:T(8,128)(2,1)}, bf16[1024,256]{1,0:T(8,128)(2,1)}, u32[]{:S(2)}, u32[]{:S(2)}) collective-permute-start(bf16[1024,256]{1,0:T(8,128)(2,1)} %collective-permute-done.28.refs_0_), channel_id=1, source_target_pairs={{0,4},{4,0},{8,12},{12,8},{16,20},{20,16},{24,28},{28,24},{1,5},{5... | collective-permute-start | bytes 1572872 | tf_op jit(solution)/shard_map/ppermute | solution.py:25
  274.7 47.1 %copy-start.1 = (bf16[2,1024,256]{2,1,0:T(8,128)(2,1)S(1)}, bf16[2,1024,256]{2,1,0:T(8,128)(2,1)}, u32[]{:S(2)}) copy-start(bf16[2,1024,256]{2,1,0:T(8,128)(2,1)} %shard_map.131.refs_0_) | copy-start | bytes 3145732
  297.7 91.2 %collective-permute-start.10 = (bf16[192,2048]{1,0:T(8,128)(2,1)}, bf16[192,2048]{1,0:T(8,128)(2,1)}, u32[]{:S(2)}, u32[]{:S(2)}) collective-permute-start(bf16[192,2048]{1,0:T(8,128)(2,1)} %get-tuple-element.44), channel_id=1, source_target_pairs={{0,8},{4,12},{8,0},{12,4},{16,24},{20,28},{24,16},{28,20},{1,9},{5... | collective-permute-start | bytes 2359304 | tf_op jit(solution)/shard_map/ppermute | solution.py:38
  306.5 82.6 %collective-permute-start.11 = (bf16[192,2048]{1,0:T(8,128)(2,1)}, bf16[192,2048]{1,0:T(8,128)(2,1)}, u32[]{:S(2)}, u32[]{:S(2)}) collective-permute-start(bf16[192,2048]{1,0:T(8,128)(2,1)} %get-tuple-element.43.refs_0_), channel_id=1, source_target_pairs={{0,2},{1,3},{2,0},{3,1},{4,6},{5,7},{6,4},{7,5},{8,10},{9,11},{10,... | collective-permute-start | bytes 2359304 | tf_op jit(solution)/shard_map/ppermute | solution.py:33
  308.0 13.8 %collective-permute-start.33 = (bf16[1024,256]{1,0:T(8,128)(2,1)}, bf16[1024,256]{1,0:T(8,128)(2,1)S(1)}, u32[]{:S(2)}, u32[]{:S(2)}) collective-permute-start(bf16[1024,256]{1,0:T(8,128)(2,1)} %collective-permute-done.29.refs_1_), channel_id=1, source_target_pairs={{0,4},{4,0},{8,12},{12,8},{16,20},{20,16},{24,28},{28,24},{1,5},{5... | collective-permute-start | bytes 1572872 | tf_op jit(solution)/shard_map/ppermute | solution.py:25
  321.8 94.0 %collective-permute-start.23 = (bf16[2,1024,256]{2,1,0:T(8,128)(2,1)S(1)}, bf16[2,1024,256]{2,1,0:T(8,128)(2,1)}, u32[]{:S(2)}, u32[]{:S(2)}) collective-permute-start(bf16[2,1024,256]{2,1,0:T(8,128)(2,1)S(1)} %copy-done.1), channel_id=1, source_target_pairs={{0,1},{1,0},{2,3},{3,2},{4,5},{5,4},{6,7},{7,6},{8,9},{9,8},{10,11... | collective-permute-start | bytes 3145736 | tf_op jit(solution)/shard_map/ppermute | solution.py:25
  322.6 66.4 %copy-start = (bf16[4,256,1024]{2,1,0:T(8,128)(2,1)}, bf16[4,256,1024]{2,1,0:T(8,128)(2,1)S(1)}, u32[]{:S(2)}) copy-start(bf16[4,256,1024]{2,1,0:T(8,128)(2,1)S(1)} %collective-permute-done.19.refs_5_.refs_3_) | copy-start | bytes 6291460
  322.6 93.2 %collective-permute-start.25 = (bf16[2,1024,256]{2,1,0:T(8,128)(2,1)}, bf16[2,1024,256]{2,1,0:T(8,128)(2,1)}, u32[]{:S(2)}, u32[]{:S(2)}) collective-permute-start(bf16[2,1024,256]{2,1,0:T(8,128)(2,1)} %collective-permute-done.24.refs_2_), channel_id=1, source_target_pairs={{0,1},{1,0},{2,3},{3,2},{4,5},{5,4},{6,7},{7,6},{8,9},{9,8},{10,11... | collective-permute-start | bytes 3145736 | tf_op jit(solution)/shard_map/ppermute | solution.py:25
  355.5 73.0 %collective-permute-start.30 = (bf16[2,1024,256]{2,1,0:T(8,128)(2,1)}, bf16[2,1024,256]{2,1,0:T(8,128)(2,1)}, u32[]{:S(2)}, u32[]{:S(2)}) collective-permute-start(bf16[2,1024,256]{2,1,0:T(8,128)(2,1)} %shard_map.135.refs_0_), channel_id=1, source_target_pairs={{0,1},{1,0},{2,3},{3,2},{4,5},{5,4},{6,7},{7,6},{8,9},{9,8},{10,11... | collective-permute-start | bytes 3145736 | tf_op jit(solution)/shard_map/ppermute | solution.py:25
  389.0 47.5 %collective-permute-start.34 = (bf16[2,1024,256]{2,1,0:T(8,128)(2,1)}, bf16[2,1024,256]{2,1,0:T(8,128)(2,1)S(1)}, u32[]{:S(2)}, u32[]{:S(2)}) collective-permute-start(bf16[2,1024,256]{2,1,0:T(8,128)(2,1)} %shard_map.138.refs_0_), channel_id=1, source_target_pairs={{0,1},{1,0},{2,3},{3,2},{4,5},{5,4},{6,7},{7,6},{8,9},{9,8},{10,11... | collective-permute-start | bytes 3145736 | tf_op jit(solution)/shard_map/ppermute | solution.py:25
  389.1 20.1 %collective-permute-start.21 = (bf16[192,2048]{1,0:T(8,128)(2,1)}, bf16[192,2048]{1,0:T(8,128)(2,1)S(1)}, u32[]{:S(2)}, u32[]{:S(2)}) collective-permute-start(bf16[192,2048]{1,0:T(8,128)(2,1)} %collective-permute-done.10.refs_1_), channel_id=1, source_target_pairs={{0,2},{1,3},{2,0},{3,1},{4,6},{5,7},{6,4},{7,5},{8,10},{9,11},{10,... | collective-permute-start | bytes 2359304 | tf_op jit(solution)/shard_map/ppermute | solution.py:33
  424.3 19.5 %collective-permute-start.26 = (bf16[384,512]{1,0:T(8,128)(2,1)}, bf16[384,512]{1,0:T(8,128)(2,1)S(1)}, u32[]{:S(2)}, u32[]{:S(2)}) collective-permute-start(bf16[384,512]{1,0:T(8,128)(2,1)} %get-tuple-element.46), channel_id=1, source_target_pairs={{0,2},{1,3},{2,0},{3,1},{4,6},{5,7},{6,4},{7,5},{8,10},{9,11},{10,... | collective-permute-start | bytes 1179656 | tf_op jit(solution)/shard_map/ppermute | solution.py:33
  424.7 24.0 %collective-permute-start.27 = (bf16[384,512]{1,0:T(8,128)(2,1)}, bf16[384,512]{1,0:T(8,128)(2,1)S(1)}, u32[]{:S(2)}, u32[]{:S(2)}) collective-permute-start(bf16[384,512]{1,0:T(8,128)(2,1)} %get-tuple-element.49), channel_id=1, source_target_pairs={{0,8},{4,12},{8,0},{12,4},{16,24},{20,28},{24,16},{28,20},{1,9},{5... | collective-permute-start | bytes 1179656 | tf_op jit(solution)/shard_map/ppermute | solution.py:38
  434.7 17.1 %collective-permute-start.31 = (bf16[384,512]{1,0:T(8,128)(2,1)}, bf16[384,512]{1,0:T(8,128)(2,1)S(1)}, u32[]{:S(2)}, u32[]{:S(2)}) collective-permute-start(bf16[384,512]{1,0:T(8,128)(2,1)} %get-tuple-element.52), channel_id=1, source_target_pairs={{0,2},{1,3},{2,0},{3,1},{4,6},{5,7},{6,4},{7,5},{8,10},{9,11},{10,... | collective-permute-start | bytes 1179656 | tf_op jit(solution)/shard_map/ppermute | solution.py:33
  436.5 1.0 copy-start.7
  443.7 12.3 %collective-permute-start.35 = (bf16[384,512]{1,0:T(8,128)(2,1)}, bf16[384,512]{1,0:T(8,128)(2,1)S(1)}, u32[]{:S(2)}, u32[]{:S(2)}) collective-permute-start(bf16[384,512]{1,0:T(8,128)(2,1)} %get-tuple-element.55), channel_id=1, source_target_pairs={{0,8},{4,12},{8,0},{12,4},{16,24},{20,28},{24,16},{28,20},{1,9},{5... | collective-permute-start | bytes 1179656 | tf_op jit(solution)/shard_map/ppermute | solution.py:38
  446.6 13.4 %collective-permute-start.36 = (bf16[192,512]{1,0:T(8,128)(2,1)}, bf16[192,512]{1,0:T(8,128)(2,1)S(1)}, u32[]{:S(2)}, u32[]{:S(2)}) collective-permute-start(bf16[192,512]{1,0:T(8,128)(2,1)} %get-tuple-element.57), channel_id=1, source_target_pairs={{0,8},{4,12},{8,0},{12,4},{16,24},{20,28},{24,16},{28,20},{1,9},{5... | collective-permute-start | bytes 589832 | tf_op jit(solution)/shard_map/ppermute | solution.py:38
  451.5 8.6 %collective-permute-start.37 = (bf16[192,512]{1,0:T(8,128)(2,1)}, bf16[192,512]{1,0:T(8,128)(2,1)S(1)}, u32[]{:S(2)}, u32[]{:S(2)}) collective-permute-start(bf16[192,512]{1,0:T(8,128)(2,1)} %get-tuple-element.58), channel_id=1, source_target_pairs={{0,2},{1,3},{2,0},{3,1},{4,6},{5,7},{6,4},{7,5},{8,10},{9,11},{10,... | collective-permute-start | bytes 589832 | tf_op jit(solution)/shard_map/ppermute | solution.py:33
  454.6 7.5 %collective-permute-start.38 = (bf16[192,512]{1,0:T(8,128)(2,1)}, bf16[192,512]{1,0:T(8,128)(2,1)S(1)}, u32[]{:S(2)}, u32[]{:S(2)}) collective-permute-start(bf16[192,512]{1,0:T(8,128)(2,1)} %get-tuple-element.59), channel_id=1, source_target_pairs={{0,8},{4,12},{8,0},{12,4},{16,24},{20,28},{24,16},{28,20},{1,9},{5... | collective-permute-start | bytes 589832 | tf_op jit(solution)/shard_map/ppermute | solution.py:38
  458.8 5.9 %collective-permute-start.39 = (bf16[192,512]{1,0:T(8,128)(2,1)}, bf16[192,512]{1,0:T(8,128)(2,1)S(1)}, u32[]{:S(2)}, u32[]{:S(2)}) collective-permute-start(bf16[192,512]{1,0:T(8,128)(2,1)} %get-tuple-element.60), channel_id=1, source_target_pairs={{0,2},{1,3},{2,0},{3,1},{4,6},{5,7},{6,4},{7,5},{8,10},{9,11},{10,... | collective-permute-start | bytes 589832 | tf_op jit(solution)/shard_map/ppermute | solution.py:33
  460.0 4.6 copy-start.19
  460.0 4.6 copy-start.20
  462.1 2.5 copy-start.21
  (7 other events, 5.4 us)
where the time goes:
time: 469 us
  Pallas kernels  309 us (66%)
  waiting for transfers between devices  111 us (24%)
  starting transfers between devices  37.6 us (8%)
  local copies, waits for them, and re-layouts  9.92 us (2%)
    pallas_call x5, Pallas kernels, pack(): pl.pallas_call(pack_kernel, out_shape=jax.ShapeDtypeStruct((len(parts),)...  228 us
    ppermute x14, waiting for transfers between devices, shift(): return lax.ppermute(value, axis, moves)  51.4 us
    ppermute x17, waiting for transfers between devices, flip(): lax.ppermute(value, axis, [(i, i ^ 1) for i in range(lax.axis_size(axis))])  44.7 us
    pallas_call x3, Pallas kernels, down_product(): pl.pallas_call(functools.partial(down_kernel, orders), out_shape=shapes,...  20.9 us
    pallas_call x2, Pallas kernels, up_product(): pl.pallas_call(functools.partial(up_kernel, len(rows), steps), out_shape=...  15.2 us
    ppermute x14, starting transfers between devices, shift(): return lax.ppermute(value, axis, moves)  14.1 us
    ppermute x17, starting transfers between devices, flip(): lax.ppermute(value, axis, [(i, i ^ 1) for i in range(lax.axis_size(axis))])  11.8 us
  transfers between devices with their start and end apart: 40, of which 15 were waited for; matrix products, arithmetic and copies ran while one was open for 1% of the time, Pallas kernels for 65%

commit v1 on v0

--- a/solution.py
+++ b/solution.py
@@ -141,6 +141,10 @@
             give[:, dv:] = side
 
 
+def room(mib):
+    return pltpu.CompilerParams(vmem_limit_bytes=mib << 20)
+
+
 SMALL = pl.BlockSpec(memory_space=pltpu.SMEM)
 LOCAL = pl.BlockSpec(memory_space=pltpu.VMEM)
 
@@ -151,7 +155,7 @@
         summary_kernel,
         out_shape=(shape, shape),
         in_specs=[SMALL, LOCAL, LOCAL, LOCAL],
-        name="summary",
+        name="summary", compiler_params=room(10),
     )(info, keys, values, gates)
 
 
@@ -162,7 +166,7 @@
 
 def pair_state(mine, got):
     return pl.pallas_call(
-        pair_kernel, out_shape=jax.ShapeDtypeStruct(mine.shape, mine.dtype), name="pair"
+        pair_kernel, out_shape=jax.ShapeDtypeStruct(mine.shape, mine.dtype), name="pair", compiler_params=room(5)
     )(mine, got)
 
 
@@ -178,7 +182,7 @@
         lead_kernel,
         out_shape=jax.ShapeDtypeStruct(states[0].shape, states[0].dtype),
         in_specs=[SMALL] + [LOCAL] * len(states),
-        name="lead",
+        name="lead", compiler_params=room(5),
     )(info, *states)
 
 
@@ -240,7 +244,7 @@
         in_specs=[by_rows(dqk), whole(keys), whole(values), whole(gates)],
         out_specs=(by_rows(dv), by_rows(dv), by_rows(LANES)),
         scratch_shapes=[pltpu.VMEM((8, length), jnp.float32), pltpu.VMEM((length, 8), jnp.float32)],
-        name="intra",
+        name="intra", compiler_params=room(16),
     )(queries, keys, values, gates)
 
 
@@ -308,7 +312,7 @@
                 pltpu.VMEM((2, 2, LANES), jnp.float32),
             ],
         ),
-        name="emit",
+        name="emit", compiler_params=room(12),
     )(info, queries, num_f, num_b, stats, out_gate, gain, *states, handed)
 
 
@@ -345,7 +349,7 @@
         ),
         in_specs=[SMALL] + [LOCAL] * (2 * len(pieces) + 2),
         scratch_shapes=[pltpu.VMEM(resid.shape, jnp.float32)],
-        name="project",
+        name="project", compiler_params=room(20),
     )(jnp.stack(sources).astype(jnp.int32), *pieces, *weights, resid, gain)
     if not inside:
         cuts = [lax.dynamic_slice_in_dim(normed, at * depth, depth, 1) for at in sources]
@@ -354,27 +358,16 @@
     return mixed, normed, beside
 
 
-ANYWHERE = pl.BlockSpec(memory_space=pl.ANY)
-
-
 def pack_kernel(*refs):
-    parts, out, sems = refs[:-2], refs[-2], refs[-1]
-    copies = [
-        pltpu.make_async_copy(part, out.at[k], sems.at[k]) for k, part in enumerate(parts)
-    ]
-    for copy in copies:
-        copy.start()
-    for copy in copies:
-        copy.wait()
+    for k, part in enumerate(refs[:-1]):
+        refs[-1][k] = part[...]
 
 
 def pack(parts):
     return pl.pallas_call(
         pack_kernel,
         out_shape=jax.ShapeDtypeStruct((len(parts),) + parts[0].shape, parts[0].dtype),
-        in_specs=[ANYWHERE] * len(parts),
-        out_specs=ANYWHERE,
-        scratch_shapes=[pltpu.SemaphoreType.DMA((len(parts),))],
+        compiler_params=room(8),
     )(*parts)
 
 
@@ -382,32 +375,22 @@
     rows = refs[:blocks]
     mine = refs[blocks : blocks + steps]
     theirs = refs[blocks + steps : blocks + 2 * steps]
-    out, row_buf, buf, sems = refs[blocks + 2 * steps :]
+    out, row_buf = refs[blocks + 2 * steps :]
     each, depth, width = mine[0].shape
-    copies, at = [], 0
-    for k, source in enumerate(rows):
-        span = pl.ds(at, source.shape[0])
-        copies.append(pltpu.make_async_copy(source, row_buf.at[span], sems.at[k]))
+    at = 0
+    for source in rows:
+        row_buf[at : at + source.shape[0]] = source[...]
         at += source.shape[0]
+    span = each * depth
     for core, weights in enumerate((mine, theirs)):
+        here = None
         for k, weight in enumerate(weights):
-            copies.append(
-                pltpu.make_async_copy(
-                    weight,
-                    buf.at[core, pl.ds(k * each, each)],
-                    sems.at[blocks + core * steps + k],
-                )
+            part = jnp.dot(
+                row_buf[:, k * span : (k + 1) * span],
+                weight[...].reshape(span, width),
+                preferred_element_type=jnp.float32,
             )
-    for copy in copies:
-        copy.start()
-    for core in range(2):
-        for copy in copies[: blocks + steps] if core == 0 else copies[blocks + steps :]:
-            copy.wait()
-        here = jnp.dot(
-            row_buf[...],
-            buf[core].reshape(steps * each * depth, width),
-            preferred_element_type=jnp.float32,
-        )
+            here = part if here is None else here + part
         out[:, core * width : (core + 1) * width] = jnp.square(jnp.maximum(here, 0.0)).astype(
             jnp.bfloat16
         )
@@ -415,17 +398,13 @@
 
 def up_product(rows, mine, theirs):
     steps = len(mine)
-    each, depth, width = mine[0].shape
+    width = mine[0].shape[2]
     total = sum(r.shape[0] for r in rows)
     return pl.pallas_call(
         functools.partial(up_kernel, len(rows), steps),
         out_shape=jax.ShapeDtypeStruct((total, 2 * width), jnp.bfloat16),
-        in_specs=[ANYWHERE] * (len(rows) + 2 * steps),
-        scratch_shapes=[
-            pltpu.VMEM((total, rows[0].shape[1]), jnp.bfloat16),
-            pltpu.VMEM((2, steps * each, depth, width), jnp.bfloat16),
-            pltpu.SemaphoreType.DMA((len(rows) + 2 * steps,)),
-        ],
+        scratch_shapes=[pltpu.VMEM((total, rows[0].shape[1]), jnp.bfloat16)],
+        compiler_params=room(26),
     )(*rows, *mine, *theirs)
 
 
@@ -437,36 +416,36 @@
     groups = len(orders)
     weights = refs[: 2 * groups]
     outs = refs[2 * groups : 4 * groups]
-    buf, sems = refs[4 * groups :]
-    split = early.shape[0]
-    copies = [
-        pltpu.make_async_copy(early, buf.at[pl.ds(0, split)], sems.at[0]),
-        pltpu.make_async_copy(late, buf.at[pl.ds(split, late.shape[0])], sems.at[1]),
-    ]
-    for copy in copies:
-        copy.start()
-    for copy in copies:
-        copy.wait()
-    half = buf.shape[1] // 2
-    rows = buf.shape[0] // 4
+    wide = refs[4 * groups]
+    half = early.shape[1] // 2
+    rows = (early.shape[0] + late.shape[0]) // 4
+    width = weights[0].shape[2]
     for g, line_first in enumerate(orders):
-        mine, theirs = weights[2 * g : 2 * g + 2]
+        for core in range(2):
+            for k in range(2):
+                wide[core * half : (core + 1) * half, k * width : (k + 1) * width] = weights[
+                    2 * g + core
+                ][k]
         keep, send = outs[2 * g : 2 * g + 2]
-        width = mine.shape[2]
         kept, sent = split_of(line_first)
-        for k in range(2):
-            part = jnp.dot(
-                buf[:, :half], mine[k], preferred_element_type=jnp.float32
-            ) + jnp.dot(buf[:, half:], theirs[k], preferred_element_type=jnp.float32)
-            for at, block in enumerate(kept):
-                keep[at * rows : (at + 1) * rows, k * width : (k + 1) * width] = part[
-                    block * rows : (block + 1) * rows
-                ]
-            to = (1 - k) if line_first else k
-            for at, block in enumerate(sent):
-                send[at * rows : (at + 1) * rows, to * width : (to + 1) * width] = part[
-                    block * rows : (block + 1) * rows
-                ].astype(jnp.bfloat16)
+        first = 0
+        for hidden in (early, late):
+            part = jnp.dot(hidden[...], wide[...], preferred_element_type=jnp.float32)
+            for k in range(hidden.shape[0] // rows):
+                value = part[k * rows : (k + 1) * rows]
+                block = first + k
+                if block in kept:
+                    at = kept.index(block) * rows
+                    keep[at : at + rows] = value
+                    continue
+                at = sent.index(block) * rows
+                value = value.astype(jnp.bfloat16)
+                if line_first:
+                    send[at : at + rows, :width] = value[:, width:]
+                    send[at : at + rows, width:] = value[:, :width]
+                else:
+                    send[at : at + rows] = value
+            first += hidden.shape[0] // rows
 
 
 def down_product(early, late, weights, orders):
@@ -481,11 +460,8 @@
     return pl.pallas_call(
         functools.partial(down_kernel, orders),
         out_shape=shapes,
-        in_specs=[ANYWHERE] * 2 + [LOCAL] * len(flat),
-        scratch_shapes=[
-            pltpu.VMEM((2 * half, early.shape[1]), jnp.bfloat16),
-            pltpu.SemaphoreType.DMA((2,)),
-        ],
+        scratch_shapes=[pltpu.VMEM((early.shape[1], width), jnp.bfloat16)],
+        compiler_params=room(18),
     )(early, late, *flat)
 
 
@@ -517,6 +493,7 @@
             jax.ShapeDtypeStruct((rows * len(kept), width), jnp.float32),
             jax.ShapeDtypeStruct((rows * len(sent), width), jnp.bfloat16),
         ),
+        compiler_params=room(5),
     )(ours, theirs)
 
 
@@ -538,7 +515,7 @@
             functools.partial(finish_kernel, len(kept)),
             out_shape=jax.ShapeDtypeStruct(mixed.shape, jnp.bfloat16),
             in_specs=[SMALL] + [LOCAL] * (1 + 2 * len(kept)),
-            name="finish",
+            name="finish", compiler_params=room(8),
         )(jnp.stack(sources).astype(jnp.int32), mixed, *kept, *got)
     out = jnp.zeros(mixed.shape, jnp.bfloat16)
     for k, source in enumerate(sources):

time: 469 us -> 237 us (0.51)
  Pallas kernels: 309 us -> 48.5 us
  waiting for transfers between devices: 111 us -> 140 us
  starting transfers between devices: 37.6 us -> 31.5 us
  local copies, waits for them, and re-layouts: 9.92 us -> 15.5 us
    pallas_call x5, Pallas kernels: 228 us -> 6.3 us  [pack(): pl.pallas_call(pack_kernel, out_shape=jax.ShapeDtypeStruct((len(parts),)...]
    ppermute x14, waiting for transfers between devices: 51.4 us -> 66 us  [shift(): return lax.ppermute(value, axis, moves)]
    pallas_call x3, Pallas kernels: 20.9 us -> 8.21 us  [down_product(): pl.pallas_call(functools.partial(down_kernel, orders), out_shape=shapes,...]
    ppermute x17, waiting for transfers between devices: 44.7 us -> 54.6 us  [flip(): lax.ppermute(value, axis, [(i, i ^ 1) for i in range(lax.axis_size(axis))])]
    pallas_call x4, Pallas kernels: 8.39 us -> 0.27 us  [add_blocks(): pl.pallas_call(functools.partial(add_kernel, kept, sent, turn), out_shape...]
    unnamed x63 -> x41, local copies, waits for them, and re-layouts: 6.39 us -> 11.9 us
  transfers between devices with their start and end apart: 40 -> 40, of which waited for: 15 -> 22; matrix products, arithmetic and copies ran while one was open for 1% -> 2% of each run, Pallas kernels for 65% -> 20%
where the time goes in v1:
time: 237 us; the launch traced here: 236 us
  waiting for transfers between devices  140 us (59%)
  Pallas kernels  48.5 us (20%)
  starting transfers between devices  31.5 us (13%)
  local copies, waits for them, and re-layouts  15.5 us (7%)
    ppermute x14, waiting for transfers between devices, shift(): return lax.ppermute(value, axis, moves)  66 us
    ppermute x17, waiting for transfers between devices, flip(): lax.ppermute(value, axis, [(i, i ^ 1) for i in range(lax.axis_size(axis))])  54.6 us
    ppermute x14, starting transfers between devices, shift(): return lax.ppermute(value, axis, moves)  13.1 us
    pallas_call x2, Pallas kernels, up_product(): pl.pallas_call(functools.partial(up_kernel, len(rows), steps), out_shape=...  12.6 us
    unnamed x41, local copies, waits for them, and re-layouts  11.9 us
    ppermute x7, waiting for transfers between devices, neighbour(): return lax.ppermute(value, 'sp', moves)  10.8 us
    ppermute x17, starting transfers between devices, flip(): lax.ppermute(value, axis, [(i, i ^ 1) for i in range(lax.axis_size(axis))])  10.4 us
    ppermute x2, waiting for transfers between devices, carry_shift(): return lax.ppermute(value, 'sp', moves)  8.66 us
  transfers between devices with their start and end apart: 40, of which 22 were waited for; matrix products, arithmetic and copies ran while one was open for 2% of the time, Pallas kernels for 20%

profile of v1, /device:TPU:0, one launch (start us, length us, event | category | flops | bytes accessed | tf_op | source)
XLA Modules:
  0.0 235.9 jit_solution(11606601359426549114)
XLA Ops:
  0.0 3.0 %collective-permute-start.8 = (bf16[512,2048]{1,0:T(8,128)(2,1)}, bf16[512,2048]{1,0:T(8,128)(2,1)}, u32[]{:S(2)}, u32[]{:S(2)}) collective-permute-start(bf16[512,2048]{1,0:T(8,128)(2,1)} %refs_4_.1), channel_id=1, source_target_pairs={{0,2},{1,3},{2,0},{3,1},{4,6},{5,7},{6,4},{7,5},{8,10},{9,11},{10,... | collective-permute-start | bytes 6291464 | tf_op jit(solution)/shard_map/ppermute | solution.py:33
  3.1 2.1 constant_dynamic-slice_fusion.2
  5.1 1.5 collective-permute-start.13
  6.6 2.6 %collective-permute-start.15 = (bf16[256,1024]{1,0:T(8,128)(2,1)S(1)}, bf16[256,1024]{1,0:T(8,128)(2,1)S(1)}, u32[]{:S(2)}, u32[]{:S(2)}) collective-permute-start(bf16[256,1024]{1,0:T(8,128)(2,1)S(1)} %get-tuple-element.64.refs_0_), channel_id=1, source_target_pairs={{0,16},{4,20},{8,24},{12,28},{16,0},{20,4},{24,8},{28,12},{1,17},{... | collective-permute-start | bytes 1572872 | tf_op jit(solution)/shard_map/ppermute | solution.py:33
  9.2 1.6 collective-permute-start.12
  11.1 2.5 %summary.1 = (bf16[256,640]{1,0:T(8,128)(2,1)S(1)}, bf16[256,640]{1,0:T(8,128)(2,1)S(1)}) custom-call(s32[6]{0:T(128)S(1)} %stack.72.info, bf16[768,256]{1,0:T(8,128)(2,1)S(1)} %copy-done.8, bf16[768,512]{1,0:T(8,128)(2,1)S(1)} %copy-done, f32[8,768]{1,0:T(8,128)S(1)} %maximum_maximum_fusion.gates), custom_call_target="tpu_custom_call" | custom-call | tf_op jit(solution)/shard_map/summary/pallas_call | solution.py:154
  14.2 1.3 constant_dynamic-slice_fusion
  15.5 10.0 %collective-permute-done.got.rest_0_ = bf16[256,640]{1,0:T(8,128)(2,1)S(1)} collective-permute-done((bf16[256,640]{1,0:T(8,128)(2,1)S(1)}, bf16[256,640]{1,0:T(8,128)(2,1)S(1)}, u32[]{:S(2)}, u32[]{:S(2)}) %collective-permute-start) | collective-permute-done | bytes 327712 | tf_op jit(solution)/shard_map/ppermute | solution.py:25
  25.5 1.6 collective-permute-start.22
  27.7 5.2 %collective-permute-done.12.refs_1_ = bf16[256,1024]{1,0:T(8,128)(2,1)} collective-permute-done((bf16[256,1024]{1,0:T(8,128)(2,1)}, bf16[256,1024]{1,0:T(8,128)(2,1)}, u32[]{:S(2)}, u32[]{:S(2)}) %collective-permute-start.12) | collective-permute-done | bytes 524320 | tf_op jit(solution)/shard_map/ppermute | solution.py:38
  32.9 1.3 collective-permute-start.1
  34.2 1.3 collective-permute-start.2
  35.6 13.4 %collective-permute-done.8.refs_6_ = bf16[512,2048]{1,0:T(8,128)(2,1)} collective-permute-done((bf16[512,2048]{1,0:T(8,128)(2,1)}, bf16[512,2048]{1,0:T(8,128)(2,1)}, u32[]{:S(2)}, u32[]{:S(2)}) %collective-permute-start.8) | collective-permute-done | bytes 2097184 | tf_op jit(solution)/shard_map/ppermute | solution.py:33
  49.0 8.7 %collective-permute-done.1.refs_0_.rest_1_ = bf16[256,640]{1,0:T(8,128)(2,1)S(1)} collective-permute-done((bf16[256,640]{1,0:T(8,128)(2,1)S(1)}, bf16[256,640]{1,0:T(8,128)(2,1)S(1)}, u32[]{:S(2)}, u32[]{:S(2)}) %collective-permute-start.1) | collective-permute-done | bytes 327712 | tf_op jit(solution)/shard_map/ppermute | solution.py:45
  57.7 1.6 collective-permute-start.14
  59.2 1.2 lead.1
  61.0 17.5 %collective-permute-done.3.rest_3_ = bf16[256,640]{1,0:T(8,128)(2,1)S(1)} collective-permute-done((bf16[256,640]{1,0:T(8,128)(2,1)S(1)}, bf16[256,640]{1,0:T(8,128)(2,1)S(1)}, u32[]{:S(2)}, u32[]{:S(2)}) %collective-permute-start.3) | collective-permute-done | bytes 327712 | tf_op jit(solution)/shard_map/ppermute | solution.py:25
  78.4 1.6 collective-permute-start.17
  80.0 2.5 %collective-permute-done.16.refs_1_ = bf16[256,1024]{1,0:T(8,128)(2,1)S(1)} collective-permute-done((bf16[256,1024]{1,0:T(8,128)(2,1)}, bf16[256,1024]{1,0:T(8,128)(2,1)S(1)}, u32[]{:S(2)}, u32[]{:S(2)}) %collective-permute-start.16) | collective-permute-done | bytes 524320 | tf_op jit(solution)/shard_map/ppermute | solution.py:33
  83.1 5.4 %intra.1 = (f32[768,512]{1,0:T(8,128)S(1)}, f32[768,512]{1,0:T(8,128)S(1)}, f32[768,128]{1,0:T(8,128)S(1)}) custom-call(bf16[768,256]{1,0:T(8,128)(2,1)S(1)} %copy-done.7, bf16[768,256]{1,0:T(8,128)(2,1)S(1)} %copy-done.8, bf16[768,512]{1,0:T(8,128)(2,1)S(1)} %copy-done, f32[8,768]{1,0:T(8,128)S(1)} %maximum_maximum_fusion.gates), custom_call_target="tpu_custom_call" | custom-call | tf_op jit(solution)/shard_map/intra/pallas_call | solution.py:240
  88.5 6.0 %emit.1 = (bf16[192,512]{1,0:T(8,128)(2,1)S(1)}, bf16[192,512]{1,0:T(8,128)(2,1)S(1)}, bf16[192,512]{1,0:T(8,128)(2,1)S(1)}, bf16[192,512]{1,0:T(8,128)(2,1)S(1)}) custom-call(s32[6]{0:T(128)S(1)} %stack.72.info, bf16[768,256]{1,0:T(8,128)(2,1)S(1)} %copy-done.7, f32[768,512]{1,0:T(8,128)S(1)} %get-tuple-element.33.num_f, ...), custom_call_target="tpu_custom_call" | custom-call | tf_op jit(solution)/shard_map/emit/pallas_call | solution.py:301
  94.6 1.3 shard_map.127.refs_3_.refs_1_
  96.0 6.4 %collective-permute-done.18.refs_3_ = bf16[256,1024]{1,0:T(8,128)(2,1)S(1)} collective-permute-done((bf16[256,1024]{1,0:T(8,128)(2,1)S(1)}, bf16[256,1024]{1,0:T(8,128)(2,1)S(1)}, u32[]{:S(2)}, u32[]{:S(2)}) %collective-permute-start.18) | collective-permute-done | bytes 524320 | tf_op jit(solution)/shard_map/ppermute | solution.py:25
  102.4 1.5 shard_map.128.refs_4_.refs_2_
  103.8 4.8 %collective-permute-done.28.refs_0_ = bf16[1024,256]{1,0:T(8,128)(2,1)} collective-permute-done((bf16[1024,256]{1,0:T(8,128)(2,1)S(1)}, bf16[1024,256]{1,0:T(8,128)(2,1)}, u32[]{:S(2)}, u32[]{:S(2)}) %collective-permute-start.28) | collective-permute-done | bytes 524320 | tf_op jit(solution)/shard_map/ppermute | solution.py:33
  109.2 6.7 %collective-permute-done.5.refs_2_ = bf16[192,512]{1,0:T(8,128)(2,1)S(1)} collective-permute-done((bf16[192,512]{1,0:T(8,128)(2,1)S(1)}, bf16[192,512]{1,0:T(8,128)(2,1)S(1)}, u32[]{:S(2)}, u32[]{:S(2)}) %collective-permute-start.5) | collective-permute-done | bytes 196640 | tf_op jit(solution)/shard_map/ppermute | solution.py:33
  116.6 1.1 shard_map.131.refs_0_
  117.7 5.9 %collective-permute-done.6.refs_3_ = bf16[192,512]{1,0:T(8,128)(2,1)S(1)} collective-permute-done((bf16[192,512]{1,0:T(8,128)(2,1)S(1)}, bf16[192,512]{1,0:T(8,128)(2,1)S(1)}, u32[]{:S(2)}, u32[]{:S(2)}) %collective-permute-start.6) | collective-permute-done | bytes 196640 | tf_op jit(solution)/shard_map/ppermute | solution.py:33
  124.3 1.2 collective-permute-start.24
  125.5 1.3 copy-done.3
  126.8 1.4 copy-done.5
  128.2 0.9 collective-permute-start.32
  129.2 1.6 copy-done.2
  130.8 1.6 copy-done.4
  132.4 1.6 copy-done.6
  134.0 1.1 copy-done.9
  135.1 0.9 copy-done.12
  136.0 0.9 copy-done.14
  137.0 3.8 %project.1 = (f32[192,2048]{1,0:T(8,128)S(1)}, bf16[192,2048]{1,0:T(8,128)(2,1)S(1)}, bf16[192,2048]{1,0:T(8,128)(2,1)S(1)}) custom-call(s32[8]{0:T(128)S(1)} %stack.65.info, bf16[192,512]{1,0:T(8,128)(2,1)S(1)} %get-tuple-element.38.refs_0_, bf16[192,512]{1,0:T(8,128)(2,1)S(1)} %collective-permute-done.4.refs_1_, bf16[192,512]{1,0:T(8,128)(2,1)S(1)} %copy-done.12, ...), custom_call_target="tpu_custom_call" | custom-call | tf_op jit(solution)/shard_map/project/pallas_call | solution.py:343
  140.7 11.1 %collective-permute-done.29.refs_1_ = bf16[1024,256]{1,0:T(8,128)(2,1)} collective-permute-done((bf16[1024,256]{1,0:T(8,128)(2,1)}, bf16[1024,256]{1,0:T(8,128)(2,1)}, u32[]{:S(2)}, u32[]{:S(2)}) %collective-permute-start.29) | collective-permute-done | bytes 524320 | tf_op jit(solution)/shard_map/ppermute | solution.py:33
  151.8 8.8 %collective-permute-done.32.refs_0_ = bf16[1024,256]{1,0:T(8,128)(2,1)} collective-permute-done((bf16[1024,256]{1,0:T(8,128)(2,1)}, bf16[1024,256]{1,0:T(8,128)(2,1)}, u32[]{:S(2)}, u32[]{:S(2)}) %collective-permute-start.32) | collective-permute-done | bytes 524320 | tf_op jit(solution)/shard_map/ppermute | solution.py:25
  160.7 0.9 collective-permute-start.11
  161.6 1.2 collective-permute-start.33
  162.8 11.8 %collective-permute-done.33.refs_1_ = bf16[1024,256]{1,0:T(8,128)(2,1)S(1)} collective-permute-done((bf16[1024,256]{1,0:T(8,128)(2,1)}, bf16[1024,256]{1,0:T(8,128)(2,1)S(1)}, u32[]{:S(2)}, u32[]{:S(2)}) %collective-permute-start.33) | collective-permute-done | bytes 524320 | tf_op jit(solution)/shard_map/ppermute | solution.py:25
  175.1 1.3 shard_map.135.refs_0_
  176.5 1.1 shard_map.138.refs_0_
  178.2 1.0 collective-permute-done.11.refs_2_
  179.2 1.1 collective-permute-start.21
  180.3 7.9 %shard_map.129.early = bf16[576,2048]{1,0:T(8,128)(2,1)S(1)} custom-call(bf16[192,2048]{1,0:T(8,128)(2,1)S(1)} %get-tuple-element.43.refs_0_, bf16[192,2048]{1,0:T(8,128)(2,1)S(1)} %collective-permute-done.10.refs_1_, bf16[192,2048]{1,0:T(8,128)(2,1)S(1)} %collective-permute-done.11.refs_2_, bf16[4,256,1024]{2,1,0:T(8,128)(2,1)S(1)} %shard_map.127.refs_3_.refs_1_, ...), custom_call_target="tpu_custom_call" | custom-call | tf_op jit(solution)/shard_map/pallas_call | solution.py:403
  188.2 9.5 %collective-permute-done.21.refs_0_ = bf16[192,2048]{1,0:T(8,128)(2,1)S(1)} collective-permute-done((bf16[192,2048]{1,0:T(8,128)(2,1)S(1)}, bf16[192,2048]{1,0:T(8,128)(2,1)S(1)}, u32[]{:S(2)}, u32[]{:S(2)}) %collective-permute-start.21) | collective-permute-done | bytes 786464 | tf_op jit(solution)/shard_map/ppermute | solution.py:33
  197.7 4.7 %shard_map.130.late = bf16[192,2048]{1,0:T(8,128)(2,1)S(1)} custom-call(bf16[192,2048]{1,0:T(8,128)(2,1)S(1)} %collective-permute-done.21.refs_0_, bf16[4,256,1024]{2,1,0:T(8,128)(2,1)S(1)} %shard_map.127.refs_3_.refs_1_, bf16[4,256,1024]{2,1,0:T(8,128)(2,1)} %shard_map.128.refs_4_.refs_2_, bf16[4,256,1024]{2,1,0:T(8,128)(2,1)} %collective-permute-done.19.refs_5_.refs_3_, ...), custom_call_target="tpu_custom_call" | custom-call | tf_op jit(solution)/shard_map/pallas_call | solution.py:403
  202.4 4.6 %shard_map.132 = (f32[384,512]{1,0:T(8,128)S(1)}, bf16[384,512]{1,0:T(8,128)(2,1)S(1)}, f32[384,512]{1,0:T(8,128)S(1)}, bf16[384,512]{1,0:T(8,128)(2,1)S(1)}) custom-call(bf16[576,2048]{1,0:T(8,128)(2,1)S(1)} %shard_map.129.early, bf16[192,2048]{1,0:T(8,128)(2,1)S(1)} %shard_map.130.late, bf16[2,1024,256]{2,1,0:T(8,128)(2,1)S(1)} %shard_map.131.refs_0_, ...), custom_call_target="tpu_custom_call" | custom-call | tf_op jit(solution)/shard_map/pallas_call | solution.py:460
  207.0 1.0 collective-permute-start.26
  208.1 1.8 shard_map.136
  209.9 1.1 collective-permute-start.31
  211.0 1.8 shard_map.139
  212.8 2.1 collective-permute-start.35
  214.9 4.2 %collective-permute-done.26.theirs = bf16[384,512]{1,0:T(8,128)(2,1)S(1)} collective-permute-done((bf16[384,512]{1,0:T(8,128)(2,1)S(1)}, bf16[384,512]{1,0:T(8,128)(2,1)S(1)}, u32[]{:S(2)}, u32[]{:S(2)}) %collective-permute-start.26) | collective-permute-done | bytes 393248 | tf_op jit(solution)/shard_map/ppermute | solution.py:33
  220.1 1.1 collective-permute-start.37
  221.3 6.3 %collective-permute-done.31.theirs = bf16[384,512]{1,0:T(8,128)(2,1)S(1)} collective-permute-done((bf16[384,512]{1,0:T(8,128)(2,1)S(1)}, bf16[384,512]{1,0:T(8,128)(2,1)S(1)}, u32[]{:S(2)}, u32[]{:S(2)}) %collective-permute-start.31) | collective-permute-done | bytes 393248 | tf_op jit(solution)/shard_map/ppermute | solution.py:33
  228.5 1.1 collective-permute-start.39
  229.7 1.9 collective-permute-done.36.refs_4_
  231.6 2.1 collective-permute-done.38.refs_6_
  234.3 1.7 finish.1
  (87 shorter events, 8.6 us)
Async XLA Ops:
  0.0 10.8 %copy-start.19 = (s32[768]{0:T(1024)S(1)}, s32[768]{0:T(1024)}, u32[]{:S(2)}) copy-start(s32[768]{0:T(1024)} %param.19) | copy-start | bytes 9220
  0.0 10.9 %copy-start.17 = (f32[2,1,768]{2,1,0:T(1,128)S(1)}, f32[2,1,768]{2,1,0:T(1,128)}, u32[]{:S(2)}) copy-start(f32[2,1,768]{2,1,0:T(1,128)} %param.18) | copy-start | bytes 18436
  0.0 10.9 %copy-start.18 = (f32[2,1,768]{2,1,0:T(1,128)S(1)}, f32[2,1,768]{2,1,0:T(1,128)}, u32[]{:S(2)}) copy-start(f32[2,1,768]{2,1,0:T(1,128)} %param.17) | copy-start | bytes 18436
  0.0 11.1 %copy-start.8 = (bf16[768,256]{1,0:T(8,128)(2,1)S(1)}, bf16[768,256]{1,0:T(8,128)(2,1)}, u32[]{:S(2)}) copy-start(bf16[768,256]{1,0:T(8,128)(2,1)} %keys.3) | copy-start | bytes 1179652
  0.0 11.1 %copy-start = (bf16[768,512]{1,0:T(8,128)(2,1)S(1)}, bf16[768,512]{1,0:T(8,128)(2,1)}, u32[]{:S(2)}) copy-start(bf16[768,512]{1,0:T(8,128)(2,1)} %values.3) | copy-start | bytes 2359300
  0.0 49.0 %collective-permute-start.8 = (bf16[512,2048]{1,0:T(8,128)(2,1)}, bf16[512,2048]{1,0:T(8,128)(2,1)}, u32[]{:S(2)}, u32[]{:S(2)}) collective-permute-start(bf16[512,2048]{1,0:T(8,128)(2,1)} %refs_4_.1), channel_id=1, source_target_pairs={{0,2},{1,3},{2,0},{3,1},{4,6},{5,7},{6,4},{7,5},{8,10},{9,11},{10,... | collective-permute-start | bytes 6291464 | tf_op jit(solution)/shard_map/ppermute | solution.py:33
  5.1 29.1 %collective-permute-start.13 = (bf16[256,1024]{1,0:T(8,128)(2,1)S(1)}, bf16[256,1024]{1,0:T(8,128)(2,1)}, u32[]{:S(2)}, u32[]{:S(2)}) collective-permute-start(bf16[256,1024]{1,0:T(8,128)(2,1)S(1)} %get-tuple-element.64.refs_0_), channel_id=1, source_target_pairs={{0,4},{4,0},{8,12},{12,8},{16,20},{20,16},{24,28},{28,24},{1,5},{5... | collective-permute-start | bytes 1572872 | tf_op jit(solution)/shard_map/ppermute | solution.py:25
  6.6 28.9 %collective-permute-start.15 = (bf16[256,1024]{1,0:T(8,128)(2,1)S(1)}, bf16[256,1024]{1,0:T(8,128)(2,1)S(1)}, u32[]{:S(2)}, u32[]{:S(2)}) collective-permute-start(bf16[256,1024]{1,0:T(8,128)(2,1)S(1)} %get-tuple-element.64.refs_0_), channel_id=1, source_target_pairs={{0,16},{4,20},{8,24},{12,28},{16,0},{20,4},{24,8},{28,12},{1,17},{... | collective-permute-start | bytes 1572872 | tf_op jit(solution)/shard_map/ppermute | solution.py:33
  9.2 23.7 %collective-permute-start.12 = (bf16[256,1024]{1,0:T(8,128)(2,1)}, bf16[256,1024]{1,0:T(8,128)(2,1)}, u32[]{:S(2)}, u32[]{:S(2)}) collective-permute-start(bf16[256,1024]{1,0:T(8,128)(2,1)} %get-tuple-element.63), channel_id=1, source_target_pairs={{0,8},{4,12},{8,0},{12,4},{16,24},{20,28},{24,16},{28,20},{1,9},{5... | collective-permute-start | bytes 1572872 | tf_op jit(solution)/shard_map/ppermute | solution.py:38
  11.1 24.4 %copy-start.1 = (bf16[512,2048]{1,0:T(8,128)(2,1)S(1)}, bf16[512,2048]{1,0:T(8,128)(2,1)}, u32[]{:S(2)}) copy-start(bf16[512,2048]{1,0:T(8,128)(2,1)} %refs_4_.1) | copy-start | bytes 6291460
  13.6 69.5 %copy-start.7 = (bf16[768,256]{1,0:T(8,128)(2,1)S(1)}, bf16[768,256]{1,0:T(8,128)(2,1)}, u32[]{:S(2)}) copy-start(bf16[768,256]{1,0:T(8,128)(2,1)} %queries.3) | copy-start | bytes 1179652
  13.6 11.9 %collective-permute-start = (bf16[256,640]{1,0:T(8,128)(2,1)S(1)}, bf16[256,640]{1,0:T(8,128)(2,1)S(1)}, u32[]{:S(2)}, u32[]{:S(2)}) collective-permute-start(bf16[256,640]{1,0:T(8,128)(2,1)S(1)} %get-tuple-element.36), channel_id=1, source_target_pairs={{0,4},{4,0},{8,12},{12,8},{16,20},{20,16},{24,28},{28,24},{1,5},{5... | collective-permute-start | bytes 983048 | tf_op jit(solution)/shard_map/ppermute | solution.py:25
  15.5 73.0 %copy-start.10 = (bf16[768,512]{1,0:T(8,128)(2,1)S(1)}, bf16[768,512]{1,0:T(8,128)(2,1)}, u32[]{:S(2)}) copy-start(bf16[768,512]{1,0:T(8,128)(2,1)} %out_gate.1) | copy-start | bytes 2359300
  15.5 73.0 %copy-start.16 = (f32[512]{0:T(512)S(1)}, f32[512]{0:T(512)}, u32[]{:S(2)}) copy-start(f32[512]{0:T(512)} %param.20) | copy-start | bytes 6148
  25.5 34.9 %collective-permute-start.22 = (bf16[1024,256]{1,0:T(8,128)(2,1)S(1)}, bf16[1024,256]{1,0:T(8,128)(2,1)}, u32[]{:S(2)}, u32[]{:S(2)}) collective-permute-start(bf16[1024,256]{1,0:T(8,128)(2,1)S(1)} %get-tuple-element.61), channel_id=1, source_target_pairs={{0,8},{4,12},{8,0},{12,4},{16,24},{20,28},{24,16},{28,20},{1,9},{5... | collective-permute-start | bytes 1572872 | tf_op jit(solution)/shard_map/ppermute | solution.py:38
  32.9 24.7 %collective-permute-start.1 = (bf16[256,640]{1,0:T(8,128)(2,1)S(1)}, bf16[256,640]{1,0:T(8,128)(2,1)S(1)}, u32[]{:S(2)}, u32[]{:S(2)}) collective-permute-start(bf16[256,640]{1,0:T(8,128)(2,1)S(1)} %pair.1), channel_id=1, source_target_pairs={{8,0},{16,8},{24,16},{4,12},{12,20},{20,28},{9,1},{17,9},{25,17},{... | collective-permute-start | bytes 983048 | tf_op jit(solution)/shard_map/ppermute | solution.py:45
  34.2 23.5 %collective-permute-start.2 = (bf16[256,640]{1,0:T(8,128)(2,1)S(1)}, bf16[256,640]{1,0:T(8,128)(2,1)S(1)}, u32[]{:S(2)}, u32[]{:S(2)}) collective-permute-start(bf16[256,640]{1,0:T(8,128)(2,1)S(1)} %pair.1), channel_id=1, source_target_pairs={{16,0},{24,8},{4,20},{12,28},{17,1},{25,9},{5,21},{13,29},{18,2},{... | collective-permute-start | bytes 983048 | tf_op jit(solution)/shard_map/ppermute | solution.py:45
  35.5 89.9 %collective-permute-start.7 = (bf16[512,2048]{1,0:T(8,128)(2,1)S(1)}, bf16[512,2048]{1,0:T(8,128)(2,1)S(1)}, u32[]{:S(2)}, u32[]{:S(2)}) collective-permute-start(bf16[512,2048]{1,0:T(8,128)(2,1)S(1)} %copy-done.1), channel_id=1, source_target_pairs={{0,1},{1,0},{2,3},{3,2},{4,5},{5,4},{6,7},{7,6},{8,9},{9,8},{10,11... | collective-permute-start | bytes 6291464 | tf_op jit(solution)/shard_map/ppermute | solution.py:25
  49.0 77.8 %collective-permute-start.9 = (bf16[512,2048]{1,0:T(8,128)(2,1)}, bf16[512,2048]{1,0:T(8,128)(2,1)S(1)}, u32[]{:S(2)}, u32[]{:S(2)}) collective-permute-start(bf16[512,2048]{1,0:T(8,128)(2,1)} %collective-permute-done.8.refs_6_), channel_id=1, source_target_pairs={{0,1},{1,0},{2,3},{3,2},{4,5},{5,4},{6,7},{7,6},{8,9},{9,8},{10,11... | collective-permute-start | bytes 6291464 | tf_op jit(solution)/shard_map/ppermute | solution.py:25
  57.7 24.9 %collective-permute-start.16 = (bf16[256,1024]{1,0:T(8,128)(2,1)}, bf16[256,1024]{1,0:T(8,128)(2,1)S(1)}, u32[]{:S(2)}, u32[]{:S(2)}) collective-permute-start(bf16[256,1024]{1,0:T(8,128)(2,1)} %collective-permute-done.12.refs_1_), channel_id=1, source_target_pairs={{0,16},{4,20},{8,24},{12,28},{16,0},{20,4},{24,8},{28,12},{1,17},{... | collective-permute-start | bytes 1572872 | tf_op jit(solution)/shard_map/ppermute | solution.py:33
  57.7 25.1 %collective-permute-start.14 = (bf16[256,1024]{1,0:T(8,128)(2,1)}, bf16[256,1024]{1,0:T(8,128)(2,1)S(1)}, u32[]{:S(2)}, u32[]{:S(2)}) collective-permute-start(bf16[256,1024]{1,0:T(8,128)(2,1)} %collective-permute-done.12.refs_1_), channel_id=1, source_target_pairs={{0,4},{4,0},{8,12},{12,8},{16,20},{20,16},{24,28},{28,24},{1,5},{5... | collective-permute-start | bytes 1572872 | tf_op jit(solution)/shard_map/ppermute | solution.py:25
  60.4 18.0 %collective-permute-start.3 = (bf16[256,640]{1,0:T(8,128)(2,1)S(1)}, bf16[256,640]{1,0:T(8,128)(2,1)S(1)}, u32[]{:S(2)}, u32[]{:S(2)}) collective-permute-start(bf16[256,640]{1,0:T(8,128)(2,1)S(1)} %lead.1), channel_id=1, source_target_pairs={{0,4},{4,0},{8,12},{12,8},{16,20},{20,16},{24,28},{28,24},{1,5},{5... | collective-permute-start | bytes 983048 | tf_op jit(solution)/shard_map/ppermute | solution.py:25
  78.4 16.1 %collective-permute-start.17 = (bf16[256,1024]{1,0:T(8,128)(2,1)S(1)}, bf16[256,1024]{1,0:T(8,128)(2,1)S(1)}, u32[]{:S(2)}, u32[]{:S(2)}) collective-permute-start(bf16[256,1024]{1,0:T(8,128)(2,1)S(1)} %collective-permute-done.15.refs_0_), channel_id=1, source_target_pairs={{0,4},{4,0},{8,12},{12,8},{16,20},{20,16},{24,28},{28,24},{1,5},{5... | collective-permute-start | bytes 1572872 | tf_op jit(solution)/shard_map/ppermute | solution.py:25
  82.5 19.8 %collective-permute-start.18 = (bf16[256,1024]{1,0:T(8,128)(2,1)S(1)}, bf16[256,1024]{1,0:T(8,128)(2,1)S(1)}, u32[]{:S(2)}, u32[]{:S(2)}) collective-permute-start(bf16[256,1024]{1,0:T(8,128)(2,1)S(1)} %collective-permute-done.16.refs_1_), channel_id=1, source_target_pairs={{0,4},{4,0},{8,12},{12,8},{16,20},{20,16},{24,28},{28,24},{1,5},{5... | collective-permute-start | bytes 1572872 | tf_op jit(solution)/shard_map/ppermute | solution.py:25
  82.8 25.8 %collective-permute-start.28 = (bf16[1024,256]{1,0:T(8,128)(2,1)S(1)}, bf16[1024,256]{1,0:T(8,128)(2,1)}, u32[]{:S(2)}, u32[]{:S(2)}) collective-permute-start(bf16[1024,256]{1,0:T(8,128)(2,1)S(1)} %get-tuple-element.62.refs_0_), channel_id=1, source_target_pairs={{0,16},{4,20},{8,24},{12,28},{16,0},{20,4},{24,8},{28,12},{1,17},{... | collective-permute-start | bytes 1572872 | tf_op jit(solution)/shard_map/ppermute | solution.py:33
  94.6 14.1 %collective-permute-start.4 = (bf16[192,512]{1,0:T(8,128)(2,1)S(1)}, bf16[192,512]{1,0:T(8,128)(2,1)S(1)}, u32[]{:S(2)}, u32[]{:S(2)}) collective-permute-start(bf16[192,512]{1,0:T(8,128)(2,1)S(1)} %get-tuple-element.39), channel_id=1, source_target_pairs={{0,1},{1,0},{2,3},{3,2},{4,5},{5,4},{6,7},{7,6},{8,9},{9,8},{10,11... | collective-permute-start | bytes 589832 | tf_op jit(solution)/shard_map/ppermute | solution.py:33
  102.4 72.3 %collective-permute-start.19 = (bf16[4,256,1024]{2,1,0:T(8,128)(2,1)S(1)}, bf16[4,256,1024]{2,1,0:T(8,128)(2,1)}, u32[]{:S(2)}, u32[]{:S(2)}) collective-permute-start(bf16[4,256,1024]{2,1,0:T(8,128)(2,1)S(1)} %shard_map.127.refs_3_.refs_1_), channel_id=1, source_target_pairs={{0,1},{1,0},{2,3},{3,2},{4,5},{5,4},{6,7},{7,6},{8,9},{9,8},{10,11... | collective-permute-start | bytes 6291464 | tf_op jit(solution)/shard_map/ppermute | solution.py:25
  103.8 25.4 %copy-start.15 = (f32[2048]{0:T(1024)S(1)}, f32[2048]{0:T(1024)}, u32[]{:S(2)}) copy-start(f32[2048]{0:T(1024)} %param.23) | copy-start | bytes 24580
  108.6 67.8 %collective-permute-start.20 = (bf16[4,256,1024]{2,1,0:T(8,128)(2,1)}, bf16[4,256,1024]{2,1,0:T(8,128)(2,1)}, u32[]{:S(2)}, u32[]{:S(2)}) collective-permute-start(bf16[4,256,1024]{2,1,0:T(8,128)(2,1)} %shard_map.128.refs_4_.refs_2_), channel_id=1, source_target_pairs={{0,1},{1,0},{2,3},{3,2},{4,5},{5,4},{6,7},{7,6},{8,9},{9,8},{10,11... | collective-permute-start | bytes 6291464 | tf_op jit(solution)/shard_map/ppermute | solution.py:25
  108.6 7.3 %collective-permute-start.5 = (bf16[192,512]{1,0:T(8,128)(2,1)S(1)}, bf16[192,512]{1,0:T(8,128)(2,1)S(1)}, u32[]{:S(2)}, u32[]{:S(2)}) collective-permute-start(bf16[192,512]{1,0:T(8,128)(2,1)S(1)} %get-tuple-element.40), channel_id=1, source_target_pairs={{0,2},{1,3},{2,0},{3,1},{4,6},{5,7},{6,4},{7,5},{8,10},{9,11},{10,... | collective-permute-start | bytes 589832 | tf_op jit(solution)/shard_map/ppermute | solution.py:33
  115.9 0.7 copy-start.11
  116.6 7.0 %collective-permute-start.6 = (bf16[192,512]{1,0:T(8,128)(2,1)S(1)}, bf16[192,512]{1,0:T(8,128)(2,1)S(1)}, u32[]{:S(2)}, u32[]{:S(2)}) collective-permute-start(bf16[192,512]{1,0:T(8,128)(2,1)S(1)} %get-tuple-element.41), channel_id=1, source_target_pairs={{0,3},{1,2},{2,1},{3,0},{4,7},{5,6},{6,5},{7,4},{8,11},{9,10},{10,... | collective-permute-start | bytes 589832 | tf_op jit(solution)/shard_map/ppermute | solution.py:33
  123.7 0.7 copy-start.13
  124.3 37.3 %collective-permute-start.24 = (bf16[2,1024,256]{2,1,0:T(8,128)(2,1)S(1)}, bf16[2,1024,256]{2,1,0:T(8,128)(2,1)}, u32[]{:S(2)}, u32[]{:S(2)}) collective-permute-start(bf16[2,1024,256]{2,1,0:T(8,128)(2,1)S(1)} %shard_map.131.refs_0_), channel_id=1, source_target_pairs={{0,4},{4,0},{8,12},{12,8},{16,20},{20,16},{24,28},{28,24},{1,5},{5... | collective-permute-start | bytes 3145736 | tf_op jit(solution)/shard_map/ppermute | solution.py:25
  125.5 1.3 copy-start.3
  126.8 25.0 %collective-permute-start.29 = (bf16[1024,256]{1,0:T(8,128)(2,1)}, bf16[1024,256]{1,0:T(8,128)(2,1)}, u32[]{:S(2)}, u32[]{:S(2)}) collective-permute-start(bf16[1024,256]{1,0:T(8,128)(2,1)} %collective-permute-done.22.refs_1_), channel_id=1, source_target_pairs={{0,16},{4,20},{8,24},{12,28},{16,0},{20,4},{24,8},{28,12},{1,17},{... | collective-permute-start | bytes 1572872 | tf_op jit(solution)/shard_map/ppermute | solution.py:33
  126.8 1.4 copy-start.5
  128.2 32.4 %collective-permute-start.32 = (bf16[1024,256]{1,0:T(8,128)(2,1)}, bf16[1024,256]{1,0:T(8,128)(2,1)}, u32[]{:S(2)}, u32[]{:S(2)}) collective-permute-start(bf16[1024,256]{1,0:T(8,128)(2,1)} %collective-permute-done.28.refs_0_), channel_id=1, source_target_pairs={{0,4},{4,0},{8,12},{12,8},{16,20},{20,16},{24,28},{28,24},{1,5},{5... | collective-permute-start | bytes 1572872 | tf_op jit(solution)/shard_map/ppermute | solution.py:25
  129.2 1.6 copy-start.2
  130.8 1.6 copy-start.4
  132.4 1.6 copy-start.6
  134.0 1.1 copy-start.9
  135.1 0.9 copy-start.12
  136.0 0.9 copy-start.14
  151.8 25.8 %collective-permute-start.10 = (bf16[192,2048]{1,0:T(8,128)(2,1)S(1)}, bf16[192,2048]{1,0:T(8,128)(2,1)S(1)}, u32[]{:S(2)}, u32[]{:S(2)}) collective-permute-start(bf16[192,2048]{1,0:T(8,128)(2,1)S(1)} %get-tuple-element.44), channel_id=1, source_target_pairs={{0,8},{4,12},{8,0},{12,4},{16,24},{20,28},{24,16},{28,20},{1,9},{5... | collective-permute-start | bytes 2359304 | tf_op jit(solution)/shard_map/ppermute | solution.py:38
  160.7 18.5 %collective-permute-start.11 = (bf16[192,2048]{1,0:T(8,128)(2,1)S(1)}, bf16[192,2048]{1,0:T(8,128)(2,1)S(1)}, u32[]{:S(2)}, u32[]{:S(2)}) collective-permute-start(bf16[192,2048]{1,0:T(8,128)(2,1)S(1)} %get-tuple-element.43.refs_0_), channel_id=1, source_target_pairs={{0,2},{1,3},{2,0},{3,1},{4,6},{5,7},{6,4},{7,5},{8,10},{9,11},{10,... | collective-permute-start | bytes 2359304 | tf_op jit(solution)/shard_map/ppermute | solution.py:33
  161.6 13.0 %collective-permute-start.33 = (bf16[1024,256]{1,0:T(8,128)(2,1)}, bf16[1024,256]{1,0:T(8,128)(2,1)S(1)}, u32[]{:S(2)}, u32[]{:S(2)}) collective-permute-start(bf16[1024,256]{1,0:T(8,128)(2,1)} %collective-permute-done.29.refs_1_), channel_id=1, source_target_pairs={{0,4},{4,0},{8,12},{12,8},{16,20},{20,16},{24,28},{28,24},{1,5},{5... | collective-permute-start | bytes 1572872 | tf_op jit(solution)/shard_map/ppermute | solution.py:25
  174.6 27.8 %collective-permute-start.23 = (bf16[2,1024,256]{2,1,0:T(8,128)(2,1)S(1)}, bf16[2,1024,256]{2,1,0:T(8,128)(2,1)S(1)}, u32[]{:S(2)}, u32[]{:S(2)}) collective-permute-start(bf16[2,1024,256]{2,1,0:T(8,128)(2,1)S(1)} %shard_map.131.refs_0_), channel_id=1, source_target_pairs={{0,1},{1,0},{2,3},{3,2},{4,5},{5,4},{6,7},{7,6},{8,9},{9,8},{10,11... | collective-permute-start | bytes 3145736 | tf_op jit(solution)/shard_map/ppermute | solution.py:25
  174.6 27.8 %collective-permute-start.25 = (bf16[2,1024,256]{2,1,0:T(8,128)(2,1)}, bf16[2,1024,256]{2,1,0:T(8,128)(2,1)S(1)}, u32[]{:S(2)}, u32[]{:S(2)}) collective-permute-start(bf16[2,1024,256]{2,1,0:T(8,128)(2,1)} %collective-permute-done.24.refs_2_), channel_id=1, source_target_pairs={{0,1},{1,0},{2,3},{3,2},{4,5},{5,4},{6,7},{7,6},{8,9},{9,8},{10,11... | collective-permute-start | bytes 3145736 | tf_op jit(solution)/shard_map/ppermute | solution.py:25
  176.4 31.7 %collective-permute-start.30 = (bf16[2,1024,256]{2,1,0:T(8,128)(2,1)S(1)}, bf16[2,1024,256]{2,1,0:T(8,128)(2,1)S(1)}, u32[]{:S(2)}, u32[]{:S(2)}) collective-permute-start(bf16[2,1024,256]{2,1,0:T(8,128)(2,1)S(1)} %shard_map.135.refs_0_), channel_id=1, source_target_pairs={{0,1},{1,0},{2,3},{3,2},{4,5},{5,4},{6,7},{7,6},{8,9},{9,8},{10,11... | collective-permute-start | bytes 3145736 | tf_op jit(solution)/shard_map/ppermute | solution.py:25
  177.6 33.4 %collective-permute-start.34 = (bf16[2,1024,256]{2,1,0:T(8,128)(2,1)S(1)}, bf16[2,1024,256]{2,1,0:T(8,128)(2,1)S(1)}, u32[]{:S(2)}, u32[]{:S(2)}) collective-permute-start(bf16[2,1024,256]{2,1,0:T(8,128)(2,1)S(1)} %shard_map.138.refs_0_), channel_id=1, source_target_pairs={{0,1},{1,0},{2,3},{3,2},{4,5},{5,4},{6,7},{7,6},{8,9},{9,8},{10,11... | collective-permute-start | bytes 3145736 | tf_op jit(solution)/shard_map/ppermute | solution.py:25
  179.2 18.5 %collective-permute-start.21 = (bf16[192,2048]{1,0:T(8,128)(2,1)S(1)}, bf16[192,2048]{1,0:T(8,128)(2,1)S(1)}, u32[]{:S(2)}, u32[]{:S(2)}) collective-permute-start(bf16[192,2048]{1,0:T(8,128)(2,1)S(1)} %collective-permute-done.10.refs_1_), channel_id=1, source_target_pairs={{0,2},{1,3},{2,0},{3,1},{4,6},{5,7},{6,4},{7,5},{8,10},{9,11},{10,... | collective-permute-start | bytes 2359304 | tf_op jit(solution)/shard_map/ppermute | solution.py:33
  207.0 12.1 %collective-permute-start.26 = (bf16[384,512]{1,0:T(8,128)(2,1)S(1)}, bf16[384,512]{1,0:T(8,128)(2,1)S(1)}, u32[]{:S(2)}, u32[]{:S(2)}) collective-permute-start(bf16[384,512]{1,0:T(8,128)(2,1)S(1)} %get-tuple-element.46), channel_id=1, source_target_pairs={{0,2},{1,3},{2,0},{3,1},{4,6},{5,7},{6,4},{7,5},{8,10},{9,11},{10,... | collective-permute-start | bytes 1179656 | tf_op jit(solution)/shard_map/ppermute | solution.py:33
  208.1 12.0 %collective-permute-start.27 = (bf16[384,512]{1,0:T(8,128)(2,1)S(1)}, bf16[384,512]{1,0:T(8,128)(2,1)S(1)}, u32[]{:S(2)}, u32[]{:S(2)}) collective-permute-start(bf16[384,512]{1,0:T(8,128)(2,1)S(1)} %get-tuple-element.49), channel_id=1, source_target_pairs={{0,8},{4,12},{8,0},{12,4},{16,24},{20,28},{24,16},{28,20},{1,9},{5... | collective-permute-start | bytes 1179656 | tf_op jit(solution)/shard_map/ppermute | solution.py:38
  209.9 17.7 %collective-permute-start.31 = (bf16[384,512]{1,0:T(8,128)(2,1)S(1)}, bf16[384,512]{1,0:T(8,128)(2,1)S(1)}, u32[]{:S(2)}, u32[]{:S(2)}) collective-permute-start(bf16[384,512]{1,0:T(8,128)(2,1)S(1)} %get-tuple-element.52), channel_id=1, source_target_pairs={{0,2},{1,3},{2,0},{3,1},{4,6},{5,7},{6,4},{7,5},{8,10},{9,11},{10,... | collective-permute-start | bytes 1179656 | tf_op jit(solution)/shard_map/ppermute | solution.py:33
  212.8 15.7 %collective-permute-start.35 = (bf16[384,512]{1,0:T(8,128)(2,1)S(1)}, bf16[384,512]{1,0:T(8,128)(2,1)S(1)}, u32[]{:S(2)}, u32[]{:S(2)}) collective-permute-start(bf16[384,512]{1,0:T(8,128)(2,1)S(1)} %get-tuple-element.55), channel_id=1, source_target_pairs={{0,8},{4,12},{8,0},{12,4},{16,24},{20,28},{24,16},{28,20},{1,9},{5... | collective-permute-start | bytes 1179656 | tf_op jit(solution)/shard_map/ppermute | solution.py:38
  219.2 12.4 %collective-permute-start.36 = (bf16[192,512]{1,0:T(8,128)(2,1)S(1)}, bf16[192,512]{1,0:T(8,128)(2,1)S(1)}, u32[]{:S(2)}, u32[]{:S(2)}) collective-permute-start(bf16[192,512]{1,0:T(8,128)(2,1)S(1)} %get-tuple-element.57), channel_id=1, source_target_pairs={{0,8},{4,12},{8,0},{12,4},{16,24},{20,28},{24,16},{28,20},{1,9},{5... | collective-permute-start | bytes 589832 | tf_op jit(solution)/shard_map/ppermute | solution.py:38
  220.1 11.5 %collective-permute-start.37 = (bf16[192,512]{1,0:T(8,128)(2,1)S(1)}, bf16[192,512]{1,0:T(8,128)(2,1)S(1)}, u32[]{:S(2)}, u32[]{:S(2)}) collective-permute-start(bf16[192,512]{1,0:T(8,128)(2,1)S(1)} %get-tuple-element.58), channel_id=1, source_target_pairs={{0,2},{1,3},{2,0},{3,1},{4,6},{5,7},{6,4},{7,5},{8,10},{9,11},{10,... | collective-permute-start | bytes 589832 | tf_op jit(solution)/shard_map/ppermute | solution.py:33
  227.6 6.1 %collective-permute-start.38 = (bf16[192,512]{1,0:T(8,128)(2,1)S(1)}, bf16[192,512]{1,0:T(8,128)(2,1)S(1)}, u32[]{:S(2)}, u32[]{:S(2)}) collective-permute-start(bf16[192,512]{1,0:T(8,128)(2,1)S(1)} %get-tuple-element.59), channel_id=1, source_target_pairs={{0,8},{4,12},{8,0},{12,4},{16,24},{20,28},{24,16},{28,20},{1,9},{5... | collective-permute-start | bytes 589832 | tf_op jit(solution)/shard_map/ppermute | solution.py:38
  228.5 5.7 %collective-permute-start.39 = (bf16[192,512]{1,0:T(8,128)(2,1)S(1)}, bf16[192,512]{1,0:T(8,128)(2,1)S(1)}, u32[]{:S(2)}, u32[]{:S(2)}) collective-permute-start(bf16[192,512]{1,0:T(8,128)(2,1)S(1)} %get-tuple-element.60), channel_id=1, source_target_pairs={{0,2},{1,3},{2,0},{3,1},{4,6},{5,7},{6,4},{7,5},{8,10},{9,11},{10,... | collective-permute-start | bytes 589832 | tf_op jit(solution)/shard_map/ppermute | solution.py:33

commit v2 on v1

--- a/solution.py
+++ b/solution.py
@@ -35,6 +35,12 @@
 
 def neighbour(value):
     moves = [(i, i ^ 2) for i in range(lax.axis_size("sp"))]
+    return lax.ppermute(value, "sp", moves)
+
+
+def skew(value):
+    outer = lax.axis_size("sp") // 2
+    moves = [(2 * a + c, 2 * (((a + 2) % outer) ^ 1) + c) for a in range(outer) for c in range(2)]
     return lax.ppermute(value, "sp", moves)
 
 
@@ -570,8 +576,13 @@
     kept = lax.dynamic_slice_in_dim(shard, (a % 2) * size, size, dim)
     given = lax.dynamic_slice_in_dim(shard, (1 - a % 2) * size, size, dim)
     steps = [[kept, neighbour(given)]]
-    for _ in range(1, outer // 2):
-        steps.append([shift(x, "sp", 2) for x in steps[-1]])
+    for step in range(1, outer // 2):
+        first = shift(steps[-1][0], "sp", 2)
+        if step == 1:
+            second = skew(given)
+        else:
+            second = shift(steps[-1][1], "sp", 2)
+        steps.append([first, second])
     return steps
 
 
@@ -591,13 +602,10 @@
 
 def down_shards(shard):
     got = []
-    for step, here in enumerate(half_shards(shard, 0)):
+    for here in half_shards(shard, 0):
         packed = pack(here)
-        if step == 0:
-            there = flip(packed, "sp")
-        else:
-            there = [flip(x, "sp") for x in here]
-            there = pack(there)
+        there = [flip(x, "sp") for x in here]
+        there = pack(there)
         got.append(both_cores(packed))
         got.append(both_cores(there))
     return got

time: 237 us -> 242 us (1.021)
  starting transfers between devices: 31.5 us -> 44 us
  waiting for transfers between devices: 140 us -> 131 us
  local copies, waits for them, and re-layouts: 15.5 us -> 18.9 us
    ppermute x7, waiting for transfers between devices: 10.8 us -> 26.5 us  [neighbour(): return lax.ppermute(value, 'sp', moves)]
    ppermute x17 -> x18, waiting for transfers between devices: 54.6 us -> 39.7 us  [flip(): lax.ppermute(value, axis, [(i, i ^ 1) for i in range(lax.axis_size(axis))])]
    ppermute x14 -> x12, waiting for transfers between devices: 66 us -> 51.9 us  [shift(): return lax.ppermute(value, axis, moves)]
    ppermute x0 -> x2, starting transfers between devices: none -> 5.18 us  [skew(): return lax.ppermute(value, 'sp', moves)]
    ppermute x2, waiting for transfers between devices: 8.66 us -> 13.2 us  [carry_shift(): return lax.ppermute(value, 'sp', moves)]
    unnamed x41 -> x49, local copies, waits for them, and re-layouts: 11.9 us -> 16.4 us
    ppermute x17 -> x18, starting transfers between devices: 10.4 us -> 14.7 us  [flip(): lax.ppermute(value, axis, [(i, i ^ 1) for i in range(lax.axis_size(axis))])]
    ppermute x7, starting transfers between devices: 5.39 us -> 8.93 us  [neighbour(): return lax.ppermute(value, 'sp', moves)]
  transfers between devices with their start and end apart: 40 -> 41, of which waited for: 22 -> 20; matrix products, arithmetic and copies ran while one was open for 2% -> 2% of each run, Pallas kernels for 20% -> 18%
where the time goes in v2:
time: 242 us; the launch traced here: 241 us
  waiting for transfers between devices  131 us (54%)
  Pallas kernels  46.2 us (19%)
  starting transfers between devices  44 us (18%)
  local copies, waits for them, and re-layouts  18.9 us (8%)
    ppermute x12, waiting for transfers between devices, shift(): return lax.ppermute(value, axis, moves)  51.9 us
    ppermute x18, waiting for transfers between devices, flip(): lax.ppermute(value, axis, [(i, i ^ 1) for i in range(lax.axis_size(axis))])  39.7 us
    ppermute x7, waiting for transfers between devices, neighbour(): return lax.ppermute(value, 'sp', moves)  26.5 us
    unnamed x49, local copies, waits for them, and re-layouts  16.4 us
    ppermute x18, starting transfers between devices, flip(): lax.ppermute(value, axis, [(i, i ^ 1) for i in range(lax.axis_size(axis))])  14.7 us
    ppermute x2, waiting for transfers between devices, carry_shift(): return lax.ppermute(value, 'sp', moves)  13.2 us
    ppermute x12, starting transfers between devices, shift(): return lax.ppermute(value, axis, moves)  12.6 us
    pallas_call x2, Pallas kernels, up_product(): pl.pallas_call(functools.partial(up_kernel, len(rows), steps), out_shape=...  12.6 us
  transfers between devices with their start and end apart: 41, of which 20 were waited for; matrix products, arithmetic and copies ran while one was open for 2% of the time, Pallas kernels for 18%

profile of v2, /device:TPU:0, one launch (start us, length us, event | category | flops | bytes accessed | tf_op | source)
XLA Modules:
  0.0 241.5 jit_solution(712912212754937052)
XLA Ops:
  0.0 3.0 %collective-permute-start.8 = (bf16[512,2048]{1,0:T(8,128)(2,1)}, bf16[512,2048]{1,0:T(8,128)(2,1)}, u32[]{:S(2)}, u32[]{:S(2)}) collective-permute-start(bf16[512,2048]{1,0:T(8,128)(2,1)} %refs_4_.1), channel_id=1, source_target_pairs={{0,2},{1,3},{2,0},{3,1},{4,6},{5,7},{6,4},{7,5},{8,10},{9,11},{10,... | collective-permute-start | bytes 6291464 | tf_op jit(solution)/shard_map/ppermute | solution.py:33
  4.6 1.1 copy-done
  5.8 1.0 copy-done.9
  6.7 2.5 %summary.1 = (bf16[256,640]{1,0:T(8,128)(2,1)S(1)}, bf16[256,640]{1,0:T(8,128)(2,1)S(1)}) custom-call(s32[6]{0:T(128)S(1)} %stack.72.info, bf16[768,256]{1,0:T(8,128)(2,1)S(1)} %copy-done.9, bf16[768,512]{1,0:T(8,128)(2,1)S(1)} %copy-done, f32[8,768]{1,0:T(8,128)S(1)} %maximum_maximum_fusion.gates), custom_call_target="tpu_custom_call" | custom-call | tf_op jit(solution)/shard_map/summary/pallas_call | solution.py:160
  9.3 1.6 collective-permute-start
  10.8 1.4 constant_dynamic-slice_fusion.2
  12.3 1.6 collective-permute-start.12
  14.4 2.6 %collective-permute-start.15 = (bf16[256,1024]{1,0:T(8,128)(2,1)S(1)}, bf16[256,1024]{1,0:T(8,128)(2,1)S(1)}, u32[]{:S(2)}, u32[]{:S(2)}) collective-permute-start(bf16[256,1024]{1,0:T(8,128)(2,1)S(1)} %get-tuple-element.64.refs_0_), channel_id=1, source_target_pairs={{0,16},{4,20},{8,24},{12,28},{16,0},{20,4},{24,8},{28,12},{1,17},{... | collective-permute-start | bytes 1572872 | tf_op jit(solution)/shard_map/ppermute | solution.py:33
  17.0 2.9 %collective-permute-done.got.rest_0_ = bf16[256,640]{1,0:T(8,128)(2,1)S(1)} collective-permute-done((bf16[256,640]{1,0:T(8,128)(2,1)S(1)}, bf16[256,640]{1,0:T(8,128)(2,1)S(1)}, u32[]{:S(2)}, u32[]{:S(2)}) %collective-permute-start) | collective-permute-done | bytes 327712 | tf_op jit(solution)/shard_map/ppermute | solution.py:25
  19.9 3.6 %collective-permute-start.16 = (bf16[256,1024]{1,0:T(8,128)(2,1)S(1)}, bf16[256,1024]{1,0:T(8,128)(2,1)S(1)}, u32[]{:S(2)}, u32[]{:S(2)}) collective-permute-start(bf16[256,1024]{1,0:T(8,128)(2,1)S(1)} %get-tuple-element.63), channel_id=1, source_target_pairs={{0,24},{4,28},{8,16},{12,20},{16,8},{20,12},{24,0},{28,4},{1,25},{... | collective-permute-start | bytes 1572872 | tf_op jit(solution)/shard_map/ppermute | solution.py:44
  23.5 0.9 constant_dynamic-slice_fusion
  24.4 11.0 %collective-permute-done.12.refs_1_ = bf16[256,1024]{1,0:T(8,128)(2,1)S(1)} collective-permute-done((bf16[256,1024]{1,0:T(8,128)(2,1)S(1)}, bf16[256,1024]{1,0:T(8,128)(2,1)S(1)}, u32[]{:S(2)}, u32[]{:S(2)}) %collective-permute-start.12) | collective-permute-done | bytes 524320 | tf_op jit(solution)/shard_map/ppermute | solution.py:38
  36.0 16.6 %collective-permute-done.15.refs_0_ = bf16[256,1024]{1,0:T(8,128)(2,1)S(1)} collective-permute-done((bf16[256,1024]{1,0:T(8,128)(2,1)S(1)}, bf16[256,1024]{1,0:T(8,128)(2,1)S(1)}, u32[]{:S(2)}, u32[]{:S(2)}) %collective-permute-start.15) | collective-permute-done | bytes 524320 | tf_op jit(solution)/shard_map/ppermute | solution.py:33
  52.6 1.3 collective-permute-start.1
  54.5 7.3 %collective-permute-done.22.refs_1_ = bf16[1024,256]{1,0:T(8,128)(2,1)S(1)} collective-permute-done((bf16[1024,256]{1,0:T(8,128)(2,1)}, bf16[1024,256]{1,0:T(8,128)(2,1)S(1)}, u32[]{:S(2)}, u32[]{:S(2)}) %collective-permute-start.22) | collective-permute-done | bytes 524320 | tf_op jit(solution)/shard_map/ppermute | solution.py:38
  61.9 1.3 collective-permute-start.2
  63.2 6.3 %collective-permute-start.14 = (bf16[256,1024]{1,0:T(8,128)(2,1)S(1)}, bf16[256,1024]{1,0:T(8,128)(2,1)S(1)}, u32[]{:S(2)}, u32[]{:S(2)}) collective-permute-start(bf16[256,1024]{1,0:T(8,128)(2,1)S(1)} %collective-permute-done.12.refs_1_), channel_id=1, source_target_pairs={{0,4},{4,0},{8,12},{12,8},{16,20},{20,16},{24,28},{28,24},{1,5},{5... | collective-permute-start | bytes 1572872 | tf_op jit(solution)/shard_map/ppermute | solution.py:25
  69.6 13.2 %collective-permute-done.2.refs_1_.rest_2_ = bf16[256,640]{1,0:T(8,128)(2,1)S(1)} collective-permute-done((bf16[256,640]{1,0:T(8,128)(2,1)S(1)}, bf16[256,640]{1,0:T(8,128)(2,1)S(1)}, u32[]{:S(2)}, u32[]{:S(2)}) %collective-permute-start.2) | collective-permute-done | bytes 327712 | tf_op jit(solution)/shard_map/ppermute | solution.py:51
  82.7 1.2 lead.1
  83.9 9.6 %collective-permute-done.17.refs_2_ = bf16[256,1024]{1,0:T(8,128)(2,1)S(1)} collective-permute-done((bf16[256,1024]{1,0:T(8,128)(2,1)S(1)}, bf16[256,1024]{1,0:T(8,128)(2,1)S(1)}, u32[]{:S(2)}, u32[]{:S(2)}) %collective-permute-start.17) | collective-permute-done | bytes 524320 | tf_op jit(solution)/shard_map/ppermute | solution.py:25
  93.5 2.0 collective-permute-start.3
  95.7 9.0 %collective-permute-done.18.refs_3_ = bf16[256,1024]{1,0:T(8,128)(2,1)S(1)} collective-permute-done((bf16[256,1024]{1,0:T(8,128)(2,1)S(1)}, bf16[256,1024]{1,0:T(8,128)(2,1)S(1)}, u32[]{:S(2)}, u32[]{:S(2)}) %collective-permute-start.18) | collective-permute-done | bytes 524320 | tf_op jit(solution)/shard_map/ppermute | solution.py:25
  104.7 1.5 shard_map.128.refs_4_.refs_2_
  106.2 4.6 %collective-permute-done.3.rest_3_ = bf16[256,640]{1,0:T(8,128)(2,1)S(1)} collective-permute-done((bf16[256,640]{1,0:T(8,128)(2,1)S(1)}, bf16[256,640]{1,0:T(8,128)(2,1)S(1)}, u32[]{:S(2)}, u32[]{:S(2)}) %collective-permute-start.3) | collective-permute-done | bytes 327712 | tf_op jit(solution)/shard_map/ppermute | solution.py:25
  110.9 5.4 %intra.1 = (f32[768,512]{1,0:T(8,128)S(1)}, f32[768,512]{1,0:T(8,128)S(1)}, f32[768,128]{1,0:T(8,128)S(1)}) custom-call(bf16[768,256]{1,0:T(8,128)(2,1)S(1)} %copy-done.8, bf16[768,256]{1,0:T(8,128)(2,1)S(1)} %copy-done.10, bf16[768,512]{1,0:T(8,128)(2,1)S(1)} %copy-done.1, f32[8,768]{1,0:T(8,128)S(1)} %maximum_maximum_fusion.gates), custom_call_target="tpu_custom_call" | custom-call | tf_op jit(solution)/shard_map/intra/pallas_call | solution.py:246
  116.3 6.1 %emit.1 = (bf16[192,512]{1,0:T(8,128)(2,1)S(1)}, bf16[192,512]{1,0:T(8,128)(2,1)S(1)}, bf16[192,512]{1,0:T(8,128)(2,1)S(1)}, bf16[192,512]{1,0:T(8,128)(2,1)S(1)}) custom-call(s32[6]{0:T(128)S(1)} %stack.72.info, bf16[768,256]{1,0:T(8,128)(2,1)S(1)} %copy-done.8, f32[768,512]{1,0:T(8,128)S(1)} %get-tuple-element.33.num_f, ...), custom_call_target="tpu_custom_call" | custom-call | tf_op jit(solution)/shard_map/emit/pallas_call | solution.py:307
  123.5 1.1 collective-permute-done.4.refs_1_
  125.1 6.7 %collective-permute-done.5.refs_2_ = bf16[192,512]{1,0:T(8,128)(2,1)S(1)} collective-permute-done((bf16[192,512]{1,0:T(8,128)(2,1)S(1)}, bf16[192,512]{1,0:T(8,128)(2,1)S(1)}, u32[]{:S(2)}, u32[]{:S(2)}) %collective-permute-start.5) | collective-permute-done | bytes 196640 | tf_op jit(solution)/shard_map/ppermute | solution.py:33
  132.5 6.9 %collective-permute-done.6.refs_3_ = bf16[192,512]{1,0:T(8,128)(2,1)S(1)} collective-permute-done((bf16[192,512]{1,0:T(8,128)(2,1)S(1)}, bf16[192,512]{1,0:T(8,128)(2,1)S(1)}, u32[]{:S(2)}, u32[]{:S(2)}) %collective-permute-start.6) | collective-permute-done | bytes 196640 | tf_op jit(solution)/shard_map/ppermute | solution.py:33
  140.0 1.6 collective-permute-start.30
  141.6 1.3 copy-done.4
  143.2 1.5 copy-done.6
  144.7 1.8 collective-permute-start.33
  146.5 1.6 copy-done.3
  148.1 1.6 copy-done.5
  149.7 1.6 copy-done.7
  151.3 1.1 copy-done.11
  152.4 0.9 copy-done.16
  153.4 0.9 copy-done.18
  154.3 0.9 copy-done.20
  155.2 3.8 %project.1 = (f32[192,2048]{1,0:T(8,128)S(1)}, bf16[192,2048]{1,0:T(8,128)(2,1)S(1)}, bf16[192,2048]{1,0:T(8,128)(2,1)S(1)}) custom-call(s32[8]{0:T(128)S(1)} %stack.65.info, bf16[192,512]{1,0:T(8,128)(2,1)S(1)} %copy-done.16, bf16[192,512]{1,0:T(8,128)(2,1)S(1)} %collective-permute-done.4.refs_1_, bf16[192,512]{1,0:T(8,128)(2,1)S(1)} %copy-done.18, ...), custom_call_target="tpu_custom_call" | custom-call | tf_op jit(solution)/shard_map/project/pallas_call | solution.py:349
  159.0 5.0 %collective-permute-start.10 = (bf16[192,2048]{1,0:T(8,128)(2,1)S(1)}, bf16[192,2048]{1,0:T(8,128)(2,1)S(1)}, u32[]{:S(2)}, u32[]{:S(2)}) collective-permute-start(bf16[192,2048]{1,0:T(8,128)(2,1)S(1)} %get-tuple-element.44), channel_id=1, source_target_pairs={{0,8},{4,12},{8,0},{12,4},{16,24},{20,28},{24,16},{28,20},{1,9},{5... | collective-permute-start | bytes 2359304 | tf_op jit(solution)/shard_map/ppermute | solution.py:38
  164.1 1.1 collective-permute-start.11
  165.2 2.4 %collective-permute-done.33.refs_0_ = bf16[1024,256]{1,0:T(8,128)(2,1)} collective-permute-done((bf16[1024,256]{1,0:T(8,128)(2,1)}, bf16[1024,256]{1,0:T(8,128)(2,1)}, u32[]{:S(2)}, u32[]{:S(2)}) %collective-permute-start.33) | collective-permute-done | bytes 524320 | tf_op jit(solution)/shard_map/ppermute | solution.py:25
  168.1 1.1 shard_map.132.refs_2_
  169.3 11.1 %collective-permute-done.34.refs_1_ = bf16[1024,256]{1,0:T(8,128)(2,1)S(1)} collective-permute-done((bf16[1024,256]{1,0:T(8,128)(2,1)}, bf16[1024,256]{1,0:T(8,128)(2,1)S(1)}, u32[]{:S(2)}, u32[]{:S(2)}) %collective-permute-start.34) | collective-permute-done | bytes 524320 | tf_op jit(solution)/shard_map/ppermute | solution.py:25
  180.9 1.3 shard_map.136.refs_0_
  182.2 1.1 shard_map.139.refs_0_
  183.9 1.4 collective-permute-start.21
  185.3 7.9 %shard_map.129.early = bf16[576,2048]{1,0:T(8,128)(2,1)S(1)} custom-call(bf16[192,2048]{1,0:T(8,128)(2,1)S(1)} %get-tuple-element.43.refs_0_, bf16[192,2048]{1,0:T(8,128)(2,1)S(1)} %collective-permute-done.10.refs_1_, bf16[192,2048]{1,0:T(8,128)(2,1)S(1)} %collective-permute-done.11.refs_2_, bf16[4,256,1024]{2,1,0:T(8,128)(2,1)S(1)} %shard_map.127.refs_3_.refs_1_, ...), custom_call_target="tpu_custom_call" | custom-call | tf_op jit(solution)/shard_map/pallas_call | solution.py:409
  193.2 10.2 %collective-permute-done.21.refs_0_ = bf16[192,2048]{1,0:T(8,128)(2,1)S(1)} collective-permute-done((bf16[192,2048]{1,0:T(8,128)(2,1)S(1)}, bf16[192,2048]{1,0:T(8,128)(2,1)S(1)}, u32[]{:S(2)}, u32[]{:S(2)}) %collective-permute-start.21) | collective-permute-done | bytes 786464 | tf_op jit(solution)/shard_map/ppermute | solution.py:33
  203.4 4.7 %shard_map.130.late = bf16[192,2048]{1,0:T(8,128)(2,1)S(1)} custom-call(bf16[192,2048]{1,0:T(8,128)(2,1)S(1)} %collective-permute-done.21.refs_0_, bf16[4,256,1024]{2,1,0:T(8,128)(2,1)S(1)} %shard_map.127.refs_3_.refs_1_, bf16[4,256,1024]{2,1,0:T(8,128)(2,1)} %shard_map.128.refs_4_.refs_2_, bf16[4,256,1024]{2,1,0:T(8,128)(2,1)} %collective-permute-done.19.refs_5_.refs_3_, ...), custom_call_target="tpu_custom_call" | custom-call | tf_op jit(solution)/shard_map/pallas_call | solution.py:409
  208.1 3.4 %shard_map.133 = (f32[384,512]{1,0:T(8,128)S(1)}, bf16[384,512]{1,0:T(8,128)(2,1)S(1)}, f32[384,512]{1,0:T(8,128)S(1)}, bf16[384,512]{1,0:T(8,128)(2,1)S(1)}) custom-call(bf16[576,2048]{1,0:T(8,128)(2,1)S(1)} %shard_map.129.early, bf16[192,2048]{1,0:T(8,128)(2,1)S(1)} %shard_map.130.late, bf16[2,1024,256]{2,1,0:T(8,128)(2,1)S(1)} %shard_map.131.refs_0_, ...), custom_call_target="tpu_custom_call" | custom-call | tf_op jit(solution)/shard_map/pallas_call | solution.py:466
  211.6 1.5 collective-permute-start.27
  213.0 1.8 shard_map.137
  215.5 1.8 shard_map.140
  217.3 2.1 collective-permute-start.36
  219.4 4.2 %collective-permute-done.27.theirs = bf16[384,512]{1,0:T(8,128)(2,1)S(1)} collective-permute-done((bf16[384,512]{1,0:T(8,128)(2,1)S(1)}, bf16[384,512]{1,0:T(8,128)(2,1)S(1)}, u32[]{:S(2)}, u32[]{:S(2)}) %collective-permute-start.27) | collective-permute-done | bytes 393248 | tf_op jit(solution)/shard_map/ppermute | solution.py:33
  223.8 1.2 collective-permute-done.28.theirs
  225.8 6.3 %collective-permute-done.32.theirs = bf16[384,512]{1,0:T(8,128)(2,1)S(1)} collective-permute-done((bf16[384,512]{1,0:T(8,128)(2,1)S(1)}, bf16[384,512]{1,0:T(8,128)(2,1)S(1)}, u32[]{:S(2)}, u32[]{:S(2)}) %collective-permute-start.32) | collective-permute-done | bytes 393248 | tf_op jit(solution)/shard_map/ppermute | solution.py:33
  232.2 1.2 collective-permute-done.36.theirs
  234.2 3.4 %collective-permute-done.37.refs_4_ = bf16[192,512]{1,0:T(8,128)(2,1)S(1)} collective-permute-done((bf16[192,512]{1,0:T(8,128)(2,1)S(1)}, bf16[192,512]{1,0:T(8,128)(2,1)S(1)}, u32[]{:S(2)}, u32[]{:S(2)}) %collective-permute-start.37) | collective-permute-done | bytes 196640 | tf_op jit(solution)/shard_map/ppermute | solution.py:38
  237.7 2.2 collective-permute-done.39.refs_6_
  239.8 1.7 finish.1
  (98 shorter events, 11.3 us)
Async XLA Ops:
  0.0 54.0 %collective-permute-start.8 = (bf16[512,2048]{1,0:T(8,128)(2,1)}, bf16[512,2048]{1,0:T(8,128)(2,1)}, u32[]{:S(2)}, u32[]{:S(2)}) collective-permute-start(bf16[512,2048]{1,0:T(8,128)(2,1)} %refs_4_.1), channel_id=1, source_target_pairs={{0,2},{1,3},{2,0},{3,1},{4,6},{5,7},{6,4},{7,5},{8,10},{9,11},{10,... | collective-permute-start | bytes 6291464 | tf_op jit(solution)/shard_map/ppermute | solution.py:33
  4.6 1.1 copy-start
  5.8 1.0 copy-start.9
  6.7 16.8 %copy-start.23 = (bf16[2048,256]{1,0:T(8,128)(2,1)S(1)}, bf16[2048,256]{1,0:T(8,128)(2,1)}, u32[]{:S(2)}) copy-start(bf16[2048,256]{1,0:T(8,128)(2,1)} %param.25) | copy-start | bytes 3145732
  9.3 10.6 %collective-permute-start = (bf16[256,640]{1,0:T(8,128)(2,1)S(1)}, bf16[256,640]{1,0:T(8,128)(2,1)S(1)}, u32[]{:S(2)}, u32[]{:S(2)}) collective-permute-start(bf16[256,640]{1,0:T(8,128)(2,1)S(1)} %get-tuple-element.36), channel_id=1, source_target_pairs={{0,4},{4,0},{8,12},{12,8},{16,20},{20,16},{24,28},{28,24},{1,5},{5... | collective-permute-start | bytes 983048 | tf_op jit(solution)/shard_map/ppermute | solution.py:25
  10.8 43.1 %copy-start.2 = (bf16[512,2048]{1,0:T(8,128)(2,1)S(1)}, bf16[512,2048]{1,0:T(8,128)(2,1)}, u32[]{:S(2)}) copy-start(bf16[512,2048]{1,0:T(8,128)(2,1)} %refs_4_.1) | copy-start | bytes 6291460
  12.3 23.1 %collective-permute-start.12 = (bf16[256,1024]{1,0:T(8,128)(2,1)S(1)}, bf16[256,1024]{1,0:T(8,128)(2,1)S(1)}, u32[]{:S(2)}, u32[]{:S(2)}) collective-permute-start(bf16[256,1024]{1,0:T(8,128)(2,1)S(1)} %get-tuple-element.63), channel_id=1, source_target_pairs={{0,8},{4,12},{8,0},{12,4},{16,24},{20,28},{24,16},{28,20},{1,9},{5... | collective-permute-start | bytes 1572872 | tf_op jit(solution)/shard_map/ppermute | solution.py:38
  13.9 21.5 %collective-permute-start.13 = (bf16[256,1024]{1,0:T(8,128)(2,1)S(1)}, bf16[256,1024]{1,0:T(8,128)(2,1)S(1)}, u32[]{:S(2)}, u32[]{:S(2)}) collective-permute-start(bf16[256,1024]{1,0:T(8,128)(2,1)S(1)} %get-tuple-element.64.refs_0_), channel_id=1, source_target_pairs={{0,4},{4,0},{8,12},{12,8},{16,20},{20,16},{24,28},{28,24},{1,5},{5... | collective-permute-start | bytes 1572872 | tf_op jit(solution)/shard_map/ppermute | solution.py:25
  14.4 38.2 %collective-permute-start.15 = (bf16[256,1024]{1,0:T(8,128)(2,1)S(1)}, bf16[256,1024]{1,0:T(8,128)(2,1)S(1)}, u32[]{:S(2)}, u32[]{:S(2)}) collective-permute-start(bf16[256,1024]{1,0:T(8,128)(2,1)S(1)} %get-tuple-element.64.refs_0_), channel_id=1, source_target_pairs={{0,16},{4,20},{8,24},{12,28},{16,0},{20,4},{24,8},{28,12},{1,17},{... | collective-permute-start | bytes 1572872 | tf_op jit(solution)/shard_map/ppermute | solution.py:33
  19.9 34.0 %collective-permute-start.16 = (bf16[256,1024]{1,0:T(8,128)(2,1)S(1)}, bf16[256,1024]{1,0:T(8,128)(2,1)S(1)}, u32[]{:S(2)}, u32[]{:S(2)}) collective-permute-start(bf16[256,1024]{1,0:T(8,128)(2,1)S(1)} %get-tuple-element.63), channel_id=1, source_target_pairs={{0,24},{4,28},{8,16},{12,20},{16,8},{20,12},{24,0},{28,4},{1,25},{... | collective-permute-start | bytes 1572872 | tf_op jit(solution)/shard_map/ppermute | solution.py:44
  35.4 26.5 %collective-permute-start.22 = (bf16[1024,256]{1,0:T(8,128)(2,1)}, bf16[1024,256]{1,0:T(8,128)(2,1)S(1)}, u32[]{:S(2)}, u32[]{:S(2)}) collective-permute-start(bf16[1024,256]{1,0:T(8,128)(2,1)} %get-tuple-element.61), channel_id=1, source_target_pairs={{0,8},{4,12},{8,0},{12,4},{16,24},{20,28},{24,16},{28,20},{1,9},{5... | collective-permute-start | bytes 1572872 | tf_op jit(solution)/shard_map/ppermute | solution.py:38
  35.4 27.8 %collective-permute-start.24 = (bf16[1024,256]{1,0:T(8,128)(2,1)S(1)}, bf16[1024,256]{1,0:T(8,128)(2,1)S(1)}, u32[]{:S(2)}, u32[]{:S(2)}) collective-permute-start(bf16[1024,256]{1,0:T(8,128)(2,1)S(1)} %get-tuple-element.62.refs_0_), channel_id=1, source_target_pairs={{0,4},{4,0},{8,12},{12,8},{16,20},{20,16},{24,28},{28,24},{1,5},{5... | collective-permute-start | bytes 1572872 | tf_op jit(solution)/shard_map/ppermute | solution.py:25
  52.6 16.8 %collective-permute-start.1 = (bf16[256,640]{1,0:T(8,128)(2,1)S(1)}, bf16[256,640]{1,0:T(8,128)(2,1)S(1)}, u32[]{:S(2)}, u32[]{:S(2)}) collective-permute-start(bf16[256,640]{1,0:T(8,128)(2,1)S(1)} %pair.1), channel_id=1, source_target_pairs={{8,0},{16,8},{24,16},{4,12},{12,20},{20,28},{9,1},{17,9},{25,17},{... | collective-permute-start | bytes 983048 | tf_op jit(solution)/shard_map/ppermute | solution.py:51
  53.9 87.7 %collective-permute-start.7 = (bf16[512,2048]{1,0:T(8,128)(2,1)S(1)}, bf16[512,2048]{1,0:T(8,128)(2,1)S(1)}, u32[]{:S(2)}, u32[]{:S(2)}) collective-permute-start(bf16[512,2048]{1,0:T(8,128)(2,1)S(1)} %copy-done.2), channel_id=1, source_target_pairs={{0,1},{1,0},{2,3},{3,2},{4,5},{5,4},{6,7},{7,6},{8,9},{9,8},{10,11... | collective-permute-start | bytes 6291464 | tf_op jit(solution)/shard_map/ppermute | solution.py:25
  54.0 89.2 %collective-permute-start.9 = (bf16[512,2048]{1,0:T(8,128)(2,1)}, bf16[512,2048]{1,0:T(8,128)(2,1)S(1)}, u32[]{:S(2)}, u32[]{:S(2)}) collective-permute-start(bf16[512,2048]{1,0:T(8,128)(2,1)} %collective-permute-done.8.refs_6_), channel_id=1, source_target_pairs={{0,1},{1,0},{2,3},{3,2},{4,5},{5,4},{6,7},{7,6},{8,9},{9,8},{10,11... | collective-permute-start | bytes 6291464 | tf_op jit(solution)/shard_map/ppermute | solution.py:25
  61.9 20.9 %collective-permute-start.2 = (bf16[256,640]{1,0:T(8,128)(2,1)S(1)}, bf16[256,640]{1,0:T(8,128)(2,1)S(1)}, u32[]{:S(2)}, u32[]{:S(2)}) collective-permute-start(bf16[256,640]{1,0:T(8,128)(2,1)S(1)} %pair.1), channel_id=1, source_target_pairs={{16,0},{24,8},{4,20},{12,28},{17,1},{25,9},{5,21},{13,29},{18,2},{... | collective-permute-start | bytes 983048 | tf_op jit(solution)/shard_map/ppermute | solution.py:51
  63.2 32.3 %copy-start.13 = (bf16[1024,256]{1,0:T(8,128)(2,1)}, bf16[1024,256]{1,0:T(8,128)(2,1)S(1)}, u32[]{:S(2)}) copy-start(bf16[1024,256]{1,0:T(8,128)(2,1)S(1)} %collective-permute-done.24.refs_0_) | copy-start | bytes 1572868
  63.2 19.5 %collective-permute-start.14 = (bf16[256,1024]{1,0:T(8,128)(2,1)S(1)}, bf16[256,1024]{1,0:T(8,128)(2,1)S(1)}, u32[]{:S(2)}, u32[]{:S(2)}) collective-permute-start(bf16[256,1024]{1,0:T(8,128)(2,1)S(1)} %collective-permute-done.12.refs_1_), channel_id=1, source_target_pairs={{0,4},{4,0},{8,12},{12,8},{16,20},{20,16},{24,28},{28,24},{1,5},{5... | collective-permute-start | bytes 1572872 | tf_op jit(solution)/shard_map/ppermute | solution.py:25
  69.5 24.0 %collective-permute-start.17 = (bf16[256,1024]{1,0:T(8,128)(2,1)S(1)}, bf16[256,1024]{1,0:T(8,128)(2,1)S(1)}, u32[]{:S(2)}, u32[]{:S(2)}) collective-permute-start(bf16[256,1024]{1,0:T(8,128)(2,1)S(1)} %collective-permute-done.15.refs_0_), channel_id=1, source_target_pairs={{0,4},{4,0},{8,12},{12,8},{16,20},{20,16},{24,28},{28,24},{1,5},{5... | collective-permute-start | bytes 1572872 | tf_op jit(solution)/shard_map/ppermute | solution.py:25
  82.7 22.0 %collective-permute-start.18 = (bf16[256,1024]{1,0:T(8,128)(2,1)S(1)}, bf16[256,1024]{1,0:T(8,128)(2,1)S(1)}, u32[]{:S(2)}, u32[]{:S(2)}) collective-permute-start(bf16[256,1024]{1,0:T(8,128)(2,1)S(1)} %collective-permute-done.16.refs_1_), channel_id=1, source_target_pairs={{0,4},{4,0},{8,12},{12,8},{16,20},{20,16},{24,28},{28,24},{1,5},{5... | collective-permute-start | bytes 1572872 | tf_op jit(solution)/shard_map/ppermute | solution.py:25
  82.7 40.3 %collective-permute-start.29 = (bf16[1024,256]{1,0:T(8,128)(2,1)S(1)}, bf16[1024,256]{1,0:T(8,128)(2,1)}, u32[]{:S(2)}, u32[]{:S(2)}) collective-permute-start(bf16[1024,256]{1,0:T(8,128)(2,1)S(1)} %get-tuple-element.62.refs_0_), channel_id=1, source_target_pairs={{0,16},{4,20},{8,24},{12,28},{16,0},{20,4},{24,8},{28,12},{1,17},{... | collective-permute-start | bytes 1572872 | tf_op jit(solution)/shard_map/ppermute | solution.py:33
  93.5 17.4 %collective-permute-start.3 = (bf16[256,640]{1,0:T(8,128)(2,1)S(1)}, bf16[256,640]{1,0:T(8,128)(2,1)S(1)}, u32[]{:S(2)}, u32[]{:S(2)}) collective-permute-start(bf16[256,640]{1,0:T(8,128)(2,1)S(1)} %lead.1), channel_id=1, source_target_pairs={{0,4},{4,0},{8,12},{12,8},{16,20},{20,16},{24,28},{28,24},{1,5},{5... | collective-permute-start | bytes 983048 | tf_op jit(solution)/shard_map/ppermute | solution.py:25
  95.7 15.2 %copy-start.1 = (bf16[768,512]{1,0:T(8,128)(2,1)S(1)}, bf16[768,512]{1,0:T(8,128)(2,1)}, u32[]{:S(2)}) copy-start(bf16[768,512]{1,0:T(8,128)(2,1)} %values.3) | copy-start | bytes 2359300
  95.7 15.2 %copy-start.8 = (bf16[768,256]{1,0:T(8,128)(2,1)S(1)}, bf16[768,256]{1,0:T(8,128)(2,1)}, u32[]{:S(2)}) copy-start(bf16[768,256]{1,0:T(8,128)(2,1)} %queries.3) | copy-start | bytes 1179652
  95.7 15.2 %copy-start.10 = (bf16[768,256]{1,0:T(8,128)(2,1)S(1)}, bf16[768,256]{1,0:T(8,128)(2,1)}, u32[]{:S(2)}) copy-start(bf16[768,256]{1,0:T(8,128)(2,1)} %keys.3) | copy-start | bytes 1179652
  95.7 20.6 %copy-start.12 = (bf16[768,512]{1,0:T(8,128)(2,1)S(1)}, bf16[768,512]{1,0:T(8,128)(2,1)}, u32[]{:S(2)}) copy-start(bf16[768,512]{1,0:T(8,128)(2,1)} %out_gate.1) | copy-start | bytes 2359300
  95.7 20.5 %copy-start.22 = (f32[512]{0:T(512)S(1)}, f32[512]{0:T(512)}, u32[]{:S(2)}) copy-start(f32[512]{0:T(512)} %param.20) | copy-start | bytes 6148
  104.7 75.6 %collective-permute-start.19 = (bf16[4,256,1024]{2,1,0:T(8,128)(2,1)S(1)}, bf16[4,256,1024]{2,1,0:T(8,128)(2,1)}, u32[]{:S(2)}, u32[]{:S(2)}) collective-permute-start(bf16[4,256,1024]{2,1,0:T(8,128)(2,1)S(1)} %shard_map.127.refs_3_.refs_1_), channel_id=1, source_target_pairs={{0,1},{1,0},{2,3},{3,2},{4,5},{5,4},{6,7},{7,6},{8,9},{9,8},{10,11... | collective-permute-start | bytes 6291464 | tf_op jit(solution)/shard_map/ppermute | solution.py:25
  110.9 71.3 %collective-permute-start.20 = (bf16[4,256,1024]{2,1,0:T(8,128)(2,1)}, bf16[4,256,1024]{2,1,0:T(8,128)(2,1)}, u32[]{:S(2)}, u32[]{:S(2)}) collective-permute-start(bf16[4,256,1024]{2,1,0:T(8,128)(2,1)} %shard_map.128.refs_4_.refs_2_), channel_id=1, source_target_pairs={{0,1},{1,0},{2,3},{3,2},{4,5},{5,4},{6,7},{7,6},{8,9},{9,8},{10,11... | collective-permute-start | bytes 6291464 | tf_op jit(solution)/shard_map/ppermute | solution.py:25
  116.3 30.3 %copy-start.21 = (f32[2048]{0:T(1024)S(1)}, f32[2048]{0:T(1024)}, u32[]{:S(2)}) copy-start(f32[2048]{0:T(1024)} %param.23) | copy-start | bytes 24580
  123.0 1.6 collective-permute-start.4
  124.6 7.2 %collective-permute-start.5 = (bf16[192,512]{1,0:T(8,128)(2,1)S(1)}, bf16[192,512]{1,0:T(8,128)(2,1)S(1)}, u32[]{:S(2)}, u32[]{:S(2)}) collective-permute-start(bf16[192,512]{1,0:T(8,128)(2,1)S(1)} %get-tuple-element.40), channel_id=1, source_target_pairs={{0,2},{1,3},{2,0},{3,1},{4,6},{5,7},{6,4},{7,5},{8,10},{9,11},{10,... | collective-permute-start | bytes 589832 | tf_op jit(solution)/shard_map/ppermute | solution.py:33
  131.8 0.7 copy-start.17
  132.5 6.9 %collective-permute-start.6 = (bf16[192,512]{1,0:T(8,128)(2,1)S(1)}, bf16[192,512]{1,0:T(8,128)(2,1)S(1)}, u32[]{:S(2)}, u32[]{:S(2)}) collective-permute-start(bf16[192,512]{1,0:T(8,128)(2,1)S(1)} %get-tuple-element.41), channel_id=1, source_target_pairs={{0,3},{1,2},{2,1},{3,0},{4,7},{5,6},{6,5},{7,4},{8,11},{9,10},{10,... | collective-permute-start | bytes 589832 | tf_op jit(solution)/shard_map/ppermute | solution.py:33
  139.4 0.7 copy-start.19
  140.0 19.0 %collective-permute-start.30 = (bf16[1024,256]{1,0:T(8,128)(2,1)}, bf16[1024,256]{1,0:T(8,128)(2,1)}, u32[]{:S(2)}, u32[]{:S(2)}) collective-permute-start(bf16[1024,256]{1,0:T(8,128)(2,1)} %get-tuple-element.61), channel_id=1, source_target_pairs={{0,24},{4,28},{8,16},{12,20},{16,8},{20,12},{24,0},{28,4},{1,25},{... | collective-permute-start | bytes 1572872 | tf_op jit(solution)/shard_map/ppermute | solution.py:44
  141.6 1.3 copy-start.4
  142.9 21.1 %collective-permute-start.25 = (bf16[1024,256]{1,0:T(8,128)(2,1)S(1)}, bf16[1024,256]{1,0:T(8,128)(2,1)}, u32[]{:S(2)}, u32[]{:S(2)}) collective-permute-start(bf16[1024,256]{1,0:T(8,128)(2,1)S(1)} %collective-permute-done.22.refs_1_), channel_id=1, source_target_pairs={{0,4},{4,0},{8,12},{12,8},{16,20},{20,16},{24,28},{28,24},{1,5},{5... | collective-permute-start | bytes 1572872 | tf_op jit(solution)/shard_map/ppermute | solution.py:25
  143.2 1.5 copy-start.6
  144.7 23.0 %collective-permute-start.33 = (bf16[1024,256]{1,0:T(8,128)(2,1)}, bf16[1024,256]{1,0:T(8,128)(2,1)}, u32[]{:S(2)}, u32[]{:S(2)}) collective-permute-start(bf16[1024,256]{1,0:T(8,128)(2,1)} %collective-permute-done.29.refs_0_), channel_id=1, source_target_pairs={{0,4},{4,0},{8,12},{12,8},{16,20},{20,16},{24,28},{28,24},{1,5},{5... | collective-permute-start | bytes 1572872 | tf_op jit(solution)/shard_map/ppermute | solution.py:25
  146.5 1.6 copy-start.3
  148.1 1.6 copy-start.5
  149.7 1.6 copy-start.7
  151.3 1.1 copy-start.11
  152.4 0.9 copy-start.16
  153.4 0.9 copy-start.18
  154.3 0.9 copy-start.20
  159.0 9.1 %copy-start.14 = (bf16[1024,256]{1,0:T(8,128)(2,1)S(1)}, bf16[1024,256]{1,0:T(8,128)(2,1)}, u32[]{:S(2)}) copy-start(bf16[1024,256]{1,0:T(8,128)(2,1)} %copy-done.13) | copy-start | bytes 1572868
  159.0 24.3 %collective-permute-start.10 = (bf16[192,2048]{1,0:T(8,128)(2,1)S(1)}, bf16[192,2048]{1,0:T(8,128)(2,1)S(1)}, u32[]{:S(2)}, u32[]{:S(2)}) collective-permute-start(bf16[192,2048]{1,0:T(8,128)(2,1)S(1)} %get-tuple-element.44), channel_id=1, source_target_pairs={{0,8},{4,12},{8,0},{12,4},{16,24},{20,28},{24,16},{28,20},{1,9},{5... | collective-permute-start | bytes 2359304 | tf_op jit(solution)/shard_map/ppermute | solution.py:38
  164.1 19.8 %collective-permute-start.11 = (bf16[192,2048]{1,0:T(8,128)(2,1)S(1)}, bf16[192,2048]{1,0:T(8,128)(2,1)S(1)}, u32[]{:S(2)}, u32[]{:S(2)}) collective-permute-start(bf16[192,2048]{1,0:T(8,128)(2,1)S(1)} %get-tuple-element.43.refs_0_), channel_id=1, source_target_pairs={{0,2},{1,3},{2,0},{3,1},{4,6},{5,7},{6,4},{7,5},{8,10},{9,11},{10,... | collective-permute-start | bytes 2359304 | tf_op jit(solution)/shard_map/ppermute | solution.py:33
  167.6 12.7 %collective-permute-start.34 = (bf16[1024,256]{1,0:T(8,128)(2,1)}, bf16[1024,256]{1,0:T(8,128)(2,1)S(1)}, u32[]{:S(2)}, u32[]{:S(2)}) collective-permute-start(bf16[1024,256]{1,0:T(8,128)(2,1)} %collective-permute-done.30.refs_1_), channel_id=1, source_target_pairs={{0,4},{4,0},{8,12},{12,8},{16,20},{20,16},{24,28},{28,24},{1,5},{5... | collective-permute-start | bytes 1572872 | tf_op jit(solution)/shard_map/ppermute | solution.py:25
  180.3 27.8 %collective-permute-start.23 = (bf16[2,1024,256]{2,1,0:T(8,128)(2,1)S(1)}, bf16[2,1024,256]{2,1,0:T(8,128)(2,1)S(1)}, u32[]{:S(2)}, u32[]{:S(2)}) collective-permute-start(bf16[2,1024,256]{2,1,0:T(8,128)(2,1)S(1)} %shard_map.131.refs_0_), channel_id=1, source_target_pairs={{0,1},{1,0},{2,3},{3,2},{4,5},{5,4},{6,7},{7,6},{8,9},{9,8},{10,11... | collective-permute-start | bytes 3145736 | tf_op jit(solution)/shard_map/ppermute | solution.py:25
  180.4 27.8 %collective-permute-start.26 = (bf16[2,1024,256]{2,1,0:T(8,128)(2,1)S(1)}, bf16[2,1024,256]{2,1,0:T(8,128)(2,1)S(1)}, u32[]{:S(2)}, u32[]{:S(2)}) collective-permute-start(bf16[2,1024,256]{2,1,0:T(8,128)(2,1)S(1)} %shard_map.132.refs_2_), channel_id=1, source_target_pairs={{0,1},{1,0},{2,3},{3,2},{4,5},{5,4},{6,7},{7,6},{8,9},{9,8},{10,11... | collective-permute-start | bytes 3145736 | tf_op jit(solution)/shard_map/ppermute | solution.py:25
  182.1 30.9 %collective-permute-start.31 = (bf16[2,1024,256]{2,1,0:T(8,128)(2,1)S(1)}, bf16[2,1024,256]{2,1,0:T(8,128)(2,1)S(1)}, u32[]{:S(2)}, u32[]{:S(2)}) collective-permute-start(bf16[2,1024,256]{2,1,0:T(8,128)(2,1)S(1)} %shard_map.136.refs_0_), channel_id=1, source_target_pairs={{0,1},{1,0},{2,3},{3,2},{4,5},{5,4},{6,7},{7,6},{8,9},{9,8},{10,11... | collective-permute-start | bytes 3145736 | tf_op jit(solution)/shard_map/ppermute | solution.py:25
  183.3 32.2 %collective-permute-start.35 = (bf16[2,1024,256]{2,1,0:T(8,128)(2,1)S(1)}, bf16[2,1024,256]{2,1,0:T(8,128)(2,1)S(1)}, u32[]{:S(2)}, u32[]{:S(2)}) collective-permute-start(bf16[2,1024,256]{2,1,0:T(8,128)(2,1)S(1)} %shard_map.139.refs_0_), channel_id=1, source_target_pairs={{0,1},{1,0},{2,3},{3,2},{4,5},{5,4},{6,7},{7,6},{8,9},{9,8},{10,11... | collective-permute-start | bytes 3145736 | tf_op jit(solution)/shard_map/ppermute | solution.py:25
  183.9 19.5 %collective-permute-start.21 = (bf16[192,2048]{1,0:T(8,128)(2,1)S(1)}, bf16[192,2048]{1,0:T(8,128)(2,1)S(1)}, u32[]{:S(2)}, u32[]{:S(2)}) collective-permute-start(bf16[192,2048]{1,0:T(8,128)(2,1)S(1)} %collective-permute-done.10.refs_1_), channel_id=1, source_target_pairs={{0,2},{1,3},{2,0},{3,1},{4,6},{5,7},{6,4},{7,5},{8,10},{9,11},{10,... | collective-permute-start | bytes 2359304 | tf_op jit(solution)/shard_map/ppermute | solution.py:33
  211.6 12.1 %collective-permute-start.27 = (bf16[384,512]{1,0:T(8,128)(2,1)S(1)}, bf16[384,512]{1,0:T(8,128)(2,1)S(1)}, u32[]{:S(2)}, u32[]{:S(2)}) collective-permute-start(bf16[384,512]{1,0:T(8,128)(2,1)S(1)} %get-tuple-element.46), channel_id=1, source_target_pairs={{0,2},{1,3},{2,0},{3,1},{4,6},{5,7},{6,4},{7,5},{8,10},{9,11},{10,... | collective-permute-start | bytes 1179656 | tf_op jit(solution)/shard_map/ppermute | solution.py:33
  213.0 12.0 %collective-permute-start.28 = (bf16[384,512]{1,0:T(8,128)(2,1)S(1)}, bf16[384,512]{1,0:T(8,128)(2,1)S(1)}, u32[]{:S(2)}, u32[]{:S(2)}) collective-permute-start(bf16[384,512]{1,0:T(8,128)(2,1)S(1)} %get-tuple-element.49), channel_id=1, source_target_pairs={{0,8},{4,12},{8,0},{12,4},{16,24},{20,28},{24,16},{28,20},{1,9},{5... | collective-permute-start | bytes 1179656 | tf_op jit(solution)/shard_map/ppermute | solution.py:38
  214.8 17.2 %collective-permute-start.32 = (bf16[384,512]{1,0:T(8,128)(2,1)S(1)}, bf16[384,512]{1,0:T(8,128)(2,1)S(1)}, u32[]{:S(2)}, u32[]{:S(2)}) collective-permute-start(bf16[384,512]{1,0:T(8,128)(2,1)S(1)} %get-tuple-element.52), channel_id=1, source_target_pairs={{0,2},{1,3},{2,0},{3,1},{4,6},{5,7},{6,4},{7,5},{8,10},{9,11},{10,... | collective-permute-start | bytes 1179656 | tf_op jit(solution)/shard_map/ppermute | solution.py:33
  217.3 16.1 %collective-permute-start.36 = (bf16[384,512]{1,0:T(8,128)(2,1)S(1)}, bf16[384,512]{1,0:T(8,128)(2,1)S(1)}, u32[]{:S(2)}, u32[]{:S(2)}) collective-permute-start(bf16[384,512]{1,0:T(8,128)(2,1)S(1)} %get-tuple-element.55), channel_id=1, source_target_pairs={{0,8},{4,12},{8,0},{12,4},{16,24},{20,28},{24,16},{28,20},{1,9},{5... | collective-permute-start | bytes 1179656 | tf_op jit(solution)/shard_map/ppermute | solution.py:38
  223.7 14.0 %collective-permute-start.37 = (bf16[192,512]{1,0:T(8,128)(2,1)S(1)}, bf16[192,512]{1,0:T(8,128)(2,1)S(1)}, u32[]{:S(2)}, u32[]{:S(2)}) collective-permute-start(bf16[192,512]{1,0:T(8,128)(2,1)S(1)} %get-tuple-element.57), channel_id=1, source_target_pairs={{0,8},{4,12},{8,0},{12,4},{16,24},{20,28},{24,16},{28,20},{1,9},{5... | collective-permute-start | bytes 589832 | tf_op jit(solution)/shard_map/ppermute | solution.py:38
  225.1 12.6 %collective-permute-start.38 = (bf16[192,512]{1,0:T(8,128)(2,1)S(1)}, bf16[192,512]{1,0:T(8,128)(2,1)S(1)}, u32[]{:S(2)}, u32[]{:S(2)}) collective-permute-start(bf16[192,512]{1,0:T(8,128)(2,1)S(1)} %get-tuple-element.58), channel_id=1, source_target_pairs={{0,2},{1,3},{2,0},{3,1},{4,6},{5,7},{6,4},{7,5},{8,10},{9,11},{10,... | collective-permute-start | bytes 589832 | tf_op jit(solution)/shard_map/ppermute | solution.py:33
  232.1 7.7 %collective-permute-start.39 = (bf16[192,512]{1,0:T(8,128)(2,1)S(1)}, bf16[192,512]{1,0:T(8,128)(2,1)S(1)}, u32[]{:S(2)}, u32[]{:S(2)}) collective-permute-start(bf16[192,512]{1,0:T(8,128)(2,1)S(1)} %get-tuple-element.59), channel_id=1, source_target_pairs={{0,8},{4,12},{8,0},{12,4},{16,24},{20,28},{24,16},{28,20},{1,9},{5... | collective-permute-start | bytes 589832 | tf_op jit(solution)/shard_map/ppermute | solution.py:38
  233.5 6.3 %collective-permute-start.40 = (bf16[192,512]{1,0:T(8,128)(2,1)S(1)}, bf16[192,512]{1,0:T(8,128)(2,1)S(1)}, u32[]{:S(2)}, u32[]{:S(2)}) collective-permute-start(bf16[192,512]{1,0:T(8,128)(2,1)S(1)} %get-tuple-element.60), channel_id=1, source_target_pairs={{0,2},{1,3},{2,0},{3,1},{4,6},{5,7},{6,4},{7,5},{8,10},{9,11},{10,... | collective-permute-start | bytes 589832 | tf_op jit(solution)/shard_map/ppermute | solution.py:33
  (1 other events, 0.7 us)

commit v3 on v2

--- a/solution.py
+++ b/solution.py
@@ -324,7 +324,8 @@
 
 def project_kernel(count, turn, info, *refs):
     pieces, weights = refs[:count], refs[count : 2 * count]
-    resid, gain, mixed_out, normed_out, beside_out, whole = refs[2 * count :]
+    resid, gain, mixed_out, normed_out, beside_top, beside_low, whole = refs[2 * count :]
+    top = beside_top.shape[0]
     mixed = resid[...].astype(jnp.float32)
     for piece, weight in zip(pieces, weights):
         mixed = mixed + jnp.dot(piece[...], weight[...], preferred_element_type=jnp.float32)
@@ -333,7 +334,8 @@
     normed = mixed * factor * gain[...]
     if not turn:
         normed_out[...] = normed.astype(jnp.bfloat16)
-        beside_out[...] = normed_out[...]
+        beside_top[...] = normed_out[:top]
+        beside_low[...] = normed_out[top:]
         return
     whole[...] = normed
     depth = mixed.shape[1] // turn
@@ -341,17 +343,20 @@
         at = pl.multiple_of(info[k] * depth, LANES)
         part = whole[:, pl.ds(at, depth)].astype(jnp.bfloat16)
         normed_out[:, k * depth : (k + 1) * depth] = part
-        beside_out[:, (k ^ 1) * depth : ((k ^ 1) + 1) * depth] = part
+        beside_top[:, (k ^ 1) * depth : ((k ^ 1) + 1) * depth] = part[:top]
+        beside_low[:, (k ^ 1) * depth : ((k ^ 1) + 1) * depth] = part[top:]
 
 
 def project(pieces, weights, resid, gain, sources, depth):
     inside = depth % LANES == 0
-    mixed, normed, beside = pl.pallas_call(
+    half = jax.ShapeDtypeStruct((resid.shape[0] // 2, resid.shape[1]), jnp.bfloat16)
+    mixed, normed, *beside = pl.pallas_call(
         functools.partial(project_kernel, len(pieces), len(sources) if inside else 0),
         out_shape=(
             jax.ShapeDtypeStruct(resid.shape, jnp.float32),
             jax.ShapeDtypeStruct(resid.shape, jnp.bfloat16),
-            jax.ShapeDtypeStruct(resid.shape, jnp.bfloat16),
+            half,
+            half,
         ),
         in_specs=[SMALL] + [LOCAL] * (2 * len(pieces) + 2),
         scratch_shapes=[pltpu.VMEM(resid.shape, jnp.float32)],
@@ -360,7 +365,8 @@
     if not inside:
         cuts = [lax.dynamic_slice_in_dim(normed, at * depth, depth, 1) for at in sources]
         normed = jnp.concatenate(cuts, axis=1)
-        beside = jnp.concatenate([cuts[k ^ 1] for k in range(len(cuts))], axis=1)
+        turned = jnp.concatenate([cuts[k ^ 1] for k in range(len(cuts))], axis=1)
+        beside = [turned[: half.shape[0]], turned[half.shape[0] :]]
     return mixed, normed, beside
 
 
@@ -558,8 +564,9 @@
     outer = places("tp")[0]
     assert outer == 2
     across = shift(value, "tp", 1)
-    beside = neighbour(given)
-    return (value, beside, across), shift(beside, "tp", 1)
+    beside = [neighbour(x) for x in given]
+    late = [shift(x, "tp", 1) for x in beside]
+    return [value, *beside, across], late
 
 
 def sum_back(keep, send, line_first):
@@ -677,7 +684,7 @@
     )
     early, late = row_blocks(normed, given)
     early = up_product(early, up_mine, up_theirs)
-    late = up_product([late], up_mine, up_theirs)
+    late = up_product(late, up_mine, up_theirs)
 
     parts = down_product(early, late, down_groups[:2], (False, True))
     for step in range(2, len(down_groups)):

time: 242 us -> 253 us (1.045)
  waiting for transfers between devices: 131 us -> 143 us
  starting transfers between devices: 44 us -> 40.4 us
    ppermute x12 -> x13, waiting for transfers between devices: 51.9 us -> 66.9 us  [shift(): return lax.ppermute(value, axis, moves)]
    ppermute x7 -> x8, waiting for transfers between devices: 26.5 us -> 17.6 us  [neighbour(): return lax.ppermute(value, 'sp', moves)]
    ppermute x2, waiting for transfers between devices: 13.2 us -> 17.1 us  [carry_shift(): return lax.ppermute(value, 'sp', moves)]
    ppermute x7 -> x8, starting transfers between devices: 8.93 us -> 5.11 us  [neighbour(): return lax.ppermute(value, 'sp', moves)]
    ppermute x12 -> x13, starting transfers between devices: 12.6 us -> 14.7 us  [shift(): return lax.ppermute(value, axis, moves)]
    unnamed x49 -> x67, local copies, waits for them, and re-layouts: 16.4 us -> 17.1 us
  transfers between devices with their start and end apart: 41 -> 43, of which waited for: 20 -> 21; matrix products, arithmetic and copies ran while one was open for 2% -> 1% of each run, Pallas kernels for 18% -> 18%
where the time goes in v3:
time: 253 us; the launch traced here: 252 us
  waiting for transfers between devices  143 us (57%)
  Pallas kernels  47.3 us (19%)
  starting transfers between devices  40.4 us (16%)
  local copies, waits for them, and re-layouts  20.7 us (8%)
    ppermute x13, waiting for transfers between devices, shift(): return lax.ppermute(value, axis, moves)  66.9 us
    ppermute x18, waiting for transfers between devices, flip(): lax.ppermute(value, axis, [(i, i ^ 1) for i in range(lax.axis_size(axis))])  41.8 us
    ppermute x8, waiting for transfers between devices, neighbour(): return lax.ppermute(value, 'sp', moves)  17.6 us
    unnamed x67, local copies, waits for them, and re-layouts  17.1 us
    ppermute x2, waiting for transfers between devices, carry_shift(): return lax.ppermute(value, 'sp', moves)  17.1 us
    ppermute x13, starting transfers between devices, shift(): return lax.ppermute(value, axis, moves)  14.7 us
    ppermute x18, starting transfers between devices, flip(): lax.ppermute(value, axis, [(i, i ^ 1) for i in range(lax.axis_size(axis))])  13.6 us
    pallas_call x2, Pallas kernels, up_product(): pl.pallas_call(functools.partial(up_kernel, len(rows), steps), out_shape=...  12.6 us
  transfers between devices with their start and end apart: 43, of which 21 were waited for; matrix products, arithmetic and copies ran while one was open for 1% of the time, Pallas kernels for 18%

profile of v3, /device:TPU:0, one launch (start us, length us, event | category | flops | bytes accessed | tf_op | source)
XLA Modules:
  0.0 252.4 jit_solution(15565869230822999977)
XLA Ops:
  0.0 3.0 %collective-permute-start.8 = (bf16[512,2048]{1,0:T(8,128)(2,1)}, bf16[512,2048]{1,0:T(8,128)(2,1)}, u32[]{:S(2)}, u32[]{:S(2)}) collective-permute-start(bf16[512,2048]{1,0:T(8,128)(2,1)} %refs_4_.1), channel_id=1, source_target_pairs={{0,2},{1,3},{2,0},{3,1},{4,6},{5,7},{6,4},{7,5},{8,10},{9,11},{10,... | collective-permute-start | bytes 6291464 | tf_op jit(solution)/shard_map/ppermute | solution.py:33
  3.1 2.1 constant_dynamic-slice_fusion.2
  5.1 1.6 collective-permute-start.13
  6.7 1.5 collective-permute-start.14
  8.5 2.5 summary.1
  11.6 2.6 %collective-permute-start.16 = (bf16[256,1024]{1,0:T(8,128)(2,1)S(1)}, bf16[256,1024]{1,0:T(8,128)(2,1)S(1)}, u32[]{:S(2)}, u32[]{:S(2)}) collective-permute-start(bf16[256,1024]{1,0:T(8,128)(2,1)S(1)} %get-tuple-element.66.refs_0_), channel_id=1, source_target_pairs={{0,16},{4,20},{8,24},{12,28},{16,0},{20,4},{24,8},{28,12},{1,17},{... | collective-permute-start | bytes 1572872 | tf_op jit(solution)/shard_map/ppermute | solution.py:33
  14.2 12.6 %collective-permute-done.got.rest_0_ = bf16[256,640]{1,0:T(8,128)(2,1)S(1)} collective-permute-done((bf16[256,640]{1,0:T(8,128)(2,1)S(1)}, bf16[256,640]{1,0:T(8,128)(2,1)S(1)}, u32[]{:S(2)}, u32[]{:S(2)}) %collective-permute-start) | collective-permute-done | bytes 327712 | tf_op jit(solution)/shard_map/ppermute | solution.py:25
  26.8 2.5 collective-permute-start.17
  29.3 1.3 constant_dynamic-slice_fusion
  31.3 1.5 collective-permute-start.26
  33.5 16.3 %collective-permute-done.16.refs_0_ = bf16[256,1024]{1,0:T(8,128)(2,1)S(1)} collective-permute-done((bf16[256,1024]{1,0:T(8,128)(2,1)S(1)}, bf16[256,1024]{1,0:T(8,128)(2,1)S(1)}, u32[]{:S(2)}, u32[]{:S(2)}) %collective-permute-start.16) | collective-permute-done | bytes 524320 | tf_op jit(solution)/shard_map/ppermute | solution.py:33
  49.8 1.3 collective-permute-start.1
  51.1 1.9 collective-permute-start.15
  53.0 6.0 %collective-permute-done.24.refs_1_ = bf16[1024,256]{1,0:T(8,128)(2,1)} collective-permute-done((bf16[1024,256]{1,0:T(8,128)(2,1)S(1)}, bf16[1024,256]{1,0:T(8,128)(2,1)}, u32[]{:S(2)}, u32[]{:S(2)}) %collective-permute-start.24) | collective-permute-done | bytes 524320 | tf_op jit(solution)/shard_map/ppermute | solution.py:38
  59.0 1.3 collective-permute-start.2
  60.9 3.9 %collective-permute-done.1.refs_0_.rest_1_ = bf16[256,640]{1,0:T(8,128)(2,1)S(1)} collective-permute-done((bf16[256,640]{1,0:T(8,128)(2,1)S(1)}, bf16[256,640]{1,0:T(8,128)(2,1)S(1)}, u32[]{:S(2)}, u32[]{:S(2)}) %collective-permute-start.1) | collective-permute-done | bytes 327712 | tf_op jit(solution)/shard_map/ppermute | solution.py:51
  64.8 1.9 collective-permute-start.18
  66.7 13.2 %collective-permute-done.2.refs_1_.rest_2_ = bf16[256,640]{1,0:T(8,128)(2,1)S(1)} collective-permute-done((bf16[256,640]{1,0:T(8,128)(2,1)S(1)}, bf16[256,640]{1,0:T(8,128)(2,1)S(1)}, u32[]{:S(2)}, u32[]{:S(2)}) %collective-permute-start.2) | collective-permute-done | bytes 327712 | tf_op jit(solution)/shard_map/ppermute | solution.py:51
  79.9 1.2 lead.1
  81.1 2.1 collective-permute-start.3
  83.2 11.5 %collective-permute-done.19.refs_3_ = bf16[256,1024]{1,0:T(8,128)(2,1)S(1)} collective-permute-done((bf16[256,1024]{1,0:T(8,128)(2,1)S(1)}, bf16[256,1024]{1,0:T(8,128)(2,1)S(1)}, u32[]{:S(2)}, u32[]{:S(2)}) %collective-permute-start.19) | collective-permute-done | bytes 524320 | tf_op jit(solution)/shard_map/ppermute | solution.py:25
  94.7 2.0 collective-permute-start.32
  97.8 1.0 copy-done.17
  98.9 1.0 copy-done.19
  100.1 1.5 shard_map.128.refs_5_.refs_3_
  101.6 14.7 %collective-permute-done.31.refs_0_ = bf16[1024,256]{1,0:T(8,128)(2,1)} collective-permute-done((bf16[1024,256]{1,0:T(8,128)(2,1)S(1)}, bf16[1024,256]{1,0:T(8,128)(2,1)}, u32[]{:S(2)}, u32[]{:S(2)}) %collective-permute-start.31) | collective-permute-done | bytes 524320 | tf_op jit(solution)/shard_map/ppermute | solution.py:33
  116.8 5.3 %intra.1 = (f32[768,512]{1,0:T(8,128)S(1)}, f32[768,512]{1,0:T(8,128)S(1)}, f32[768,128]{1,0:T(8,128)S(1)}) custom-call(bf16[768,256]{1,0:T(8,128)(2,1)S(1)} %copy-done.9, bf16[768,256]{1,0:T(8,128)(2,1)S(1)} %copy-done.11, bf16[768,512]{1,0:T(8,128)(2,1)S(1)} %copy-done, f32[8,768]{1,0:T(8,128)S(1)} %maximum_maximum_fusion.gates), custom_call_target="tpu_custom_call" | custom-call | tf_op jit(solution)/shard_map/intra/pallas_call | solution.py:246
  122.2 6.1 %emit.1 = (bf16[192,512]{1,0:T(8,128)(2,1)S(1)}, bf16[192,512]{1,0:T(8,128)(2,1)S(1)}, bf16[192,512]{1,0:T(8,128)(2,1)S(1)}, bf16[192,512]{1,0:T(8,128)(2,1)S(1)}) custom-call(s32[6]{0:T(128)S(1)} %stack.72.info, bf16[768,256]{1,0:T(8,128)(2,1)S(1)} %copy-done.9, f32[768,512]{1,0:T(8,128)S(1)} %get-tuple-element.34.num_f, ...), custom_call_target="tpu_custom_call" | custom-call | tf_op jit(solution)/shard_map/emit/pallas_call | solution.py:307
  129.0 1.4 collective-permute-done.4.refs_1_
  131.7 6.3 %collective-permute-done.5.refs_2_ = bf16[192,512]{1,0:T(8,128)(2,1)S(1)} collective-permute-done((bf16[192,512]{1,0:T(8,128)(2,1)S(1)}, bf16[192,512]{1,0:T(8,128)(2,1)S(1)}, u32[]{:S(2)}, u32[]{:S(2)}) %collective-permute-start.5) | collective-permute-done | bytes 196640 | tf_op jit(solution)/shard_map/ppermute | solution.py:33
  138.7 6.7 %collective-permute-done.6.refs_3_ = bf16[192,512]{1,0:T(8,128)(2,1)S(1)} collective-permute-done((bf16[192,512]{1,0:T(8,128)(2,1)S(1)}, bf16[192,512]{1,0:T(8,128)(2,1)S(1)}, u32[]{:S(2)}, u32[]{:S(2)}) %collective-permute-start.6) | collective-permute-done | bytes 196640 | tf_op jit(solution)/shard_map/ppermute | solution.py:33
  146.3 1.3 copy-done.3
  147.6 1.7 collective-permute-start.35
  149.4 1.4 copy-done.5
  151.2 1.6 copy-done.2
  152.8 1.6 copy-done.4
  154.4 1.6 copy-done.6
  159.7 3.7 %project.1 = (f32[192,2048]{1,0:T(8,128)S(1)}, bf16[192,2048]{1,0:T(8,128)(2,1)S(1)}, bf16[96,2048]{1,0:T(8,128)(2,1)S(1)}, bf16[96,2048]{1,0:T(8,128)(2,1)S(1)}) custom-call(s32[8]{0:T(128)S(1)} %stack.65.info, bf16[192,512]{1,0:T(8,128)(2,1)S(1)} %copy-done.21, bf16[192,512]{1,0:T(8,128)(2,1)S(1)} %copy-done.23, bf16[192,512]{1,0:T(8,128)(2,1)S(1)} %copy-done.25, ...), custom_call_target="tpu_custom_call" | custom-call | tf_op jit(solution)/shard_map/project/pallas_call | solution.py:353
  163.5 1.2 collective-permute-start.12
  164.6 7.7 %collective-permute-done.35.refs_0_ = bf16[1024,256]{1,0:T(8,128)(2,1)} collective-permute-done((bf16[1024,256]{1,0:T(8,128)(2,1)}, bf16[1024,256]{1,0:T(8,128)(2,1)}, u32[]{:S(2)}, u32[]{:S(2)}) %collective-permute-start.35) | collective-permute-done | bytes 524320 | tf_op jit(solution)/shard_map/ppermute | solution.py:25
  172.4 9.8 %collective-permute-done.36.refs_1_ = bf16[1024,256]{1,0:T(8,128)(2,1)} collective-permute-done((bf16[1024,256]{1,0:T(8,128)(2,1)}, bf16[1024,256]{1,0:T(8,128)(2,1)}, u32[]{:S(2)}, u32[]{:S(2)}) %collective-permute-start.36) | collective-permute-done | bytes 524320 | tf_op jit(solution)/shard_map/ppermute | solution.py:25
  182.2 1.1 shard_map.131.refs_0_
  183.4 1.1 shard_map.132.refs_2_
  185.1 1.3 shard_map.136.refs_0_
  186.5 1.3 shard_map.139.refs_0_
  187.8 4.2 %collective-permute-done.11.refs_2_ = bf16[96,2048]{1,0:T(8,128)(2,1)S(1)} collective-permute-done((bf16[96,2048]{1,0:T(8,128)(2,1)S(1)}, bf16[96,2048]{1,0:T(8,128)(2,1)S(1)}, u32[]{:S(2)}, u32[]{:S(2)}) %collective-permute-start.11) | collective-permute-done | bytes 393248 | tf_op jit(solution)/shard_map/ppermute | solution.py:38
  192.0 2.0 collective-permute-start.22
  194.0 9.8 %collective-permute-done.22.refs_0_ = bf16[96,2048]{1,0:T(8,128)(2,1)S(1)} collective-permute-done((bf16[96,2048]{1,0:T(8,128)(2,1)S(1)}, bf16[96,2048]{1,0:T(8,128)(2,1)S(1)}, u32[]{:S(2)}, u32[]{:S(2)}) %collective-permute-start.22) | collective-permute-done | bytes 393248 | tf_op jit(solution)/shard_map/ppermute | solution.py:33
  203.8 1.7 collective-permute-start.23
  205.5 7.9 %shard_map.129.early = bf16[576,2048]{1,0:T(8,128)(2,1)S(1)} custom-call(bf16[192,2048]{1,0:T(8,128)(2,1)S(1)} %get-tuple-element.44.refs_0_, bf16[96,2048]{1,0:T(8,128)(2,1)S(1)} %collective-permute-done.10.refs_1_, bf16[96,2048]{1,0:T(8,128)(2,1)S(1)} %collective-permute-done.11.refs_2_, bf16[192,2048]{1,0:T(8,128)(2,1)S(1)} %collective-permute-done.12.refs_3_, ...), custom_call_target="tpu_custom_call" | custom-call | tf_op jit(solution)/shard_map/pallas_call | solution.py:415
  213.4 1.3 collective-permute-done.23.refs_1_
  214.7 4.7 %shard_map.130.late = bf16[192,2048]{1,0:T(8,128)(2,1)S(1)} custom-call(bf16[96,2048]{1,0:T(8,128)(2,1)S(1)} %collective-permute-done.22.refs_0_, bf16[96,2048]{1,0:T(8,128)(2,1)S(1)} %collective-permute-done.23.refs_1_, bf16[4,256,1024]{2,1,0:T(8,128)(2,1)S(1)} %shard_map.127.refs_4_.refs_2_, bf16[4,256,1024]{2,1,0:T(8,128)(2,1)} %shard_map.128.refs_5_.refs_3_, ...), custom_call_target="tpu_custom_call" | custom-call | tf_op jit(solution)/shard_map/pallas_call | solution.py:415
  219.4 3.4 %shard_map.133 = (f32[384,512]{1,0:T(8,128)S(1)}, bf16[384,512]{1,0:T(8,128)(2,1)S(1)}, f32[384,512]{1,0:T(8,128)S(1)}, bf16[384,512]{1,0:T(8,128)(2,1)S(1)}) custom-call(bf16[576,2048]{1,0:T(8,128)(2,1)S(1)} %shard_map.129.early, bf16[192,2048]{1,0:T(8,128)(2,1)S(1)} %shard_map.130.late, bf16[2,1024,256]{2,1,0:T(8,128)(2,1)S(1)} %shard_map.131.refs_0_, ...), custom_call_target="tpu_custom_call" | custom-call | tf_op jit(solution)/shard_map/pallas_call | solution.py:472
  222.9 1.5 collective-permute-start.29
  224.7 1.8 shard_map.137
  227.1 1.8 shard_map.140
  228.9 1.8 collective-permute-start.38
  230.7 4.2 %collective-permute-done.29.theirs = bf16[384,512]{1,0:T(8,128)(2,1)S(1)} collective-permute-done((bf16[384,512]{1,0:T(8,128)(2,1)S(1)}, bf16[384,512]{1,0:T(8,128)(2,1)S(1)}, u32[]{:S(2)}, u32[]{:S(2)}) %collective-permute-start.29) | collective-permute-done | bytes 393248 | tf_op jit(solution)/shard_map/ppermute | solution.py:33
  235.3 1.0 collective-permute-done.30.theirs
  237.1 6.3 %collective-permute-done.34.theirs = bf16[384,512]{1,0:T(8,128)(2,1)S(1)} collective-permute-done((bf16[384,512]{1,0:T(8,128)(2,1)S(1)}, bf16[384,512]{1,0:T(8,128)(2,1)S(1)}, u32[]{:S(2)}, u32[]{:S(2)}) %collective-permute-start.34) | collective-permute-done | bytes 393248 | tf_op jit(solution)/shard_map/ppermute | solution.py:33
  243.8 1.0 collective-permute-done.38.theirs
  245.5 3.2 %collective-permute-done.39.refs_4_ = bf16[192,512]{1,0:T(8,128)(2,1)S(1)} collective-permute-done((bf16[192,512]{1,0:T(8,128)(2,1)S(1)}, bf16[192,512]{1,0:T(8,128)(2,1)S(1)}, u32[]{:S(2)}, u32[]{:S(2)}) %collective-permute-start.39) | collective-permute-done | bytes 196640 | tf_op jit(solution)/shard_map/ppermute | solution.py:38
  248.7 2.1 collective-permute-done.41.refs_6_
  250.8 1.7 finish.1
  (120 shorter events, 16.2 us)
Async XLA Ops:
  0.0 8.2 %copy-start.32 = (s32[768]{0:T(1024)S(1)}, s32[768]{0:T(1024)}, u32[]{:S(2)}) copy-start(s32[768]{0:T(1024)} %param.19) | copy-start | bytes 9220
  0.0 8.3 %copy-start.30 = (f32[2,1,768]{2,1,0:T(1,128)S(1)}, f32[2,1,768]{2,1,0:T(1,128)}, u32[]{:S(2)}) copy-start(f32[2,1,768]{2,1,0:T(1,128)} %param.18) | copy-start | bytes 18436
  0.0 8.3 %copy-start.31 = (f32[2,1,768]{2,1,0:T(1,128)S(1)}, f32[2,1,768]{2,1,0:T(1,128)}, u32[]{:S(2)}) copy-start(f32[2,1,768]{2,1,0:T(1,128)} %param.17) | copy-start | bytes 18436
  0.0 8.5 %copy-start.10 = (bf16[768,256]{1,0:T(8,128)(2,1)S(1)}, bf16[768,256]{1,0:T(8,128)(2,1)}, u32[]{:S(2)}) copy-start(bf16[768,256]{1,0:T(8,128)(2,1)} %keys.3) | copy-start | bytes 1179652
  0.0 8.5 %copy-start = (bf16[768,512]{1,0:T(8,128)(2,1)S(1)}, bf16[768,512]{1,0:T(8,128)(2,1)}, u32[]{:S(2)}) copy-start(bf16[768,512]{1,0:T(8,128)(2,1)} %values.3) | copy-start | bytes 2359300
  0.0 60.4 %collective-permute-start.8 = (bf16[512,2048]{1,0:T(8,128)(2,1)}, bf16[512,2048]{1,0:T(8,128)(2,1)}, u32[]{:S(2)}, u32[]{:S(2)}) collective-permute-start(bf16[512,2048]{1,0:T(8,128)(2,1)} %refs_4_.1), channel_id=1, source_target_pairs={{0,2},{1,3},{2,0},{3,1},{4,6},{5,7},{6,4},{7,5},{8,10},{9,11},{10,... | collective-permute-start | bytes 6291464 | tf_op jit(solution)/shard_map/ppermute | solution.py:33
  5.1 28.4 %copy-start.7 = (bf16[256,1024]{1,0:T(8,128)(2,1)}, bf16[256,1024]{1,0:T(8,128)(2,1)S(1)}, u32[]{:S(2)}) copy-start(bf16[256,1024]{1,0:T(8,128)(2,1)S(1)} %get-tuple-element.66.refs_0_) | copy-start | bytes 1572868
  5.1 25.5 %collective-permute-start.13 = (bf16[256,1024]{1,0:T(8,128)(2,1)}, bf16[256,1024]{1,0:T(8,128)(2,1)S(1)}, u32[]{:S(2)}, u32[]{:S(2)}) collective-permute-start(bf16[256,1024]{1,0:T(8,128)(2,1)} %get-tuple-element.65), channel_id=1, source_target_pairs={{0,8},{4,12},{8,0},{12,4},{16,24},{20,28},{24,16},{28,20},{1,9},{5... | collective-permute-start | bytes 1572872 | tf_op jit(solution)/shard_map/ppermute | solution.py:38
  6.7 24.6 %collective-permute-start.14 = (bf16[256,1024]{1,0:T(8,128)(2,1)S(1)}, bf16[256,1024]{1,0:T(8,128)(2,1)S(1)}, u32[]{:S(2)}, u32[]{:S(2)}) collective-permute-start(bf16[256,1024]{1,0:T(8,128)(2,1)S(1)} %get-tuple-element.66.refs_0_), channel_id=1, source_target_pairs={{0,4},{4,0},{8,12},{12,8},{16,20},{20,16},{24,28},{28,24},{1,5},{5... | collective-permute-start | bytes 1572872 | tf_op jit(solution)/shard_map/ppermute | solution.py:25
  8.5 51.8 %copy-start.1 = (bf16[512,2048]{1,0:T(8,128)(2,1)S(1)}, bf16[512,2048]{1,0:T(8,128)(2,1)}, u32[]{:S(2)}) copy-start(bf16[512,2048]{1,0:T(8,128)(2,1)} %refs_4_.1) | copy-start | bytes 6291460
  11.1 15.8 %collective-permute-start = (bf16[256,640]{1,0:T(8,128)(2,1)S(1)}, bf16[256,640]{1,0:T(8,128)(2,1)S(1)}, u32[]{:S(2)}, u32[]{:S(2)}) collective-permute-start(bf16[256,640]{1,0:T(8,128)(2,1)S(1)} %get-tuple-element.37), channel_id=1, source_target_pairs={{0,4},{4,0},{8,12},{12,8},{16,20},{20,16},{24,28},{28,24},{1,5},{5... | collective-permute-start | bytes 983048 | tf_op jit(solution)/shard_map/ppermute | solution.py:25
  11.6 38.2 %collective-permute-start.16 = (bf16[256,1024]{1,0:T(8,128)(2,1)S(1)}, bf16[256,1024]{1,0:T(8,128)(2,1)S(1)}, u32[]{:S(2)}, u32[]{:S(2)}) collective-permute-start(bf16[256,1024]{1,0:T(8,128)(2,1)S(1)} %get-tuple-element.66.refs_0_), channel_id=1, source_target_pairs={{0,16},{4,20},{8,24},{12,28},{16,0},{20,4},{24,8},{28,12},{1,17},{... | collective-permute-start | bytes 1572872 | tf_op jit(solution)/shard_map/ppermute | solution.py:33
  26.8 24.3 %collective-permute-start.17 = (bf16[256,1024]{1,0:T(8,128)(2,1)}, bf16[256,1024]{1,0:T(8,128)(2,1)S(1)}, u32[]{:S(2)}, u32[]{:S(2)}) collective-permute-start(bf16[256,1024]{1,0:T(8,128)(2,1)} %get-tuple-element.65), channel_id=1, source_target_pairs={{0,24},{4,28},{8,16},{12,20},{16,8},{20,12},{24,0},{28,4},{1,25},{... | collective-permute-start | bytes 1572872 | tf_op jit(solution)/shard_map/ppermute | solution.py:44
  30.6 64.1 %copy-start.16 = (bf16[256,1024]{1,0:T(8,128)(2,1)}, bf16[256,1024]{1,0:T(8,128)(2,1)S(1)}, u32[]{:S(2)}) copy-start(bf16[256,1024]{1,0:T(8,128)(2,1)S(1)} %collective-permute-done.13.refs_1_) | copy-start | bytes 1572868
  30.6 28.4 %collective-permute-start.24 = (bf16[1024,256]{1,0:T(8,128)(2,1)S(1)}, bf16[1024,256]{1,0:T(8,128)(2,1)}, u32[]{:S(2)}, u32[]{:S(2)}) collective-permute-start(bf16[1024,256]{1,0:T(8,128)(2,1)S(1)} %get-tuple-element.63), channel_id=1, source_target_pairs={{0,8},{4,12},{8,0},{12,4},{16,24},{20,28},{24,16},{28,20},{1,9},{5... | collective-permute-start | bytes 1572872 | tf_op jit(solution)/shard_map/ppermute | solution.py:38
  31.3 63.4 %copy-start.18 = (bf16[256,1024]{1,0:T(8,128)(2,1)}, bf16[256,1024]{1,0:T(8,128)(2,1)S(1)}, u32[]{:S(2)}) copy-start(bf16[256,1024]{1,0:T(8,128)(2,1)S(1)} %collective-permute-done.14.refs_2_) | copy-start | bytes 1572868
  31.3 29.0 %collective-permute-start.26 = (bf16[1024,256]{1,0:T(8,128)(2,1)S(1)}, bf16[1024,256]{1,0:T(8,128)(2,1)S(1)}, u32[]{:S(2)}, u32[]{:S(2)}) collective-permute-start(bf16[1024,256]{1,0:T(8,128)(2,1)S(1)} %get-tuple-element.64.refs_0_), channel_id=1, source_target_pairs={{0,4},{4,0},{8,12},{12,8},{16,20},{20,16},{24,28},{28,24},{1,5},{5... | collective-permute-start | bytes 1572872 | tf_op jit(solution)/shard_map/ppermute | solution.py:25
  49.8 15.0 %collective-permute-start.1 = (bf16[256,640]{1,0:T(8,128)(2,1)S(1)}, bf16[256,640]{1,0:T(8,128)(2,1)S(1)}, u32[]{:S(2)}, u32[]{:S(2)}) collective-permute-start(bf16[256,640]{1,0:T(8,128)(2,1)S(1)} %pair.1), channel_id=1, source_target_pairs={{8,0},{16,8},{24,16},{4,12},{12,20},{20,28},{9,1},{17,9},{25,17},{... | collective-permute-start | bytes 983048 | tf_op jit(solution)/shard_map/ppermute | solution.py:51
  51.1 28.8 %collective-permute-start.15 = (bf16[256,1024]{1,0:T(8,128)(2,1)S(1)}, bf16[256,1024]{1,0:T(8,128)(2,1)S(1)}, u32[]{:S(2)}, u32[]{:S(2)}) collective-permute-start(bf16[256,1024]{1,0:T(8,128)(2,1)S(1)} %collective-permute-done.13.refs_1_), channel_id=1, source_target_pairs={{0,4},{4,0},{8,12},{12,8},{16,20},{20,16},{24,28},{28,24},{1,5},{5... | collective-permute-start | bytes 1572872 | tf_op jit(solution)/shard_map/ppermute | solution.py:25
  59.0 20.9 %collective-permute-start.2 = (bf16[256,640]{1,0:T(8,128)(2,1)S(1)}, bf16[256,640]{1,0:T(8,128)(2,1)S(1)}, u32[]{:S(2)}, u32[]{:S(2)}) collective-permute-start(bf16[256,640]{1,0:T(8,128)(2,1)S(1)} %pair.1), channel_id=1, source_target_pairs={{16,0},{24,8},{4,20},{12,28},{17,1},{25,9},{5,21},{13,29},{18,2},{... | collective-permute-start | bytes 983048 | tf_op jit(solution)/shard_map/ppermute | solution.py:51
  60.3 34.4 %copy-start.14 = (bf16[1024,256]{1,0:T(8,128)(2,1)}, bf16[1024,256]{1,0:T(8,128)(2,1)S(1)}, u32[]{:S(2)}) copy-start(bf16[1024,256]{1,0:T(8,128)(2,1)S(1)} %collective-permute-done.26.refs_0_) | copy-start | bytes 1572868
  60.3 86.0 %collective-permute-start.7 = (bf16[512,2048]{1,0:T(8,128)(2,1)S(1)}, bf16[512,2048]{1,0:T(8,128)(2,1)S(1)}, u32[]{:S(2)}, u32[]{:S(2)}) collective-permute-start(bf16[512,2048]{1,0:T(8,128)(2,1)S(1)} %copy-done.1), channel_id=1, source_target_pairs={{0,1},{1,0},{2,3},{3,2},{4,5},{5,4},{6,7},{7,6},{8,9},{9,8},{10,11... | collective-permute-start | bytes 6291464 | tf_op jit(solution)/shard_map/ppermute | solution.py:25
  60.4 89.0 %collective-permute-start.9 = (bf16[512,2048]{1,0:T(8,128)(2,1)}, bf16[512,2048]{1,0:T(8,128)(2,1)S(1)}, u32[]{:S(2)}, u32[]{:S(2)}) collective-permute-start(bf16[512,2048]{1,0:T(8,128)(2,1)} %collective-permute-done.8.refs_6_), channel_id=1, source_target_pairs={{0,1},{1,0},{2,3},{3,2},{4,5},{5,4},{6,7},{7,6},{8,9},{9,8},{10,11... | collective-permute-start | bytes 6291464 | tf_op jit(solution)/shard_map/ppermute | solution.py:25
  64.8 16.3 %collective-permute-start.18 = (bf16[256,1024]{1,0:T(8,128)(2,1)S(1)}, bf16[256,1024]{1,0:T(8,128)(2,1)S(1)}, u32[]{:S(2)}, u32[]{:S(2)}) collective-permute-start(bf16[256,1024]{1,0:T(8,128)(2,1)S(1)} %collective-permute-done.16.refs_0_), channel_id=1, source_target_pairs={{0,4},{4,0},{8,12},{12,8},{16,20},{20,16},{24,28},{28,24},{1,5},{5... | collective-permute-start | bytes 1572872 | tf_op jit(solution)/shard_map/ppermute | solution.py:25
  79.9 14.8 %collective-permute-start.19 = (bf16[256,1024]{1,0:T(8,128)(2,1)S(1)}, bf16[256,1024]{1,0:T(8,128)(2,1)S(1)}, u32[]{:S(2)}, u32[]{:S(2)}) collective-permute-start(bf16[256,1024]{1,0:T(8,128)(2,1)S(1)} %collective-permute-done.17.refs_1_), channel_id=1, source_target_pairs={{0,4},{4,0},{8,12},{12,8},{16,20},{20,16},{24,28},{28,24},{1,5},{5... | collective-permute-start | bytes 1572872 | tf_op jit(solution)/shard_map/ppermute | solution.py:25
  79.9 36.4 %collective-permute-start.31 = (bf16[1024,256]{1,0:T(8,128)(2,1)S(1)}, bf16[1024,256]{1,0:T(8,128)(2,1)}, u32[]{:S(2)}, u32[]{:S(2)}) collective-permute-start(bf16[1024,256]{1,0:T(8,128)(2,1)S(1)} %get-tuple-element.64.refs_0_), channel_id=1, source_target_pairs={{0,16},{4,20},{8,24},{12,28},{16,0},{20,4},{24,8},{28,12},{1,17},{... | collective-permute-start | bytes 1572872 | tf_op jit(solution)/shard_map/ppermute | solution.py:33
  81.1 35.2 %collective-permute-start.3 = (bf16[256,640]{1,0:T(8,128)(2,1)S(1)}, bf16[256,640]{1,0:T(8,128)(2,1)S(1)}, u32[]{:S(2)}, u32[]{:S(2)}) collective-permute-start(bf16[256,640]{1,0:T(8,128)(2,1)S(1)} %lead.1), channel_id=1, source_target_pairs={{0,4},{4,0},{8,12},{12,8},{16,20},{20,16},{24,28},{28,24},{1,5},{5... | collective-permute-start | bytes 983048 | tf_op jit(solution)/shard_map/ppermute | solution.py:25
  94.7 34.2 %collective-permute-start.32 = (bf16[1024,256]{1,0:T(8,128)(2,1)S(1)}, bf16[1024,256]{1,0:T(8,128)(2,1)}, u32[]{:S(2)}, u32[]{:S(2)}) collective-permute-start(bf16[1024,256]{1,0:T(8,128)(2,1)S(1)} %get-tuple-element.63), channel_id=1, source_target_pairs={{0,24},{4,28},{8,16},{12,20},{16,8},{20,12},{24,0},{28,4},{1,25},{... | collective-permute-start | bytes 1572872 | tf_op jit(solution)/shard_map/ppermute | solution.py:44
  100.0 16.8 %copy-start.9 = (bf16[768,256]{1,0:T(8,128)(2,1)S(1)}, bf16[768,256]{1,0:T(8,128)(2,1)}, u32[]{:S(2)}) copy-start(bf16[768,256]{1,0:T(8,128)(2,1)} %queries.3) | copy-start | bytes 1179652
  100.0 16.8 %copy-start.11 = (bf16[768,256]{1,0:T(8,128)(2,1)S(1)}, bf16[768,256]{1,0:T(8,128)(2,1)}, u32[]{:S(2)}) copy-start(bf16[768,256]{1,0:T(8,128)(2,1)} %keys.3) | copy-start | bytes 1179652
  100.1 22.1 %copy-start.13 = (bf16[768,512]{1,0:T(8,128)(2,1)S(1)}, bf16[768,512]{1,0:T(8,128)(2,1)}, u32[]{:S(2)}) copy-start(bf16[768,512]{1,0:T(8,128)(2,1)} %out_gate.1) | copy-start | bytes 2359300
  100.1 22.1 %copy-start.29 = (f32[512]{0:T(512)S(1)}, f32[512]{0:T(512)}, u32[]{:S(2)}) copy-start(f32[512]{0:T(512)} %param.20) | copy-start | bytes 6148
  116.3 68.2 %collective-permute-start.20 = (bf16[4,256,1024]{2,1,0:T(8,128)(2,1)S(1)}, bf16[4,256,1024]{2,1,0:T(8,128)(2,1)}, u32[]{:S(2)}, u32[]{:S(2)}) collective-permute-start(bf16[4,256,1024]{2,1,0:T(8,128)(2,1)S(1)} %shard_map.127.refs_4_.refs_2_), channel_id=1, source_target_pairs={{0,1},{1,0},{2,3},{3,2},{4,5},{5,4},{6,7},{7,6},{8,9},{9,8},{10,11... | collective-permute-start | bytes 6291464 | tf_op jit(solution)/shard_map/ppermute | solution.py:25
  116.3 68.2 %collective-permute-start.21 = (bf16[4,256,1024]{2,1,0:T(8,128)(2,1)}, bf16[4,256,1024]{2,1,0:T(8,128)(2,1)}, u32[]{:S(2)}, u32[]{:S(2)}) collective-permute-start(bf16[4,256,1024]{2,1,0:T(8,128)(2,1)} %shard_map.128.refs_5_.refs_3_), channel_id=1, source_target_pairs={{0,1},{1,0},{2,3},{3,2},{4,5},{5,4},{6,7},{7,6},{8,9},{9,8},{10,11... | collective-permute-start | bytes 6291464 | tf_op jit(solution)/shard_map/ppermute | solution.py:25
  122.2 29.0 %copy-start.12 = (bf16[192,2048]{1,0:T(8,128)(2,1)S(1)}, bf16[192,2048]{1,0:T(8,128)(2,1)}, u32[]{:S(2)}) copy-start(bf16[192,2048]{1,0:T(8,128)(2,1)} %refs_8_.1) | copy-start | bytes 2359300
  122.2 29.0 %copy-start.28 = (f32[2048]{0:T(1024)S(1)}, f32[2048]{0:T(1024)}, u32[]{:S(2)}) copy-start(f32[2048]{0:T(1024)} %param.23) | copy-start | bytes 24580
  129.0 1.4 collective-permute-start.4
  131.1 6.9 %collective-permute-start.5 = (bf16[192,512]{1,0:T(8,128)(2,1)S(1)}, bf16[192,512]{1,0:T(8,128)(2,1)S(1)}, u32[]{:S(2)}, u32[]{:S(2)}) collective-permute-start(bf16[192,512]{1,0:T(8,128)(2,1)S(1)} %get-tuple-element.41), channel_id=1, source_target_pairs={{0,2},{1,3},{2,0},{3,1},{4,6},{5,7},{6,4},{7,5},{8,10},{9,11},{10,... | collective-permute-start | bytes 589832 | tf_op jit(solution)/shard_map/ppermute | solution.py:33
  138.7 6.7 %collective-permute-start.6 = (bf16[192,512]{1,0:T(8,128)(2,1)S(1)}, bf16[192,512]{1,0:T(8,128)(2,1)S(1)}, u32[]{:S(2)}, u32[]{:S(2)}) collective-permute-start(bf16[192,512]{1,0:T(8,128)(2,1)S(1)} %get-tuple-element.42), channel_id=1, source_target_pairs={{0,3},{1,2},{2,1},{3,0},{4,7},{5,6},{6,5},{7,4},{8,11},{9,10},{10,... | collective-permute-start | bytes 589832 | tf_op jit(solution)/shard_map/ppermute | solution.py:33
  146.0 17.4 %collective-permute-start.27 = (bf16[1024,256]{1,0:T(8,128)(2,1)}, bf16[1024,256]{1,0:T(8,128)(2,1)}, u32[]{:S(2)}, u32[]{:S(2)}) collective-permute-start(bf16[1024,256]{1,0:T(8,128)(2,1)} %collective-permute-done.24.refs_1_), channel_id=1, source_target_pairs={{0,4},{4,0},{8,12},{12,8},{16,20},{20,16},{24,28},{28,24},{1,5},{5... | collective-permute-start | bytes 1572872 | tf_op jit(solution)/shard_map/ppermute | solution.py:25
  147.6 24.7 %collective-permute-start.35 = (bf16[1024,256]{1,0:T(8,128)(2,1)}, bf16[1024,256]{1,0:T(8,128)(2,1)}, u32[]{:S(2)}, u32[]{:S(2)}) collective-permute-start(bf16[1024,256]{1,0:T(8,128)(2,1)} %collective-permute-done.31.refs_0_), channel_id=1, source_target_pairs={{0,4},{4,0},{8,12},{12,8},{16,20},{20,16},{24,28},{28,24},{1,5},{5... | collective-permute-start | bytes 1572872 | tf_op jit(solution)/shard_map/ppermute | solution.py:25
  149.4 1.4 copy-start.5
  150.8 31.4 %collective-permute-start.36 = (bf16[1024,256]{1,0:T(8,128)(2,1)}, bf16[1024,256]{1,0:T(8,128)(2,1)}, u32[]{:S(2)}, u32[]{:S(2)}) collective-permute-start(bf16[1024,256]{1,0:T(8,128)(2,1)} %collective-permute-done.32.refs_1_), channel_id=1, source_target_pairs={{0,4},{4,0},{8,12},{12,8},{16,20},{20,16},{24,28},{28,24},{1,5},{5... | collective-permute-start | bytes 1572872 | tf_op jit(solution)/shard_map/ppermute | solution.py:25
  151.2 1.6 copy-start.2
  152.8 1.6 copy-start.4
  154.4 1.6 copy-start.6
  163.4 19.9 %copy-start.15 = (bf16[1024,256]{1,0:T(8,128)(2,1)S(1)}, bf16[1024,256]{1,0:T(8,128)(2,1)}, u32[]{:S(2)}) copy-start(bf16[1024,256]{1,0:T(8,128)(2,1)} %copy-done.14) | copy-start | bytes 1572868
  163.5 28.5 %collective-permute-start.12 = (bf16[192,2048]{1,0:T(8,128)(2,1)S(1)}, bf16[192,2048]{1,0:T(8,128)(2,1)S(1)}, u32[]{:S(2)}, u32[]{:S(2)}) collective-permute-start(bf16[192,2048]{1,0:T(8,128)(2,1)S(1)} %get-tuple-element.44.refs_0_), channel_id=1, source_target_pairs={{0,2},{1,3},{2,0},{3,1},{4,6},{5,7},{6,4},{7,5},{8,10},{9,11},{10,... | collective-permute-start | bytes 2359304 | tf_op jit(solution)/shard_map/ppermute | solution.py:33
  172.4 13.9 %collective-permute-start.10 = (bf16[96,2048]{1,0:T(8,128)(2,1)S(1)}, bf16[96,2048]{1,0:T(8,128)(2,1)S(1)}, u32[]{:S(2)}, u32[]{:S(2)}) collective-permute-start(bf16[96,2048]{1,0:T(8,128)(2,1)S(1)} %get-tuple-element.45), channel_id=1, source_target_pairs={{0,8},{4,12},{8,0},{12,4},{16,24},{20,28},{24,16},{28,20},{1,9},{5... | collective-permute-start | bytes 1179656 | tf_op jit(solution)/shard_map/ppermute | solution.py:38
  182.2 9.7 %collective-permute-start.11 = (bf16[96,2048]{1,0:T(8,128)(2,1)S(1)}, bf16[96,2048]{1,0:T(8,128)(2,1)S(1)}, u32[]{:S(2)}, u32[]{:S(2)}) collective-permute-start(bf16[96,2048]{1,0:T(8,128)(2,1)S(1)} %get-tuple-element.46), channel_id=1, source_target_pairs={{0,8},{4,12},{8,0},{12,4},{16,24},{20,28},{24,16},{28,20},{1,9},{5... | collective-permute-start | bytes 1179656 | tf_op jit(solution)/shard_map/ppermute | solution.py:38
  184.5 34.9 %collective-permute-start.25 = (bf16[2,1024,256]{2,1,0:T(8,128)(2,1)S(1)}, bf16[2,1024,256]{2,1,0:T(8,128)(2,1)S(1)}, u32[]{:S(2)}, u32[]{:S(2)}) collective-permute-start(bf16[2,1024,256]{2,1,0:T(8,128)(2,1)S(1)} %shard_map.131.refs_0_), channel_id=1, source_target_pairs={{0,1},{1,0},{2,3},{3,2},{4,5},{5,4},{6,7},{7,6},{8,9},{9,8},{10,11... | collective-permute-start | bytes 3145736 | tf_op jit(solution)/shard_map/ppermute | solution.py:25
  184.6 34.9 %collective-permute-start.28 = (bf16[2,1024,256]{2,1,0:T(8,128)(2,1)S(1)}, bf16[2,1024,256]{2,1,0:T(8,128)(2,1)S(1)}, u32[]{:S(2)}, u32[]{:S(2)}) collective-permute-start(bf16[2,1024,256]{2,1,0:T(8,128)(2,1)S(1)} %shard_map.132.refs_2_), channel_id=1, source_target_pairs={{0,1},{1,0},{2,3},{3,2},{4,5},{5,4},{6,7},{7,6},{8,9},{9,8},{10,11... | collective-permute-start | bytes 3145736 | tf_op jit(solution)/shard_map/ppermute | solution.py:25
  186.3 38.3 %collective-permute-start.33 = (bf16[2,1024,256]{2,1,0:T(8,128)(2,1)S(1)}, bf16[2,1024,256]{2,1,0:T(8,128)(2,1)S(1)}, u32[]{:S(2)}, u32[]{:S(2)}) collective-permute-start(bf16[2,1024,256]{2,1,0:T(8,128)(2,1)S(1)} %shard_map.136.refs_0_), channel_id=1, source_target_pairs={{0,1},{1,0},{2,3},{3,2},{4,5},{5,4},{6,7},{7,6},{8,9},{9,8},{10,11... | collective-permute-start | bytes 3145736 | tf_op jit(solution)/shard_map/ppermute | solution.py:25
  192.0 35.1 %collective-permute-start.37 = (bf16[2,1024,256]{2,1,0:T(8,128)(2,1)S(1)}, bf16[2,1024,256]{2,1,0:T(8,128)(2,1)S(1)}, u32[]{:S(2)}, u32[]{:S(2)}) collective-permute-start(bf16[2,1024,256]{2,1,0:T(8,128)(2,1)S(1)} %shard_map.139.refs_0_), channel_id=1, source_target_pairs={{0,1},{1,0},{2,3},{3,2},{4,5},{5,4},{6,7},{7,6},{8,9},{9,8},{10,11... | collective-permute-start | bytes 3145736 | tf_op jit(solution)/shard_map/ppermute | solution.py:25
  192.0 11.8 %collective-permute-start.22 = (bf16[96,2048]{1,0:T(8,128)(2,1)S(1)}, bf16[96,2048]{1,0:T(8,128)(2,1)S(1)}, u32[]{:S(2)}, u32[]{:S(2)}) collective-permute-start(bf16[96,2048]{1,0:T(8,128)(2,1)S(1)} %collective-permute-done.10.refs_1_), channel_id=1, source_target_pairs={{0,2},{1,3},{2,0},{3,1},{4,6},{5,7},{6,4},{7,5},{8,10},{9,11},{10,... | collective-permute-start | bytes 1179656 | tf_op jit(solution)/shard_map/ppermute | solution.py:33
  203.8 10.9 %collective-permute-start.23 = (bf16[96,2048]{1,0:T(8,128)(2,1)S(1)}, bf16[96,2048]{1,0:T(8,128)(2,1)S(1)}, u32[]{:S(2)}, u32[]{:S(2)}) collective-permute-start(bf16[96,2048]{1,0:T(8,128)(2,1)S(1)} %collective-permute-done.11.refs_2_), channel_id=1, source_target_pairs={{0,2},{1,3},{2,0},{3,1},{4,6},{5,7},{6,4},{7,5},{8,10},{9,11},{10,... | collective-permute-start | bytes 1179656 | tf_op jit(solution)/shard_map/ppermute | solution.py:33
  222.9 12.1 %collective-permute-start.29 = (bf16[384,512]{1,0:T(8,128)(2,1)S(1)}, bf16[384,512]{1,0:T(8,128)(2,1)S(1)}, u32[]{:S(2)}, u32[]{:S(2)}) collective-permute-start(bf16[384,512]{1,0:T(8,128)(2,1)S(1)} %get-tuple-element.48), channel_id=1, source_target_pairs={{0,2},{1,3},{2,0},{3,1},{4,6},{5,7},{6,4},{7,5},{8,10},{9,11},{10,... | collective-permute-start | bytes 1179656 | tf_op jit(solution)/shard_map/ppermute | solution.py:33
  224.4 12.0 %collective-permute-start.30 = (bf16[384,512]{1,0:T(8,128)(2,1)S(1)}, bf16[384,512]{1,0:T(8,128)(2,1)S(1)}, u32[]{:S(2)}, u32[]{:S(2)}) collective-permute-start(bf16[384,512]{1,0:T(8,128)(2,1)S(1)} %get-tuple-element.51), channel_id=1, source_target_pairs={{0,8},{4,12},{8,0},{12,4},{16,24},{20,28},{24,16},{28,20},{1,9},{5... | collective-permute-start | bytes 1179656 | tf_op jit(solution)/shard_map/ppermute | solution.py:38
  226.5 16.9 %collective-permute-start.34 = (bf16[384,512]{1,0:T(8,128)(2,1)S(1)}, bf16[384,512]{1,0:T(8,128)(2,1)S(1)}, u32[]{:S(2)}, u32[]{:S(2)}) collective-permute-start(bf16[384,512]{1,0:T(8,128)(2,1)S(1)} %get-tuple-element.54), channel_id=1, source_target_pairs={{0,2},{1,3},{2,0},{3,1},{4,6},{5,7},{6,4},{7,5},{8,10},{9,11},{10,... | collective-permute-start | bytes 1179656 | tf_op jit(solution)/shard_map/ppermute | solution.py:33
  228.9 15.9 %collective-permute-start.38 = (bf16[384,512]{1,0:T(8,128)(2,1)S(1)}, bf16[384,512]{1,0:T(8,128)(2,1)S(1)}, u32[]{:S(2)}, u32[]{:S(2)}) collective-permute-start(bf16[384,512]{1,0:T(8,128)(2,1)S(1)} %get-tuple-element.57), channel_id=1, source_target_pairs={{0,8},{4,12},{8,0},{12,4},{16,24},{20,28},{24,16},{28,20},{1,9},{5... | collective-permute-start | bytes 1179656 | tf_op jit(solution)/shard_map/ppermute | solution.py:38
  235.0 13.7 %collective-permute-start.39 = (bf16[192,512]{1,0:T(8,128)(2,1)S(1)}, bf16[192,512]{1,0:T(8,128)(2,1)S(1)}, u32[]{:S(2)}, u32[]{:S(2)}) collective-permute-start(bf16[192,512]{1,0:T(8,128)(2,1)S(1)} %get-tuple-element.59), channel_id=1, source_target_pairs={{0,8},{4,12},{8,0},{12,4},{16,24},{20,28},{24,16},{28,20},{1,9},{5... | collective-permute-start | bytes 589832 | tf_op jit(solution)/shard_map/ppermute | solution.py:38
  236.4 12.2 %collective-permute-start.40 = (bf16[192,512]{1,0:T(8,128)(2,1)S(1)}, bf16[192,512]{1,0:T(8,128)(2,1)S(1)}, u32[]{:S(2)}, u32[]{:S(2)}) collective-permute-start(bf16[192,512]{1,0:T(8,128)(2,1)S(1)} %get-tuple-element.60), channel_id=1, source_target_pairs={{0,2},{1,3},{2,0},{3,1},{4,6},{5,7},{6,4},{7,5},{8,10},{9,11},{10,... | collective-permute-start | bytes 589832 | tf_op jit(solution)/shard_map/ppermute | solution.py:33
  243.4 7.4 %collective-permute-start.41 = (bf16[192,512]{1,0:T(8,128)(2,1)S(1)}, bf16[192,512]{1,0:T(8,128)(2,1)S(1)}, u32[]{:S(2)}, u32[]{:S(2)}) collective-permute-start(bf16[192,512]{1,0:T(8,128)(2,1)S(1)} %get-tuple-element.61), channel_id=1, source_target_pairs={{0,8},{4,12},{8,0},{12,4},{16,24},{20,28},{24,16},{28,20},{1,9},{5... | collective-permute-start | bytes 589832 | tf_op jit(solution)/shard_map/ppermute | solution.py:38
  244.9 5.9 %collective-permute-start.42 = (bf16[192,512]{1,0:T(8,128)(2,1)S(1)}, bf16[192,512]{1,0:T(8,128)(2,1)S(1)}, u32[]{:S(2)}, u32[]{:S(2)}) collective-permute-start(bf16[192,512]{1,0:T(8,128)(2,1)S(1)} %get-tuple-element.62), channel_id=1, source_target_pairs={{0,2},{1,3},{2,0},{3,1},{4,6},{5,7},{6,4},{7,5},{8,10},{9,11},{10,... | collective-permute-start | bytes 589832 | tf_op jit(solution)/shard_map/ppermute | solution.py:33
  (12 other events, 10.9 us)
